TPU v7x, 32 devices: a whole 2x2x4 slice. The times are simulated.
32 devices in a mesh: sp: 4 (over y, x), tp: 8 (over z, core).
Axes of the slice: x: 2, y: 2, z: 4, core: 2. Of those that a mesh axis runs over, the one named last changes fastest.
Arguments:
- residual: bfloat16 [16384, 2048], P(('sp', 'tp')), may hold values from -6 to 6
- query_values: bfloat16 [16384, 1024], P('sp', 'tp'), may hold values from -6 to 6
- forget_preact: bfloat16 [16384, 1024], P('sp', 'tp'), may hold values from -6 to 6
- value_written: bfloat16 [16384, 1024], P('sp', 'tp'), may hold values from -6 to 6
- output_gate_preact: bfloat16 [16384, 1024], P('sp', 'tp'), may hold values from -6 to 6
- forget_margin: float32 [1024], P('tp'), may hold values from 0 to 0.1
- sudden_decay: float32 [16, 16384], P('tp', 'sp'), may hold values from -0.7 to 0
- head_norm_gain: float32 [64], replicated, may hold values from 0.1 to 1.9
- output_weight_matrix: bfloat16 [1024, 2048], replicated, may hold values from -0.1875 to 0.1875
- mixer_norm_gain: float32 [2048], replicated, may hold values from 0.1 to 1.9
- feedforward_gain: float32 [2048], replicated, may hold values from 0.1 to 1.9
- routed_expert_index: int32 [16384, 2], P(('sp', 'tp')), may hold values from 0 to 3, all different within a row; in each aligned block of 512 rows (0 to 511, 512 to 1023, ...) at most 384 rows name the same one
- routed_expert_weight: float32 [16384, 2], P(('sp', 'tp')), may hold values from 0.2 to 1.5
- expert_gate_matrix: bfloat16 [4, 2048, 1024], P('sp', None, 'tp'), may hold values from -0.125 to 0.125
- expert_up_matrix: bfloat16 [4, 2048, 1024], P('sp', None, 'tp'), may hold values from -0.125 to 0.125
- expert_down_matrix: bfloat16 [4, 2048, 1024], P('sp', None, 'tp'), may hold values from -0.1875 to 0.1875
- common_gate_matrix: bfloat16 [2048, 256], replicated, may hold values from -0.125 to 0.125
- common_up_matrix: bfloat16 [2048, 256], replicated, may hold values from -0.125 to 0.125
- common_down_matrix: bfloat16 [256, 2048], replicated, may hold values from -0.375 to 0.375
- final_norm_gain: float32 [2048], replicated, may hold values from 0.1 to 1.9
Outputs:
- layer_out: bfloat16 [16384, 2048], P(('sp', 'tp'))
Inputs may be any that keep to these rules, and one draw needn't show every extreme that they name: `routed_expert_index`: each row names 2 different experts. Among the rows of one device no expert is named by more than 384 rows, and in some devices' rows one expert is named by exactly 384.
All inputs are finite; a program needn't handle non-finite values.
Results may differ from a plain program's by a relative error of at most 0.0075.
Values may be sent and summed in bfloat16 or wider, within the bound.
No kernel may reach another device: no remote copies, remote signals or barrier semaphores. Data moves between devices by JAX's collectives and lax.ppermute only.
A program may use at most 128 MiB of HBM per device.

v0:
```python
import functools

import jax
import jax.numpy as jnp
from jax import lax
from jax.experimental import pallas as pl
from jax.experimental.pallas import tpu as pltpu
from jax.sharding import Mesh, PartitionSpec as P

HEAD_CHANNELS = 64
BLOCK = 64
EPS = 1e-06
TOP_PRECISION = lax.Precision.HIGHEST
F32 = jnp.float32
BF16 = jnp.bfloat16

LANES_LANES = (((1,), (1,)), ((), ()))
ROWS_ROWS = (((0,), (0,)), ((), ()))


def rms_scale(values):
    return values * lax.rsqrt(jnp.mean(values * values, axis=-1, keepdims=True) + EPS)


def mm(a, b, dims=(((1,), (0,)), ((), ()))):
    return lax.dot_general(a, b, dims, preferred_element_type=F32)


def scan_kernel(
    q_ref, f_ref, v_ref, margin_ref, sudden_ref, local_ref, lifted_ref, final_ref, state_ref, total_ref
):
    step = pl.program_id(0)
    span, channels = q_ref.shape
    heads = channels // HEAD_CHANNELS

    @pl.when(step == 0)
    def _():
        state_ref[...] = jnp.zeros_like(state_ref)
        total_ref[...] = jnp.zeros_like(total_ref)

    lane = lax.broadcasted_iota(jnp.int32, (BLOCK, channels), 1) // HEAD_CHANNELS

    def per_head(block):
        if heads == 1:
            return block
        return jnp.concatenate(
            [jnp.where(lane == h, block, jnp.zeros_like(block)) for h in range(heads)], axis=0
        )

    rows = lax.broadcasted_iota(jnp.int32, (BLOCK, heads * BLOCK), 0)
    cols = lax.broadcasted_iota(jnp.int32, (BLOCK, heads * BLOCK), 1) % BLOCK
    lower = rows >= cols
    sum_rows = lax.broadcasted_iota(jnp.int32, (BLOCK, 3 * BLOCK), 0)
    sum_cols = lax.broadcasted_iota(jnp.int32, (BLOCK, 3 * BLOCK), 1) % BLOCK
    summing = (sum_rows >= sum_cols).astype(F32).astype(BF16)
    own_head = (
        lax.broadcasted_iota(jnp.int32, (channels, channels), 0) // HEAD_CHANNELS
        == lax.broadcasted_iota(jnp.int32, (channels, channels), 1) // HEAD_CHANNELS
    )
    margin = margin_ref[...]
    sudden = sudden_ref[...]
    sudden = jnp.concatenate([sudden, jnp.zeros((8 - heads, span), F32)], axis=0).T
    state = state_ref[...]
    total = total_ref[...]
    for j in range(span // BLOCK):
        at = pl.ds(j * BLOCK, BLOCK)
        strength = margin * jax.nn.sigmoid(-f_ref[at, :].astype(F32))
        extra = sudden[j * BLOCK : (j + 1) * BLOCK]
        jump = jnp.broadcast_to(extra[:, 0:1], (BLOCK, channels))
        for h in range(1, heads):
            jump = jnp.where(lane == h, jnp.broadcast_to(extra[:, h : h + 1], (BLOCK, channels)), jump)
        keep = jnp.log1p(-strength) + jump
        top = keep.astype(BF16)
        rest = keep - top.astype(F32)
        second = rest.astype(BF16)
        third = (rest - second.astype(F32)).astype(BF16)
        running = mm(summing, jnp.concatenate([top, second, third], axis=0))
        middle = running[BLOCK // 2 - 1 : BLOCK // 2]
        closing = running[BLOCK - 1 : BLOCK]
        scaled_q = q_ref[at, :].astype(F32) * jnp.exp(running - middle)
        scaled_k = strength * jnp.exp(middle - running)
        values = v_ref[at, :]
        scores = mm(scaled_q.astype(BF16), per_head(scaled_k.astype(BF16)), LANES_LANES)
        scores = jnp.where(lower, scores, 0.0).astype(BF16)
        lifted = scaled_q * jnp.exp(middle)
        local_ref[at, :] = mm(scores, per_head(values)) + mm(
            lifted.astype(BF16), state.astype(BF16), LANES_LANES
        )
        lifted_ref[at, :] = (lifted * jnp.exp(total)).astype(BF16)
        closed_k = (scaled_k * jnp.exp(closing - middle)).astype(BF16)
        added = mm(values, closed_k, ROWS_ROWS)
        state = state * jnp.exp(closing) + jnp.where(own_head, added, 0.0)
        total = total + closing
    state_ref[...] = state
    total_ref[...] = total
    final_ref[0:channels, :] = state
    final_ref[channels:, :] = jnp.broadcast_to(jnp.exp(total), (8, channels))


def scan_call(q, f, v, margin, sudden):
    tokens, channels = q.shape
    heads = channels // HEAD_CHANNELS
    span = min(tokens, 512)
    block = pl.BlockSpec((span, channels), lambda i: (i, 0))
    return pl.pallas_call(
        scan_kernel,
        grid=(tokens // span,),
        in_specs=[
            block,
            block,
            block,
            pl.BlockSpec((1, channels), lambda i: (0, 0)),
            pl.BlockSpec((heads, span), lambda i: (0, i)),
        ],
        out_specs=[block, block, pl.BlockSpec((channels + 8, channels), lambda i: (0, 0))],
        out_shape=[
            jax.ShapeDtypeStruct((tokens, channels), F32),
            jax.ShapeDtypeStruct((tokens, channels), BF16),
            jax.ShapeDtypeStruct((channels + 8, channels), F32),
        ],
        scratch_shapes=[pltpu.VMEM((channels, channels), F32), pltpu.VMEM((1, channels), F32)],
        compiler_params=pltpu.CompilerParams(dimension_semantics=("arbitrary",)),
        cost_estimate=pl.CostEstimate(
            flops=tokens * channels * 2000, bytes_accessed=tokens * channels * 14, transcendentals=0
        ),
        name="scan",
    )(q, f, v, margin.reshape(1, channels), sudden)


def gate_kernel(mine_ref, local_ref, lifted_ref, open_ref, pieces_ref, gain_ref, mixed_ref):
    span, channels = local_ref.shape
    mine = mine_ref[0]
    incoming = jnp.zeros((channels, channels), F32)
    for j in range(pieces_ref.shape[0] - 1):
        longer = incoming * pieces_ref[j, channels : channels + 1, :] + pieces_ref[j, 0:channels, :]
        incoming = jnp.where(j < mine, longer, incoming)
    heads_out = local_ref[...] + mm(lifted_ref[...], incoming.astype(BF16), LANES_LANES)
    own_head = (
        lax.broadcasted_iota(jnp.int32, (channels, channels), 0) // HEAD_CHANNELS
        == lax.broadcasted_iota(jnp.int32, (channels, channels), 1) // HEAD_CHANNELS
    )
    averaging = jnp.where(own_head, 1.0 / HEAD_CHANNELS, 0.0).astype(BF16)
    square = heads_out * heads_out
    top = square.astype(BF16)
    rest = (square - top.astype(F32)).astype(BF16)
    mean = mm(top, averaging) + mm(rest, averaging)
    opening = jax.nn.sigmoid(open_ref[...].astype(F32))
    mixed_ref[...] = (heads_out * lax.rsqrt(mean + EPS) * gain_ref[...] * opening).astype(BF16)


def gate_call(mine, local, lifted, opening, pieces, gain):
    tokens, channels = local.shape
    span = min(tokens, 1024)
    block = pl.BlockSpec((span, channels), lambda i: (i, 0))
    return pl.pallas_call(
        gate_kernel,
        grid=(tokens // span,),
        in_specs=[
            pl.BlockSpec(memory_space=pltpu.SMEM),
            block,
            block,
            block,
            pl.BlockSpec(pieces.shape, lambda i: (0, 0, 0)),
            pl.BlockSpec((1, channels), lambda i: (0, 0)),
        ],
        out_specs=block,
        out_shape=jax.ShapeDtypeStruct((tokens, channels), BF16),
        compiler_params=pltpu.CompilerParams(dimension_semantics=("arbitrary",)),
        cost_estimate=pl.CostEstimate(
            flops=tokens * channels * 800, bytes_accessed=tokens * channels * 10, transcendentals=0
        ),
        name="gate",
    )(mine, local, lifted, opening, pieces, gain)


def project_kernel(mixed_ref, weight_ref, residual_ref, mixer_ref, gain_ref, stream_ref, normed_ref):
    mixed = jnp.concatenate([mixed_ref[j] for j in range(mixed_ref.shape[0])], axis=1)
    projected = mm(mixed, weight_ref[...]).astype(BF16).astype(F32)
    stream = (residual_ref[...].astype(F32) + rms_scale(projected) * mixer_ref[...]).astype(BF16)
    stream_ref[...] = stream
    normed_ref[...] = (rms_scale(stream.astype(F32)) * gain_ref[...]).astype(BF16)


def project_call(mixed, weight, residual, mixer_gain, gain):
    sources, rows, channels = mixed.shape
    width = weight.shape[1]
    span = min(rows, 256)
    block = pl.BlockSpec((span, width), lambda i: (i, 0))
    vector = pl.BlockSpec((1, width), lambda i: (0, 0))
    return pl.pallas_call(
        project_kernel,
        grid=(rows // span,),
        in_specs=[
            pl.BlockSpec((sources, span, channels), lambda i: (0, i, 0)),
            pl.BlockSpec(weight.shape, lambda i: (0, 0)),
            block,
            vector,
            vector,
        ],
        out_specs=[block, block],
        out_shape=[jax.ShapeDtypeStruct((rows, width), BF16)] * 2,
        compiler_params=pltpu.CompilerParams(dimension_semantics=("arbitrary",)),
        cost_estimate=pl.CostEstimate(
            flops=2 * rows * width * weight.shape[0],
            bytes_accessed=2 * weight.size + 8 * rows * width,
            transcendentals=0,
        ),
        name="project",
    )(mixed, weight, residual, mixer_gain.reshape(1, width), gain.reshape(1, width))


def expert_kernel(rows_ref, share_ref, weights_ref, out_ref, sum_ref):
    expert, piece = pl.program_id(0), pl.program_id(1)
    first = jnp.logical_and(expert == 0, piece == 0)
    last = jnp.logical_and(expert == pl.num_programs(0) - 1, piece == pl.num_programs(1) - 1)
    rows = rows_ref[...]

    def joined(which):
        return jnp.concatenate([weights_ref[0, j, which] for j in range(weights_ref.shape[1])], axis=1)

    share = share_ref[...]
    lanes = lax.broadcasted_iota(jnp.int32, share.shape, 1)
    share = jnp.sum(jnp.where(lanes == expert, share, 0.0), axis=1, keepdims=True)
    gate = mm(rows, joined(0))
    up = mm(rows, joined(1))
    hidden = (gate * jax.nn.sigmoid(gate) * up * share).astype(BF16)
    added = mm(hidden, joined(2), LANES_LANES)

    @pl.when(first)
    def _():
        sum_ref[...] = added

    @pl.when(jnp.logical_not(first))
    def _():
        sum_ref[...] += added

    @pl.when(last)
    def _():
        out_ref[...] = sum_ref[...].astype(out_ref.dtype)


def expert_call(rows, share, weights, kind, name):
    count, width = rows.shape
    experts, shards, parts, _, units = weights.shape
    together = 2
    return pl.pallas_call(
        expert_kernel,
        grid=(experts, shards // together),
        in_specs=[
            pl.BlockSpec((count, width), lambda e, s: (0, 0)),
            pl.BlockSpec(share.shape, lambda e, s: (0, 0)),
            pl.BlockSpec((1, together, parts, width, units), lambda e, s: (e, s, 0, 0, 0)),
        ],
        out_specs=pl.BlockSpec((count, width), lambda e, s: (0, 0)),
        out_shape=jax.ShapeDtypeStruct((count, width), kind),
        scratch_shapes=[pltpu.VMEM((count, width), F32)],
        compiler_params=pltpu.CompilerParams(
            dimension_semantics=("arbitrary", "arbitrary"), vmem_limit_bytes=48 * 1024 * 1024
        ),
        cost_estimate=pl.CostEstimate(
            flops=2 * count * weights.size, bytes_accessed=2 * weights.size, transcendentals=0
        ),
        name=name,
    )(rows, share, weights)


def shared_expert(normed, gate_w, up_w, down_w):
    hidden = (
        jax.nn.silu(jnp.dot(normed, gate_w, preferred_element_type=F32))
        * jnp.dot(normed, up_w, preferred_element_type=F32)
    ).astype(BF16)
    return jnp.dot(hidden, down_w, preferred_element_type=F32)


def expert_rows(slot_rows, gate_w, up_w, down_w):
    hidden = (
        jax.nn.silu(jnp.dot(slot_rows, gate_w, preferred_element_type=F32))
        * jnp.dot(slot_rows, up_w, preferred_element_type=F32)
    ).astype(BF16)
    return lax.dot_general(hidden, down_w, LANES_LANES, preferred_element_type=F32)


def routed_by_slots(normed, index, weight, gate_w, up_w, down_w, sp):
    rows_here, routes_each = index.shape
    experts_all = lax.axis_size(sp)
    capacity = 3 * rows_here * routes_each // (2 * experts_all)
    numbers = jnp.arange(experts_all, dtype=jnp.int32)
    matches = (index[:, :, None] == numbers).astype(F32)
    hits = jnp.sum(matches, axis=1)
    strictly_lower = jnp.tril(jnp.ones((rows_here, rows_here), F32), -1)
    before_hits = jnp.dot(strictly_lower, hits, precision=TOP_PRECISION)
    slots = jnp.sum(before_hits[:, None, :] * matches, axis=2).astype(jnp.int32)
    targets = index * capacity + slots
    slot_numbers = jnp.arange(experts_all * capacity, dtype=jnp.int32)
    selector = (targets[:, :, None] == slot_numbers).astype(BF16)
    outgoing = jnp.einsum("rks,rd->sd", selector, normed, preferred_element_type=F32)
    outgoing = outgoing.astype(BF16).reshape(experts_all, capacity, normed.shape[1])
    arrived = lax.all_to_all(outgoing, sp, split_axis=0, concat_axis=0, tiled=True)
    sources, items, width = arrived.shape
    slot_rows = arrived.reshape(sources * items, width)
    gate_piece = lax.all_gather(gate_w, "tp", axis=2, tiled=True)[0]
    up_piece = lax.all_gather(up_w, "tp", axis=2, tiled=True)[0]
    down_piece = lax.all_gather(down_w, "tp", axis=2, tiled=True)[0]
    produced = expert_rows(slot_rows, gate_piece, up_piece, down_piece)
    results = produced.astype(BF16).reshape(sources, items, width)
    answered = lax.all_to_all(results, sp, split_axis=0, concat_axis=0, tiled=True)
    flat_answers = answered.reshape(experts_all * capacity, normed.shape[1])
    per_route = jnp.einsum("rks,sd->rkd", selector, flat_answers, preferred_element_type=F32)
    return jnp.sum(per_route * weight[:, :, None], axis=1)


def body(
    residual,
    query_values,
    forget_preact,
    value_written,
    output_gate_preact,
    forget_margin,
    sudden_decay,
    head_norm_gain,
    output_weight_matrix,
    mixer_norm_gain,
    feedforward_gain,
    routed_expert_index,
    routed_expert_weight,
    expert_gate_matrix,
    expert_up_matrix,
    expert_down_matrix,
    common_gate_matrix,
    common_up_matrix,
    common_down_matrix,
    final_norm_gain,
    *,
    sp,
):
    tokens, channels = query_values.shape
    rows = residual.shape[0]
    peers = lax.axis_size("tp")
    paired = len(sp) == 2
    if paired:
        outer, inner = sp
        packed = jnp.concatenate([expert_gate_matrix, expert_up_matrix, expert_down_matrix], axis=0)
        held = lax.all_gather(packed, (inner, "tp"))
        held = held.reshape((lax.axis_size(inner), peers) + packed.shape)
        experts_all = lax.axis_size(outer) * lax.axis_size(inner)
        numbers = jnp.arange(experts_all, dtype=jnp.int32)
        share = jnp.sum(
            (routed_expert_index[:, :, None] == numbers) * routed_expert_weight[:, :, None], axis=1
        )
        share = share.reshape(rows, lax.axis_size(outer), lax.axis_size(inner))
        swap = [(0, 1), (1, 0)]
        here = lax.axis_index(outer)
        own_share = jnp.where(here == 0, share[:, 0], share[:, 1])
        far_share = lax.ppermute(jnp.where(here == 0, share[:, 1], share[:, 0]), outer, swap)

    local, lifted, final = scan_call(
        query_values, forget_preact, value_written, forget_margin, sudden_decay
    )
    pieces = lax.all_gather(final, sp)
    mine = lax.axis_index(sp).reshape(1)
    gain = jnp.tile(head_norm_gain, channels // HEAD_CHANNELS).reshape(1, channels)
    mixed = gate_call(mine, local, lifted, output_gate_preact, pieces, gain)
    mixed = lax.all_to_all(
        mixed.reshape(peers, tokens // peers, channels), "tp", split_axis=0, concat_axis=0, tiled=True
    )
    if channels % 128 == 0:
        stream, normed = project_call(
            mixed, output_weight_matrix, residual, mixer_norm_gain, feedforward_gain
        )
    else:
        mixed = mixed.transpose(1, 0, 2).reshape(rows, peers * channels)
        projected = jnp.dot(mixed, output_weight_matrix, preferred_element_type=F32).astype(BF16)
        stream = (residual.astype(F32) + rms_scale(projected.astype(F32)) * mixer_norm_gain).astype(BF16)
        normed = (rms_scale(stream.astype(F32)) * feedforward_gain).astype(BF16)
    shared = shared_expert(normed, common_gate_matrix, common_up_matrix, common_down_matrix)
    if not paired:
        routed = routed_by_slots(
            normed,
            routed_expert_index,
            routed_expert_weight,
            expert_gate_matrix,
            expert_up_matrix,
            expert_down_matrix,
            sp,
        )
        layer_out = stream.astype(F32) + rms_scale(shared + routed) * final_norm_gain
        return layer_out.astype(BF16)
    far_rows = lax.ppermute(normed, outer, swap)
    chunks = 2
    part = rows // chunks
    answers = []
    for c in range(chunks):
        cut = slice(c * part, (c + 1) * part)
        partial = expert_call(far_rows[cut], far_share[cut], held, BF16, "far%d" % c)
        answers.append(lax.ppermute(partial, outer, swap))
    own = expert_call(normed, own_share, held, F32, "own")
    base = shared + own
    outs = []
    for c in range(chunks):
        cut = slice(c * part, (c + 1) * part)
        summed = base[cut] + answers[c].astype(F32)
        outs.append((stream[cut].astype(F32) + rms_scale(summed) * final_norm_gain).astype(BF16))
    return jnp.concatenate(outs, axis=0)


def solution(mesh):
    sp_size, tp_size = mesh.shape["sp"], mesh.shape["tp"]
    if sp_size == 4:
        sp = ("far", "near")
        mesh = Mesh(mesh.devices.reshape(2, 2, tp_size), sp + ("tp",))
    else:
        sp = ("sp",)
    every = P(sp + ("tp",), None)
    split = P(sp, "tp")
    shard = P(sp, None, "tp")
    placed = (
        every,
        split,
        split,
        split,
        split,
        P("tp"),
        P("tp", sp),
        P(),
        P(),
        P(),
        P(),
        every,
        every,
        shard,
        shard,
        shard,
        P(),
        P(),
        P(),
        P(),
    )
    return jax.shard_map(
        functools.partial(body, sp=sp), mesh=mesh, in_specs=placed, out_specs=every, check_vma=False
    )
```

profile of v0, /device:TPU:8, one launch (start us, length us, event | category | flops | bytes accessed | tf_op | source)
XLA Modules:
  0.0 239.9 jit_solution(3775572890237823459)
XLA Ops:
  6.5 0.0 copy-start
  6.5 0.0 copy-start.10
  6.5 0.0 all-gather.4.cloned.1.call-start
  6.5 2.8 %pad_maximum_fusion.1 = bf16[3,2048,128]{2,1,0:T(8,128)(2,1)} fusion(bf16[1,2048,128]{2,1,0:T(8,128)(2,1)} %param.35, bf16[1,2048,128]{2,1,0:T(8,128)(2,1)} %param.34, bf16[1,2048,128]{2,1,0:T(8,128)(2,1)} %param.33), kind=kLoop, calls=%fused_computation.8 | loop fusion | flops 1572864 | bytes 3145728 | tf_op jit(solution)/shard_map/concatenate | solution.py:342
  9.3 0.0 all-gather.4.cloned.1.call-update
  9.3 0.0 copy-done.10
  9.4 0.6 reshape_tile.3.gain_ref
  10.0 18.8 %scan.1 = (f32[4096,128]{1,0:T(8,128)}, bf16[4096,128]{1,0:T(8,128)(2,1)}, f32[136,128]{1,0:T(8,128)}) custom-call(bf16[4096,128]{1,0:T(8,128)(2,1)} %q_ref.1, bf16[4096,128]{1,0:T(8,128)(2,1)} %f_ref.1, bf16[4096,128]{1,0:T(8,128)(2,1)} %v_ref.1, f32[1,128]{1,0:T(1,128)} %bitcast.25, f32[2,4096]{1,0:T(2,128)} %sudden_ref.1), custom_call_target="tpu_custom_call" | custom-call | flops 1048576000 | bytes 7340032 | tf_op jit(solution)/shard_map/scan/pallas_call | solution.py:105
  28.8 10.7 %all-gather = f32[544,128]{1,0:T(8,128)} all-gather(f32[136,128]{1,0:T(8,128)} %get-tuple-element.12), channel_id=2, replica_groups=mesh['far'=2,'near'=2,'tp'=8] {'far','near'}, dimensions={0}, use_global_device_ids=true | all-gather | bytes 348160 | tf_op jit(solution)/shard_map/all_gather | solution.py:359
  39.5 5.2 %gate.1 = bf16[4096,128]{1,0:T(8,128)(2,1)} custom-call(s32[1]{0:T(128)} %bitcast.mine_ref, f32[4096,128]{1,0:T(8,128)} %get-tuple-element.10.local_ref, bf16[4096,128]{1,0:T(8,128)(2,1)} %get-tuple-element.11.lifted_ref, bf16[4096,128]{1,0:T(8,128)(2,1)} %open_ref.1, f32[4,136,128]{2,1,0:T(8,128)} %bitcast.22, f32[1,128]{1,0:T(1,128)} %reshape_tile.3.gain_ref), custom_call_target="tpu_custom_call" | custom-call | flops 419430400 | bytes 5242880 | tf_op jit(solution)/shard_map/gate/pallas_call | solution.py:155
  44.7 45.0 %all_to_all.5.mixed_ref = bf16[8,512,128]{2,1,0:T(8,128)(2,1)} all-to-all(bf16[8,512,128]{2,1,0:T(8,128)(2,1)} %bitcast.21), channel_id=1, replica_groups=mesh['far'=2,'near'=2,'tp'=8] {'tp'}, dimensions={0} | all-to-all | bytes 2097152 | tf_op jit(solution)/shard_map/all_to_all | solution.py:363
  89.7 0.0 copy-start.8
  89.7 0.0 copy-start.9
  89.7 8.0 %project.1 = (bf16[512,2048]{1,0:T(8,128)(2,1)}, bf16[512,2048]{1,0:T(8,128)(2,1)}) custom-call(bf16[8,512,128]{2,1,0:T(8,128)(2,1)} %all_to_all.5.mixed_ref, bf16[1024,2048]{1,0:T(8,128)(2,1)} %weight_ref.1, bf16[512,2048]{1,0:T(8,128)(2,1)} %residual_ref.1, f32[1,2048]{1,0:T(1,128)} %bitcast.23, f32[1,2048]{1,0:T(1,128)} %bitcast.24), custom_call_target="tpu_custom_call" | custom-call | flops 2147483648 | bytes 12582912 | tf_op jit(solution)/shard_map/project/pallas_call | solution.py:190
  97.7 0.0 copy-start.1
  97.7 1.4 collective-permute-start
  99.1 0.0 copy-done.8
  99.1 0.0 copy-done.9
  99.1 0.1 copy.33
  99.3 0.9 copy.34
  100.1 1.7 select_bitcast_fusion.1
  101.8 0.7 collective-permute-start.1
  102.5 48.3 %collective-permute-done.1 = f32[512,2]{1,0:T(8,128)S(1)} collective-permute-done((f32[512,2]{1,0:T(8,128)S(1)}, f32[512,2]{1,0:T(8,128)S(1)}, u32[]{:S(2)}, u32[]{:S(2)}) %collective-permute-start.1) | collective-permute-done | bytes 4128 | tf_op jit(solution)/shard_map/ppermute | solution.py:354
  150.8 0.0 copy-done.1
  150.8 2.7 %fusion.11 = f32[512,256]{1,0:T(8,128)} fusion(bf16[512,2048]{1,0:T(8,128)(2,1)S(1)} %copy-done.1, bf16[2048,256]{1,0:T(8,128)(2,1)} %param.36), kind=kOutput, calls=%fused_computation.27 | convolution fusion | flops 536870912 | bytes 3670016 | tf_op jit(solution)/shard_map/dot_general | solution.py:269
  153.5 0.0 collective-permute-done
  153.5 1.7 fusion.8
  155.2 6.4 %all-gather.4.cloned.1.call-done = bf16[48,2048,128]{2,1,0:T(8,128)(2,1)} async-done(((bf16[3,2048,128]{2,1,0:T(8,128)(2,1)}), bf16[48,2048,128]{2,1,0:T(8,128)(2,1)}) %all-gather.4.cloned.1.call-update) | async-done | bytes 25165840 | tf_op jit(solution)/shard_map/all_gather | solution.py:343
  161.6 15.3 %far1.1 = bf16[256,2048]{1,0:T(8,128)(2,1)} custom-call(bf16[256,2048]{1,0:T(8,128)(2,1)S(1)} %get-tuple-element.20.rows_ref, f32[256,2]{1,0:T(8,128)S(1)} %get-tuple-element.24.share_ref, bf16[2,8,3,2048,128]{4,3,2,1,0:T(8,128)(2,1)} %bitcast.18), custom_call_target="tpu_custom_call" | custom-call | flops 6442450944 | bytes 25165824 | tf_op jit(solution)/shard_map/far1/pallas_call | solution.py:246
  177.0 1.5 collective-permute-start.3
  178.5 0.0 copy-start.2
  178.5 0.0 copy-start.4
  178.5 15.5 %far0.1 = bf16[256,2048]{1,0:T(8,128)(2,1)} custom-call(bf16[256,2048]{1,0:T(8,128)(2,1)S(1)} %get-tuple-element.19.rows_ref, f32[256,2]{1,0:T(8,128)S(1)} %get-tuple-element.23.share_ref, bf16[2,8,3,2048,128]{4,3,2,1,0:T(8,128)(2,1)} %bitcast.19), custom_call_target="tpu_custom_call" | custom-call | flops 6442450944 | bytes 25165824 | tf_op jit(solution)/shard_map/far0/pallas_call | solution.py:246
  194.0 0.5 collective-permute-start.2
  194.5 0.0 copy-done.2
  194.5 0.0 copy-done.4
  194.5 0.0 copy-start.3
  194.5 21.9 %own.1 = f32[512,2048]{1,0:T(8,128)} custom-call(bf16[512,2048]{1,0:T(8,128)(2,1)S(1)} %copy-done.2, f32[512,2]{1,0:T(8,128)S(1)} %copy-done.4, bf16[2,8,3,2048,128]{4,3,2,1,0:T(8,128)(2,1)} %bitcast.20), custom_call_target="tpu_custom_call" | custom-call | flops 12884901888 | bytes 25165824 | tf_op jit(solution)/shard_map/own/pallas_call | solution.py:246
  216.4 0.0 copy-done
  216.4 0.0 copy-done.3
  216.4 7.0 %convolution_add_fusion = f32[512,2048]{1,0:T(8,128)} fusion(f32[512,2048]{1,0:T(8,128)} %own.1, bf16[256,2048]{1,0:T(8,128)(2,1)S(1)} %copy-done, bf16[512,2048]{1,0:T(8,128)(2,1)S(1)} %copy-done.3, bf16[2048,256]{1,0:T(8,128)(2,1)} %param.37, f32[512,256]{1,0:T(8,128)} %fusion.11), kind=kOutput, calls=%fused_computation | convolution fusion | flops 1075576832 | bytes 13107200 | tf_op jit(solution)/shard_map/dot_general | solution.py:272
  223.3 0.0 copy-start.5
  223.3 0.0 copy-start.6
  223.3 0.0 copy-start.7
  223.3 0.0 collective-permute-done.3
  223.3 1.8 collective-permute-done.2
  225.1 3.5 %multiply_reduce_fusion.1 = (f32[256]{0:T(256)S(1)}, f32[256]{0:T(256)S(1)}) fusion(bf16[256,2048]{1,0:T(8,128)(2,1)} %collective-permute-done.2, f32[512,2048]{1,0:T(8,128)} %convolution_add_fusion, bf16[256,2048]{1,0:T(8,128)(2,1)} %collective-permute-done.3), kind=kLoop, calls=%fused_computation.7 | loop fusion | flops 4193792 | bytes 6293504 | tf_op jit(solution)/shard_map/reduce_sum | solution.py:22
  228.6 0.0 copy-done.5
  228.6 0.0 copy-done.6
  228.6 0.0 copy-done.7
  228.7 3.0 %add_convert_fusion.1 = (bf16[256,2048]{1,0:T(8,128)(2,1)S(1)}, bf16[256,2048]{1,0:T(8,128)(2,1)S(1)}) fusion(bf16[256,2048]{1,0:T(8,128)(2,1)} %collective-permute-done.2, f32[512,2048]{1,0:T(8,128)S(1)} %copy-done.5, f32[2048]{0:T(1024)S(1)} %copy-done.7, f32[256]{0:T(256)S(1)} %get-tuple-element.28, bf16[512,2048]{1,0:T(8,128)(2,1)S(1)} %copy-done.6, ...), kind=kLoop, calls=%fused_computation.6 | loop fusion | flops 7340032 | bytes 10496000 | tf_op jit(solution)/shard_map/convert_element_type | solution.py:402
  231.6 1.5 pad_maximum_fusion
  (6 shorter events, 0.1 us)
Async XLA Ops:
  6.5 209.8 %copy-start = (bf16[256,2048]{1,0:T(8,128)(2,1)S(1)}, bf16[256,2048]{1,0:T(8,128)(2,1)}, u32[]{:S(2)}) copy-start(bf16[256,2048]{1,0:T(8,128)(2,1)} %param.38) | copy-start | bytes 3145732
  6.5 2.8 %copy-start.10 = (f32[64]{0:T(128)S(1)}, f32[64]{0:T(128)}, u32[]{:S(2)}) copy-start(f32[64]{0:T(128)} %param.27) | copy-start | bytes 772
  6.5 155.1 %all-gather.4.cloned.1.call-start = ((), (), s32[]{:S(2)}) async-start(), calls=%async_computation.1 | async-start | bytes 26738688 | tf_op jit(solution)/shard_map/all_gather | solution.py:343
  89.7 9.3 %copy-start.8 = (f32[512,2]{0,1:T(2,128)S(1)}, f32[512,2]{0,1:T(2,128)}, u32[]{:S(2)}) copy-start(f32[512,2]{0,1:T(2,128)} %param.32) | copy-start | bytes 12292
  89.7 9.3 %copy-start.9 = (s32[512,2]{0,1:T(2,128)S(1)}, s32[512,2]{0,1:T(2,128)}, u32[]{:S(2)}) copy-start(s32[512,2]{0,1:T(2,128)} %param.31) | copy-start | bytes 12292
  97.7 53.1 %copy-start.1 = (bf16[512,2048]{1,0:T(8,128)(2,1)S(1)}, bf16[512,2048]{1,0:T(8,128)(2,1)}, u32[]{:S(2)}) copy-start(bf16[512,2048]{1,0:T(8,128)(2,1)} %get-tuple-element.14.rows_ref) | copy-start | bytes 6291460
  97.7 55.8 %collective-permute-start = (bf16[512,2048]{1,0:T(8,128)(2,1)}, bf16[512,2048]{1,0:T(8,128)(2,1)}, u32[]{:S(2)}, u32[]{:S(2)}) collective-permute-start(bf16[512,2048]{1,0:T(8,128)(2,1)} %get-tuple-element.14.rows_ref), channel_id=1, source_target_pairs={{0,16},{16,0},{1,17},{17,1},{2,18},{18,2},{3,19},{19,3},{4,20},{20... | collective-permute-start | bytes 6291464 | tf_op jit(solution)/shard_map/ppermute | solution.py:388
  101.8 48.9 %collective-permute-start.1 = (f32[512,2]{1,0:T(8,128)S(1)}, f32[512,2]{1,0:T(8,128)S(1)}, u32[]{:S(2)}, u32[]{:S(2)}) collective-permute-start(f32[512,2]{1,0:T(8,128)S(1)} %get-tuple-element.22), channel_id=1, source_target_pairs={{0,16},{16,0},{1,17},{17,1},{2,18},{18,2},{3,19},{19,3},{4,20},{20... | collective-permute-start | bytes 12296 | tf_op jit(solution)/shard_map/ppermute | solution.py:354
  177.0 46.3 %collective-permute-start.3 = (bf16[256,2048]{1,0:T(8,128)(2,1)}, bf16[256,2048]{1,0:T(8,128)(2,1)}, u32[]{:S(2)}, u32[]{:S(2)}) collective-permute-start(bf16[256,2048]{1,0:T(8,128)(2,1)} %far1.1), channel_id=1, source_target_pairs={{0,16},{16,0},{1,17},{17,1},{2,18},{18,2},{3,19},{19,3},{4,20},{20... | collective-permute-start | bytes 3145736 | tf_op jit(solution)/shard_map/ppermute | solution.py:395
  178.5 16.0 %copy-start.2 = (bf16[512,2048]{1,0:T(8,128)(2,1)S(1)}, bf16[512,2048]{1,0:T(8,128)(2,1)}, u32[]{:S(2)}) copy-start(bf16[512,2048]{1,0:T(8,128)(2,1)} %get-tuple-element.14.rows_ref) | copy-start | bytes 6291460
  178.5 16.0 %copy-start.4 = (f32[512,2]{1,0:T(8,128)S(1)}, f32[512,2]{1,0:T(8,128)}, u32[]{:S(2)}) copy-start(f32[512,2]{1,0:T(8,128)} %get-tuple-element.21.share_ref) | copy-start | bytes 12292
  194.0 31.1 %collective-permute-start.2 = (bf16[256,2048]{1,0:T(8,128)(2,1)}, bf16[256,2048]{1,0:T(8,128)(2,1)}, u32[]{:S(2)}, u32[]{:S(2)}) collective-permute-start(bf16[256,2048]{1,0:T(8,128)(2,1)} %far0.1), channel_id=1, source_target_pairs={{0,16},{16,0},{1,17},{17,1},{2,18},{18,2},{3,19},{19,3},{4,20},{20... | collective-permute-start | bytes 3145736 | tf_op jit(solution)/shard_map/ppermute | solution.py:395
  194.5 21.9 %copy-start.3 = (bf16[512,2048]{1,0:T(8,128)(2,1)S(1)}, bf16[512,2048]{1,0:T(8,128)(2,1)}, u32[]{:S(2)}) copy-start(bf16[512,2048]{1,0:T(8,128)(2,1)} %get-tuple-element.14.rows_ref) | copy-start | bytes 6291460
  223.3 5.3 %copy-start.5 = (f32[512,2048]{1,0:T(8,128)S(1)}, f32[512,2048]{1,0:T(8,128)}, u32[]{:S(2)}) copy-start(f32[512,2048]{1,0:T(8,128)} %convolution_add_fusion) | copy-start | bytes 12582916
  223.3 5.3 %copy-start.6 = (bf16[512,2048]{1,0:T(8,128)(2,1)S(1)}, bf16[512,2048]{1,0:T(8,128)(2,1)}, u32[]{:S(2)}) copy-start(bf16[512,2048]{1,0:T(8,128)(2,1)} %get-tuple-element.13) | copy-start | bytes 6291460
  223.3 5.3 %copy-start.7 = (f32[2048]{0:T(1024)S(1)}, f32[2048]{0:T(1024)}, u32[]{:S(2)}) copy-start(f32[2048]{0:T(1024)} %param.39) | copy-start | bytes 24580
Sparse Core Ops, SparseCore 0:
  9.5 152.1 all-gather.3
where the time goes:
time: 241 us; the launch traced here: 240 us
  Pallas kernels  84.7 us (35%)
  waiting for transfers between devices  56.5 us (23%)
  blocking collectives  55.7 us (23%)
  between operations  13.5 us (6%)
  other arithmetic  12.4 us (5%)
  matrix products  9.7 us (4%)
  starting transfers between devices  4.06 us (2%)
  local copies, waits for them, and re-layouts  3.41 us (1%)
    pallas_call x3, Pallas kernels, expert_call(): pl.pallas_call(expert_kernel, grid=(experts, shards // together), in_spec...  52.7 us
    ppermute x1, waiting for transfers between devices, body(): lax.ppermute(jnp.where(here == 0, share[:, 1], share[:, 0]), outer, swap)  48.3 us
    all_to_all x1, blocking collectives, body(): lax.all_to_all(mixed.reshape(peers, tokens // peers, channels), 'tp', spl...  45 us
    pallas_call x1, Pallas kernels, scan_call(): pl.pallas_call(scan_kernel, grid=(tokens // span,), in_specs=[block, bloc...  18.8 us
    all_gather x1, blocking collectives, body(): pieces = lax.all_gather(final, sp)  10.7 us
    pallas_call x1, Pallas kernels, project_call(): pl.pallas_call(project_kernel, grid=(rows // span,), in_specs=[pl.BlockSp...  7.97 us
    dot_general x1, matrix products, shared_expert(): return jnp.dot(hidden, down_w, preferred_element_type=F32)  6.95 us
    all_gather x1, waiting for transfers between devices, body(): held = lax.all_gather(packed, (inner, 'tp'))  6.43 us
  transfers between devices with their start and end apart: 5, of which 3 were waited for; matrix products, arithmetic and copies ran while one was open for 6% of the time, Pallas kernels for 29%

commit v1 on v0

--- a/solution.py
+++ b/solution.py
@@ -24,6 +24,21 @@
 
 def mm(a, b, dims=(((1,), (0,)), ((), ()))):
     return lax.dot_general(a, b, dims, preferred_element_type=F32)
+
+
+def halves(value):
+    top = value.astype(BF16)
+    return top, (value - top.astype(F32)).astype(BF16)
+
+
+def fine_mm(a, b):
+    a_top, a_rest = a
+    b_top, b_rest = b
+    return mm(
+        jnp.concatenate([a_top, a_rest, a_top], axis=1),
+        jnp.concatenate([b_top, b_top, b_rest], axis=1),
+        LANES_LANES,
+    )
 
 
 def scan_kernel(
@@ -80,15 +95,17 @@
         scaled_q = q_ref[at, :].astype(F32) * jnp.exp(running - middle)
         scaled_k = strength * jnp.exp(middle - running)
         values = v_ref[at, :]
-        scores = mm(scaled_q.astype(BF16), per_head(scaled_k.astype(BF16)), LANES_LANES)
-        scores = jnp.where(lower, scores, 0.0).astype(BF16)
+        k_top, k_rest = halves(scaled_k)
+        scores = fine_mm(halves(scaled_q), (per_head(k_top), per_head(k_rest)))
+        score_top, score_rest = halves(jnp.where(lower, scores, 0.0))
+        spread = per_head(values)
         lifted = scaled_q * jnp.exp(middle)
-        local_ref[at, :] = mm(scores, per_head(values)) + mm(
-            lifted.astype(BF16), state.astype(BF16), LANES_LANES
-        )
-        lifted_ref[at, :] = (lifted * jnp.exp(total)).astype(BF16)
-        closed_k = (scaled_k * jnp.exp(closing - middle)).astype(BF16)
-        added = mm(values, closed_k, ROWS_ROWS)
+        local_ref[at, :] = mm(
+            jnp.concatenate([score_top, score_rest], axis=1), jnp.concatenate([spread, spread], axis=0)
+        ) + fine_mm(halves(lifted), halves(state))
+        lifted_ref[at, :] = lifted * jnp.exp(total)
+        closed_k = jnp.concatenate(halves(scaled_k * jnp.exp(closing - middle)), axis=0)
+        added = mm(jnp.concatenate([values, values], axis=0), closed_k, ROWS_ROWS)
         state = state * jnp.exp(closing) + jnp.where(own_head, added, 0.0)
         total = total + closing
     state_ref[...] = state
@@ -115,7 +132,7 @@
         out_specs=[block, block, pl.BlockSpec((channels + 8, channels), lambda i: (0, 0))],
         out_shape=[
             jax.ShapeDtypeStruct((tokens, channels), F32),
-            jax.ShapeDtypeStruct((tokens, channels), BF16),
+            jax.ShapeDtypeStruct((tokens, channels), F32),
             jax.ShapeDtypeStruct((channels + 8, channels), F32),
         ],
         scratch_shapes=[pltpu.VMEM((channels, channels), F32), pltpu.VMEM((1, channels), F32)],
@@ -134,7 +151,7 @@
     for j in range(pieces_ref.shape[0] - 1):
         longer = incoming * pieces_ref[j, channels : channels + 1, :] + pieces_ref[j, 0:channels, :]
         incoming = jnp.where(j < mine, longer, incoming)
-    heads_out = local_ref[...] + mm(lifted_ref[...], incoming.astype(BF16), LANES_LANES)
+    heads_out = local_ref[...] + fine_mm(halves(lifted_ref[...]), halves(incoming))
     own_head = (
         lax.broadcasted_iota(jnp.int32, (channels, channels), 0) // HEAD_CHANNELS
         == lax.broadcasted_iota(jnp.int32, (channels, channels), 1) // HEAD_CHANNELS
@@ -209,47 +226,68 @@
     )(mixed, weight, residual, mixer_gain.reshape(1, width), gain.reshape(1, width))
 
 
+def pack_kernel(gate_ref, up_ref, down_ref, packed_ref):
+    width, units = gate_ref.shape[1:]
+    packed_ref[0:width, 0:units] = gate_ref[0]
+    packed_ref[0:width, units:] = up_ref[0]
+    for j in range(width // (2 * units)):
+        turned = down_ref[0, j * 2 * units : (j + 1) * 2 * units, :].T
+        packed_ref[width + j * units : width + (j + 1) * units, :] = turned
+
+
+def pack_call(gate, up, down):
+    _, width, units = gate.shape
+    return pl.pallas_call(
+        pack_kernel,
+        out_shape=jax.ShapeDtypeStruct((width + width // 2, 2 * units), gate.dtype),
+        cost_estimate=pl.CostEstimate(flops=0, bytes_accessed=12 * width * units, transcendentals=0),
+        name="pack",
+    )(gate, up, down)
+
+
 def expert_kernel(rows_ref, share_ref, weights_ref, out_ref, sum_ref):
     expert, piece = pl.program_id(0), pl.program_id(1)
     first = jnp.logical_and(expert == 0, piece == 0)
     last = jnp.logical_and(expert == pl.num_programs(0) - 1, piece == pl.num_programs(1) - 1)
-    rows = rows_ref[...]
-
-    def joined(which):
-        return jnp.concatenate([weights_ref[0, j, which] for j in range(weights_ref.shape[1])], axis=1)
+    count, width = rows_ref.shape
+    shards, _, double = weights_ref.shape[1:]
+    units = double // 2
+
+    @pl.when(first)
+    def _():
+        sum_ref[...] = jnp.zeros_like(sum_ref)
 
     share = share_ref[...]
     lanes = lax.broadcasted_iota(jnp.int32, share.shape, 1)
     share = jnp.sum(jnp.where(lanes == expert, share, 0.0), axis=1, keepdims=True)
-    gate = mm(rows, joined(0))
-    up = mm(rows, joined(1))
-    hidden = (gate * jax.nn.sigmoid(gate) * up * share).astype(BF16)
-    added = mm(hidden, joined(2), LANES_LANES)
-
-    @pl.when(first)
-    def _():
-        sum_ref[...] = added
-
-    @pl.when(jnp.logical_not(first))
-    def _():
-        sum_ref[...] += added
+    hidden = []
+    for j in range(shards):
+        both = mm(rows_ref[...], weights_ref[0, j, 0:width, :])
+        gate, up = both[:, :units], both[:, units:]
+        hidden.append((gate * jax.nn.sigmoid(gate) * up * share).astype(BF16))
+    hidden = jnp.concatenate(hidden, axis=1)
+    for c in range(width // double):
+        at = slice(width + c * units, width + (c + 1) * units)
+        down = jnp.concatenate([weights_ref[0, j, at, :] for j in range(shards)], axis=0)
+        sum_ref[:, c * double : (c + 1) * double] += mm(hidden, down)
 
     @pl.when(last)
     def _():
         out_ref[...] = sum_ref[...].astype(out_ref.dtype)
 
 
-def expert_call(rows, share, weights, kind, name):
+def expert_call(rows, share, weights, kind, name, chunk, chunks):
     count, width = rows.shape
-    experts, shards, parts, _, units = weights.shape
+    count = count // chunks
+    experts, shards, depth, double = weights.shape
     together = 2
     return pl.pallas_call(
         expert_kernel,
         grid=(experts, shards // together),
         in_specs=[
-            pl.BlockSpec((count, width), lambda e, s: (0, 0)),
-            pl.BlockSpec(share.shape, lambda e, s: (0, 0)),
-            pl.BlockSpec((1, together, parts, width, units), lambda e, s: (e, s, 0, 0, 0)),
+            pl.BlockSpec((count, width), lambda e, s: (chunk, 0)),
+            pl.BlockSpec((count, share.shape[1]), lambda e, s: (chunk, 0)),
+            pl.BlockSpec((1, together, depth, double), lambda e, s: (e, s, 0, 0)),
         ],
         out_specs=pl.BlockSpec((count, width), lambda e, s: (0, 0)),
         out_shape=jax.ShapeDtypeStruct((count, width), kind),
@@ -262,6 +300,40 @@
         ),
         name=name,
     )(rows, share, weights)
+
+
+def combine_kernel(*refs):
+    stream_ref, shared_ref, own_ref, answer_ref, gain_ref, out_ref = refs[-6:]
+    summed = shared_ref[...] + own_ref[...] + answer_ref[...].astype(F32)
+    out_ref[...] = (stream_ref[...].astype(F32) + rms_scale(summed) * gain_ref[...]).astype(BF16)
+
+
+def combine_call(so_far, stream, shared, own, answer, gain, chunk, chunks):
+    rows, width = stream.shape
+    span = min(rows // chunks, 128)
+    steps = rows // chunks // span
+    block = pl.BlockSpec((span, width), lambda i: (chunk * steps + i, 0))
+    specs = [block, block, block, pl.BlockSpec((span, width), lambda i: (i, 0))]
+    specs.append(pl.BlockSpec((1, width), lambda i: (0, 0)))
+    operands = [stream, shared, own, answer, gain.reshape(1, width)]
+    aliases = {}
+    if so_far is not None:
+        specs.insert(0, pl.BlockSpec(memory_space=pl.ANY))
+        operands.insert(0, so_far)
+        aliases = {0: 0}
+    return pl.pallas_call(
+        combine_kernel,
+        grid=(steps,),
+        in_specs=specs,
+        out_specs=block,
+        out_shape=jax.ShapeDtypeStruct((rows, width), BF16),
+        input_output_aliases=aliases,
+        compiler_params=pltpu.CompilerParams(dimension_semantics=("arbitrary",)),
+        cost_estimate=pl.CostEstimate(
+            flops=rows * width, bytes_accessed=14 * rows * width // chunks, transcendentals=0
+        ),
+        name="combine%d" % chunk,
+    )(*operands)
 
 
 def shared_expert(normed, gate_w, up_w, down_w):
@@ -339,7 +411,7 @@
     paired = len(sp) == 2
     if paired:
         outer, inner = sp
-        packed = jnp.concatenate([expert_gate_matrix, expert_up_matrix, expert_down_matrix], axis=0)
+        packed = pack_call(expert_gate_matrix, expert_up_matrix, expert_down_matrix)
         held = lax.all_gather(packed, (inner, "tp"))
         held = held.reshape((lax.axis_size(inner), peers) + packed.shape)
         experts_all = lax.axis_size(outer) * lax.axis_size(inner)
@@ -386,21 +458,19 @@
         layer_out = stream.astype(F32) + rms_scale(shared + routed) * final_norm_gain
         return layer_out.astype(BF16)
     far_rows = lax.ppermute(normed, outer, swap)
+    far_rows, shared = lax.optimization_barrier((far_rows, shared))
     chunks = 2
-    part = rows // chunks
     answers = []
     for c in range(chunks):
-        cut = slice(c * part, (c + 1) * part)
-        partial = expert_call(far_rows[cut], far_share[cut], held, BF16, "far%d" % c)
+        partial = expert_call(far_rows, far_share, held, BF16, "far%d" % c, c, chunks)
         answers.append(lax.ppermute(partial, outer, swap))
-    own = expert_call(normed, own_share, held, F32, "own")
-    base = shared + own
-    outs = []
+    own = expert_call(normed, own_share, held, F32, "own", 0, 1)
+    layer_out = None
     for c in range(chunks):
-        cut = slice(c * part, (c + 1) * part)
-        summed = base[cut] + answers[c].astype(F32)
-        outs.append((stream[cut].astype(F32) + rms_scale(summed) * final_norm_gain).astype(BF16))
-    return jnp.concatenate(outs, axis=0)
+        layer_out = combine_call(
+            layer_out, stream, shared, own, answers[c], final_norm_gain, c, chunks
+        )
+    return layer_out
 
 
 def solution(mesh):

time: 241 us -> 236 us (0.979)
  Pallas kernels: 84.7 us -> 98.3 us
  other arithmetic: 12.4 us -> 1.8 us
  waiting for transfers between devices: 56.5 us -> 48.4 us
    ppermute x1, waiting for transfers between devices: 48.3 us -> 4.25 us  [body(): lax.ppermute(jnp.where(here == 0, share[:, 1], share[:, 0]), outer, swap)]
    ppermute x1, waiting for transfers between devices: 0.01 us -> 33.9 us  [body(): far_rows = lax.ppermute(normed, outer, swap)]
    pallas_call x0 -> x3, Pallas kernels: none -> 11.1 us  [the longest x2 8.18 us: combine_call(): pl.pallas_call(combine_kernel, grid=(steps,), in_specs=specs, out_specs=b...]
    pallas_call x1, Pallas kernels: 18.8 us -> 25.2 us  [scan_call(): pl.pallas_call(scan_kernel, grid=(tokens // span,), in_specs=[block, bloc...]
    pallas_call x3, Pallas kernels: 52.7 us -> 47.5 us  [expert_call(): pl.pallas_call(expert_kernel, grid=(experts, shards // together), in_spec...]
    ppermute x2, waiting for transfers between devices: 1.75 us -> 6.88 us  [body(): answers.append(lax.ppermute(partial, outer, swap))]
    concatenate x2 -> x0, other arithmetic: 4.22 us -> none  [the longest x1 2.77 us: body(): jnp.concatenate([expert_gate_matrix, expert_up_matrix, expert_down_matrix...]
    reduce_sum x1 -> x0, other arithmetic: 3.53 us -> none  [rms_scale(): jnp.mean(values * values, axis=-1, keepdims=True) + EPS]
  transfers between devices with their start and end apart: 5 -> 5, of which waited for: 3 -> 4; matrix products, arithmetic and copies ran while one was open for 6% -> 6% of each run, Pallas kernels for 29% -> 33%
where the time goes in v1:
time: 236 us; the launch traced here: 235 us
  Pallas kernels  98.3 us (42%)
  blocking collectives  55.6 us (24%)
  waiting for transfers between devices  48.4 us (21%)
  between operations  13.5 us (6%)
  matrix products  9.87 us (4%)
  starting transfers between devices  4.18 us (2%)
  local copies, waits for them, and re-layouts  3.68 us (2%)
    pallas_call x3, Pallas kernels, expert_call(): pl.pallas_call(expert_kernel, grid=(experts, shards // together), in_spec...  47.5 us
    all_to_all x1, blocking collectives, body(): lax.all_to_all(mixed.reshape(peers, tokens // peers, channels), 'tp', spl...  44.9 us
    ppermute x1, waiting for transfers between devices, body(): far_rows = lax.ppermute(normed, outer, swap)  33.9 us
    pallas_call x1, Pallas kernels, scan_call(): pl.pallas_call(scan_kernel, grid=(tokens // span,), in_specs=[block, bloc...  25.2 us
    all_gather x1, blocking collectives, body(): pieces = lax.all_gather(final, sp)  10.7 us
    pallas_call x2, Pallas kernels, combine_call(): pl.pallas_call(combine_kernel, grid=(steps,), in_specs=specs, out_specs=b...  8.18 us
    pallas_call x1, Pallas kernels, project_call(): pl.pallas_call(project_kernel, grid=(rows // span,), in_specs=[pl.BlockSp...  8.09 us
    ppermute x2, waiting for transfers between devices, body(): answers.append(lax.ppermute(partial, outer, swap))  6.88 us
  transfers between devices with their start and end apart: 5, of which 4 were waited for; matrix products, arithmetic and copies ran while one was open for 6% of the time, Pallas kernels for 33%

profile of v1, /device:TPU:8, one launch (start us, length us, event | category | flops | bytes accessed | tf_op | source)
XLA Modules:
  0.0 235.4 jit_solution(10286107794883683643)
XLA Ops:
  6.5 0.0 copy-start
  6.5 0.0 copy-start.8
  6.5 0.0 all-gather.4.cloned.1.call-start
  6.5 2.9 %pack.1 = bf16[3072,256]{1,0:T(8,128)(2,1)} custom-call(bf16[1,2048,128]{2,1,0:T(8,128)(2,1)} %gate_ref.1, bf16[1,2048,128]{2,1,0:T(8,128)(2,1)} %up_ref.1, bf16[1,2048,128]{2,1,0:T(8,128)(2,1)} %down_ref.1), custom_call_target="tpu_custom_call" | custom-call | bytes 3145728 | tf_op jit(solution)/shard_map/pack/pallas_call | solution.py:240
  9.5 0.0 all-gather.4.cloned.1.call-update
  9.5 0.0 copy-done.8
  9.5 0.6 reshape_tile.3.gain_ref
  10.1 25.2 %scan.1 = (f32[4096,128]{1,0:T(8,128)}, f32[4096,128]{1,0:T(8,128)}, f32[136,128]{1,0:T(8,128)}) custom-call(bf16[4096,128]{1,0:T(8,128)(2,1)} %q_ref.1, bf16[4096,128]{1,0:T(8,128)(2,1)} %f_ref.1, bf16[4096,128]{1,0:T(8,128)(2,1)} %v_ref.1, f32[1,128]{1,0:T(1,128)} %bitcast.28, f32[2,4096]{1,0:T(2,128)} %sudden_ref.1), custom_call_target="tpu_custom_call" | custom-call | flops 1048576000 | bytes 7340032 | tf_op jit(solution)/shard_map/scan/pallas_call | solution.py:122
  35.3 10.7 %all-gather = f32[544,128]{1,0:T(8,128)} all-gather(f32[136,128]{1,0:T(8,128)} %get-tuple-element.14), channel_id=2, replica_groups=mesh['far'=2,'near'=2,'tp'=8] {'far','near'}, dimensions={0}, use_global_device_ids=true | all-gather | bytes 348160 | tf_op jit(solution)/shard_map/all_gather | solution.py:431
  46.0 6.5 %gate.1 = bf16[4096,128]{1,0:T(8,128)(2,1)} custom-call(s32[1]{0:T(128)} %bitcast.mine_ref, f32[4096,128]{1,0:T(8,128)} %get-tuple-element.12.local_ref, f32[4096,128]{1,0:T(8,128)} %get-tuple-element.13.lifted_ref, bf16[4096,128]{1,0:T(8,128)(2,1)} %open_ref.1, f32[4,136,128]{2,1,0:T(8,128)} %bitcast.23, f32[1,128]{1,0:T(1,128)} %reshape_tile.3.gain_ref), custom_call_target="tpu_custom_call" | custom-call | flops 419430400 | bytes 5242880 | tf_op jit(solution)/shard_map/gate/pallas_call | solution.py:172
  52.5 44.9 %all_to_all.5.mixed_ref = bf16[8,512,128]{2,1,0:T(8,128)(2,1)} all-to-all(bf16[8,512,128]{2,1,0:T(8,128)(2,1)} %bitcast.22), channel_id=1, replica_groups=mesh['far'=2,'near'=2,'tp'=8] {'tp'}, dimensions={0} | all-to-all | bytes 2097152 | tf_op jit(solution)/shard_map/all_to_all | solution.py:435
  97.4 0.0 copy-start.6
  97.4 0.0 copy-start.7
  97.4 8.1 %project.1 = (bf16[512,2048]{1,0:T(8,128)(2,1)}, bf16[512,2048]{1,0:T(8,128)(2,1)}) custom-call(bf16[8,512,128]{2,1,0:T(8,128)(2,1)} %all_to_all.5.mixed_ref, bf16[1024,2048]{1,0:T(8,128)(2,1)} %weight_ref.1, bf16[512,2048]{1,0:T(8,128)(2,1)} %residual_ref.1, f32[1,2048]{1,0:T(1,128)} %bitcast.26, f32[1,2048]{1,0:T(1,128)} %bitcast.27), custom_call_target="tpu_custom_call" | custom-call | flops 2147483648 | bytes 12582912 | tf_op jit(solution)/shard_map/project/pallas_call | solution.py:207
  105.5 1.4 collective-permute-start
  106.9 0.0 copy-done.6
  106.9 0.0 copy-done.7
  106.9 0.1 copy.31
  107.1 0.9 copy.30
  108.0 1.8 select_bitcast_fusion
  109.8 0.6 collective-permute-start.1
  110.4 3.4 %fusion.10 = f32[512,256]{1,0:T(8,128)} fusion(bf16[512,2048]{1,0:T(8,128)(2,1)} %get-tuple-element.16.rows_ref, bf16[2048,256]{1,0:T(8,128)(2,1)} %param.36), kind=kOutput, calls=%fused_computation.15 | convolution fusion | flops 536870912 | bytes 3670016 | tf_op jit(solution)/shard_map/dot_general | solution.py:341
  113.8 0.0 copy-done
  113.8 6.5 %fusion.1.refs_1_.refs_2_ = f32[512,2048]{1,0:T(8,128)} fusion(bf16[256,2048]{1,0:T(8,128)(2,1)S(1)} %copy-done, bf16[512,2048]{1,0:T(8,128)(2,1)} %get-tuple-element.16.rows_ref, bf16[2048,256]{1,0:T(8,128)(2,1)} %param.37, f32[512,256]{1,0:T(8,128)} %fusion.10), kind=kOutput, calls=%fused_computation.2 | convolution fusion | flops 1074528256 | bytes 8912896 | tf_op jit(solution)/shard_map/dot_general | solution.py:344
  120.3 33.9 %collective-permute-done.rows_ref = bf16[512,2048]{1,0:T(8,128)(2,1)S(1)} collective-permute-done((bf16[512,2048]{1,0:T(8,128)(2,1)}, bf16[512,2048]{1,0:T(8,128)(2,1)S(1)}, u32[]{:S(2)}, u32[]{:S(2)}) %collective-permute-start) | collective-permute-done | bytes 2097184 | tf_op jit(solution)/shard_map/ppermute | solution.py:460
  154.2 4.3 %collective-permute-done.1.share_ref = f32[512,2]{1,0:T(8,128)S(1)} collective-permute-done((f32[512,2]{1,0:T(8,128)}, f32[512,2]{1,0:T(8,128)S(1)}, u32[]{:S(2)}, u32[]{:S(2)}) %collective-permute-start.1) | collective-permute-done | bytes 4128 | tf_op jit(solution)/shard_map/ppermute | solution.py:426
  158.5 3.4 %all-gather.4.cloned.1.call-done = bf16[49152,256]{1,0:T(8,128)(2,1)} async-done(((bf16[3072,256]{1,0:T(8,128)(2,1)}), bf16[49152,256]{1,0:T(8,128)(2,1)}) %all-gather.4.cloned.1.call-update) | async-done | bytes 25165840 | tf_op jit(solution)/shard_map/all_gather | solution.py:415
  161.8 13.7 %far0.1 = bf16[256,2048]{1,0:T(8,128)(2,1)S(1)} custom-call(bf16[512,2048]{1,0:T(8,128)(2,1)S(1)} %collective-permute-done.rows_ref, f32[512,2]{1,0:T(8,128)S(1)} %collective-permute-done.1.share_ref, bf16[2,8,3072,256]{3,2,1,0:T(8,128)(2,1)} %bitcast.19), custom_call_target="tpu_custom_call" | custom-call | flops 6442450944 | bytes 25165824 | tf_op jit(solution)/shard_map/far0/pallas_call | solution.py:284
  175.6 0.0 copy-start.2
  175.6 0.0 copy-start.3
  175.6 1.5 collective-permute-start.2
  177.1 14.7 %far1.1 = bf16[256,2048]{1,0:T(8,128)(2,1)} custom-call(bf16[512,2048]{1,0:T(8,128)(2,1)S(1)} %collective-permute-done.rows_ref, f32[512,2]{1,0:T(8,128)S(1)} %collective-permute-done.1.share_ref, bf16[2,8,3072,256]{3,2,1,0:T(8,128)(2,1)} %bitcast.20), custom_call_target="tpu_custom_call" | custom-call | flops 6442450944 | bytes 25165824 | tf_op jit(solution)/shard_map/far1/pallas_call | solution.py:284
  191.8 0.6 collective-permute-start.3
  192.4 0.0 copy-done.2
  192.4 0.0 copy-done.3
  192.4 19.1 %own.1.refs_2_.refs_3_ = f32[512,2048]{1,0:T(8,128)} custom-call(bf16[512,2048]{1,0:T(8,128)(2,1)S(1)} %copy-done.2, f32[512,2]{1,0:T(8,128)S(1)} %copy-done.3, bf16[2,8,3072,256]{3,2,1,0:T(8,128)(2,1)} %bitcast.21), custom_call_target="tpu_custom_call" | custom-call | flops 12884901888 | bytes 25165824 | tf_op jit(solution)/shard_map/own/pallas_call | solution.py:284
  211.5 0.0 collective-permute-done.2.refs_3_
  211.5 0.0 copy-start.5
  211.5 1.0 copy-done.5
  212.5 4.0 %combine0.1.refs_0_ = bf16[512,2048]{1,0:T(8,128)(2,1)} custom-call(bf16[512,2048]{1,0:T(8,128)(2,1)} %get-tuple-element.15.refs_0_.refs_1_, f32[512,2048]{1,0:T(8,128)} %fusion.1.refs_1_.refs_2_, f32[512,2048]{1,0:T(8,128)} %own.1.refs_2_.refs_3_, bf16[256,2048]{1,0:T(8,128)(2,1)} %copy-done.5, f32[1,2048]{1,0:T(1,128)} %bitcast.24), custom_call_target="tpu_custom_call" | custom-call | flops 1048576 | bytes 7340032 | tf_op jit(solution)/shard_map/combine0/pallas_call | solution.py:324
  216.5 6.9 %collective-permute-done.3.refs_4_ = bf16[256,2048]{1,0:T(8,128)(2,1)S(1)} collective-permute-done((bf16[256,2048]{1,0:T(8,128)(2,1)}, bf16[256,2048]{1,0:T(8,128)(2,1)S(1)}, u32[]{:S(2)}, u32[]{:S(2)}) %collective-permute-start.3) | collective-permute-done | bytes 1048608 | tf_op jit(solution)/shard_map/ppermute | solution.py:466
  223.4 0.0 copy-start.4
  223.4 1.0 copy-done.4
  224.4 0.0 copy-start.1
  224.4 4.1 %combine1.1 = bf16[512,2048]{1,0:T(8,128)(2,1)} custom-call(bf16[512,2048]{1,0:T(8,128)(2,1)} %combine0.1.refs_0_, bf16[512,2048]{1,0:T(8,128)(2,1)} %get-tuple-element.15.refs_0_.refs_1_, f32[512,2048]{1,0:T(8,128)} %fusion.1.refs_1_.refs_2_, f32[512,2048]{1,0:T(8,128)} %own.1.refs_2_.refs_3_, ...), custom_call_target="tpu_custom_call", output_to_operand_aliasing={{}: (0, {})} | custom-call | flops 1048576 | bytes 7340032 | tf_op jit(solution)/shard_map/combine1/pallas_call | solution.py:324
  228.5 0.0 copy-done.1
  (4 shorter events, 0.0 us)
Async XLA Ops:
  6.5 107.3 %copy-start = (bf16[256,2048]{1,0:T(8,128)(2,1)S(1)}, bf16[256,2048]{1,0:T(8,128)(2,1)}, u32[]{:S(2)}) copy-start(bf16[256,2048]{1,0:T(8,128)(2,1)} %param.38) | copy-start | bytes 3145732
  6.5 3.0 %copy-start.8 = (f32[64]{0:T(128)S(1)}, f32[64]{0:T(128)}, u32[]{:S(2)}) copy-start(f32[64]{0:T(128)} %param.27) | copy-start | bytes 772
  6.5 155.3 %all-gather.4.cloned.1.call-start = ((), (), s32[]{:S(2)}) async-start(), calls=%async_computation.1 | async-start | bytes 26738688 | tf_op jit(solution)/shard_map/all_gather | solution.py:415
  97.4 9.5 %copy-start.6 = (f32[512,2]{0,1:T(2,128)S(1)}, f32[512,2]{0,1:T(2,128)}, u32[]{:S(2)}) copy-start(f32[512,2]{0,1:T(2,128)} %param.32) | copy-start | bytes 12292
  97.4 9.5 %copy-start.7 = (s32[512,2]{0,1:T(2,128)S(1)}, s32[512,2]{0,1:T(2,128)}, u32[]{:S(2)}) copy-start(s32[512,2]{0,1:T(2,128)} %param.31) | copy-start | bytes 12292
  105.5 48.7 %collective-permute-start = (bf16[512,2048]{1,0:T(8,128)(2,1)}, bf16[512,2048]{1,0:T(8,128)(2,1)S(1)}, u32[]{:S(2)}, u32[]{:S(2)}) collective-permute-start(bf16[512,2048]{1,0:T(8,128)(2,1)} %get-tuple-element.16.rows_ref), channel_id=1, source_target_pairs={{0,16},{16,0},{1,17},{17,1},{2,18},{18,2},{3,19},{19,3},{4,20},{20... | collective-permute-start | bytes 6291464 | tf_op jit(solution)/shard_map/ppermute | solution.py:460
  109.8 48.7 %collective-permute-start.1 = (f32[512,2]{1,0:T(8,128)}, f32[512,2]{1,0:T(8,128)S(1)}, u32[]{:S(2)}, u32[]{:S(2)}) collective-permute-start(f32[512,2]{1,0:T(8,128)} %get-tuple-element.19), channel_id=1, source_target_pairs={{0,16},{16,0},{1,17},{17,1},{2,18},{18,2},{3,19},{19,3},{4,20},{20... | collective-permute-start | bytes 12296 | tf_op jit(solution)/shard_map/ppermute | solution.py:426
  175.6 16.8 %copy-start.2 = (bf16[512,2048]{1,0:T(8,128)(2,1)S(1)}, bf16[512,2048]{1,0:T(8,128)(2,1)}, u32[]{:S(2)}) copy-start(bf16[512,2048]{1,0:T(8,128)(2,1)} %get-tuple-element.16.rows_ref) | copy-start | bytes 6291460
  175.6 16.8 %copy-start.3 = (f32[512,2]{1,0:T(8,128)S(1)}, f32[512,2]{1,0:T(8,128)}, u32[]{:S(2)}) copy-start(f32[512,2]{1,0:T(8,128)} %get-tuple-element.20.share_ref) | copy-start | bytes 12292
  175.6 35.9 %collective-permute-start.2 = (bf16[256,2048]{1,0:T(8,128)(2,1)S(1)}, bf16[256,2048]{1,0:T(8,128)(2,1)S(1)}, u32[]{:S(2)}, u32[]{:S(2)}) collective-permute-start(bf16[256,2048]{1,0:T(8,128)(2,1)S(1)} %far0.1), channel_id=1, source_target_pairs={{0,16},{16,0},{1,17},{17,1},{2,18},{18,2},{3,19},{19,3},{4,20},{20... | collective-permute-start | bytes 3145736 | tf_op jit(solution)/shard_map/ppermute | solution.py:466
  191.8 31.7 %collective-permute-start.3 = (bf16[256,2048]{1,0:T(8,128)(2,1)}, bf16[256,2048]{1,0:T(8,128)(2,1)S(1)}, u32[]{:S(2)}, u32[]{:S(2)}) collective-permute-start(bf16[256,2048]{1,0:T(8,128)(2,1)} %far1.1), channel_id=1, source_target_pairs={{0,16},{16,0},{1,17},{17,1},{2,18},{18,2},{3,19},{19,3},{4,20},{20... | collective-permute-start | bytes 3145736 | tf_op jit(solution)/shard_map/ppermute | solution.py:466
  211.5 1.0 copy-start.5
  223.4 1.0 copy-start.4
  224.4 4.1 %copy-start.1 = (bf16[256,2048]{1,0:T(8,128)(2,1)S(1)}, bf16[256,2048]{1,0:T(8,128)(2,1)}, u32[]{:S(2)}) copy-start(bf16[256,2048]{1,0:T(8,128)(2,1)} %param.38) | copy-start | bytes 3145732
Sparse Core Ops, SparseCore 0:
  9.6 152.1 all-gather.3

commit v2 on v1

--- a/solution.py
+++ b/solution.py
@@ -190,40 +190,62 @@
     )(mine, local, lifted, opening, pieces, gain)
 
 
-def project_kernel(mixed_ref, weight_ref, residual_ref, mixer_ref, gain_ref, stream_ref, normed_ref):
+def project_kernel(
+    mixed_ref,
+    weight_ref,
+    residual_ref,
+    mixer_ref,
+    gain_ref,
+    gate_ref,
+    up_ref,
+    down_ref,
+    stream_ref,
+    normed_ref,
+    shared_ref,
+):
     mixed = jnp.concatenate([mixed_ref[j] for j in range(mixed_ref.shape[0])], axis=1)
     projected = mm(mixed, weight_ref[...]).astype(BF16).astype(F32)
     stream = (residual_ref[...].astype(F32) + rms_scale(projected) * mixer_ref[...]).astype(BF16)
     stream_ref[...] = stream
-    normed_ref[...] = (rms_scale(stream.astype(F32)) * gain_ref[...]).astype(BF16)
-
-
-def project_call(mixed, weight, residual, mixer_gain, gain):
+    normed = (rms_scale(stream.astype(F32)) * gain_ref[...]).astype(BF16)
+    normed_ref[...] = normed
+    gate = mm(normed, gate_ref[...])
+    hidden = (gate * jax.nn.sigmoid(gate) * mm(normed, up_ref[...])).astype(BF16)
+    shared_ref[...] = mm(hidden, down_ref[...])
+
+
+def project_call(mixed, weight, residual, mixer_gain, gain, shared_weights):
     sources, rows, channels = mixed.shape
     width = weight.shape[1]
     span = min(rows, 256)
     block = pl.BlockSpec((span, width), lambda i: (i, 0))
-    vector = pl.BlockSpec((1, width), lambda i: (0, 0))
+
+    def whole(array):
+        return pl.BlockSpec(array.shape, lambda i: (0, 0))
+
+    vectors = [mixer_gain.reshape(1, width), gain.reshape(1, width)]
+    hidden = shared_weights[0].shape[1]
     return pl.pallas_call(
         project_kernel,
         grid=(rows // span,),
-        in_specs=[
-            pl.BlockSpec((sources, span, channels), lambda i: (0, i, 0)),
-            pl.BlockSpec(weight.shape, lambda i: (0, 0)),
-            block,
-            vector,
-            vector,
+        in_specs=[pl.BlockSpec((sources, span, channels), lambda i: (0, i, 0)), whole(weight), block]
+        + [whole(array) for array in vectors + list(shared_weights)],
+        out_specs=[block, block, block],
+        out_shape=[
+            jax.ShapeDtypeStruct((rows, width), BF16),
+            jax.ShapeDtypeStruct((rows, width), BF16),
+            jax.ShapeDtypeStruct((rows, width), F32),
         ],
-        out_specs=[block, block],
-        out_shape=[jax.ShapeDtypeStruct((rows, width), BF16)] * 2,
-        compiler_params=pltpu.CompilerParams(dimension_semantics=("arbitrary",)),
+        compiler_params=pltpu.CompilerParams(
+            dimension_semantics=("arbitrary",), vmem_limit_bytes=48 * 1024 * 1024
+        ),
         cost_estimate=pl.CostEstimate(
-            flops=2 * rows * width * weight.shape[0],
-            bytes_accessed=2 * weight.size + 8 * rows * width,
+            flops=2 * rows * width * (weight.shape[0] + 3 * hidden),
+            bytes_accessed=2 * weight.size + 12 * rows * width,
             transcendentals=0,
         ),
         name="project",
-    )(mixed, weight, residual, mixer_gain.reshape(1, width), gain.reshape(1, width))
+    )(mixed, weight, residual, *vectors, *shared_weights)
 
 
 def pack_kernel(gate_ref, up_ref, down_ref, packed_ref):
@@ -245,11 +267,13 @@
     )(gate, up, down)
 
 
-def expert_kernel(rows_ref, share_ref, weights_ref, out_ref, sum_ref):
+def expert_kernel(*refs, based):
+    rows_ref, share_ref, weights_ref = refs[:3]
+    out_refs, sum_ref = refs[3 + based : -1], refs[-1]
     expert, piece = pl.program_id(0), pl.program_id(1)
     first = jnp.logical_and(expert == 0, piece == 0)
     last = jnp.logical_and(expert == pl.num_programs(0) - 1, piece == pl.num_programs(1) - 1)
-    count, width = rows_ref.shape
+    width = rows_ref.shape[1]
     shards, _, double = weights_ref.shape[1:]
     units = double // 2
 
@@ -257,7 +281,7 @@
     def _():
         sum_ref[...] = jnp.zeros_like(sum_ref)
 
-    share = share_ref[...]
+    share = share_ref[...].T
     lanes = lax.broadcasted_iota(jnp.int32, share.shape, 1)
     share = jnp.sum(jnp.where(lanes == expert, share, 0.0), axis=1, keepdims=True)
     hidden = []
@@ -273,24 +297,36 @@
 
     @pl.when(last)
     def _():
-        out_ref[...] = sum_ref[...].astype(out_ref.dtype)
-
-
-def expert_call(rows, share, weights, kind, name, chunk, chunks):
+        start = 0
+        for out_ref in out_refs:
+            at = slice(start, start + out_ref.shape[0])
+            total = sum_ref[at, :] + refs[3][at, :] if based else sum_ref[at, :]
+            out_ref[...] = total.astype(out_ref.dtype)
+            start += out_ref.shape[0]
+
+
+def expert_call(rows, share, weights, base, pieces, kind, name, together):
     count, width = rows.shape
-    count = count // chunks
     experts, shards, depth, double = weights.shape
-    together = 2
+
+    def whole(size):
+        return pl.BlockSpec((size, width), lambda e, s: (0, 0))
+
+    specs = [
+        whole(count),
+        pl.BlockSpec(share.shape, lambda e, s: (0, 0)),
+        pl.BlockSpec((1, together, depth, double), lambda e, s: (e, s, 0, 0)),
+    ]
+    operands = [rows, share, weights]
+    if base is not None:
+        specs.append(whole(count))
+        operands.append(base)
     return pl.pallas_call(
-        expert_kernel,
+        functools.partial(expert_kernel, based=base is not None),
         grid=(experts, shards // together),
-        in_specs=[
-            pl.BlockSpec((count, width), lambda e, s: (chunk, 0)),
-            pl.BlockSpec((count, share.shape[1]), lambda e, s: (chunk, 0)),
-            pl.BlockSpec((1, together, depth, double), lambda e, s: (e, s, 0, 0)),
-        ],
-        out_specs=pl.BlockSpec((count, width), lambda e, s: (0, 0)),
-        out_shape=jax.ShapeDtypeStruct((count, width), kind),
+        in_specs=specs,
+        out_specs=[whole(size) for size in pieces],
+        out_shape=[jax.ShapeDtypeStruct((size, width), kind) for size in pieces],
         scratch_shapes=[pltpu.VMEM((count, width), F32)],
         compiler_params=pltpu.CompilerParams(
             dimension_semantics=("arbitrary", "arbitrary"), vmem_limit_bytes=48 * 1024 * 1024
@@ -299,23 +335,23 @@
             flops=2 * count * weights.size, bytes_accessed=2 * weights.size, transcendentals=0
         ),
         name=name,
-    )(rows, share, weights)
+    )(*operands)
 
 
 def combine_kernel(*refs):
-    stream_ref, shared_ref, own_ref, answer_ref, gain_ref, out_ref = refs[-6:]
-    summed = shared_ref[...] + own_ref[...] + answer_ref[...].astype(F32)
+    stream_ref, base_ref, answer_ref, gain_ref, out_ref = refs[-5:]
+    summed = base_ref[...] + answer_ref[...].astype(F32)
     out_ref[...] = (stream_ref[...].astype(F32) + rms_scale(summed) * gain_ref[...]).astype(BF16)
 
 
-def combine_call(so_far, stream, shared, own, answer, gain, chunk, chunks):
+def combine_call(so_far, stream, base, answer, gain, start):
     rows, width = stream.shape
-    span = min(rows // chunks, 128)
-    steps = rows // chunks // span
-    block = pl.BlockSpec((span, width), lambda i: (chunk * steps + i, 0))
-    specs = [block, block, block, pl.BlockSpec((span, width), lambda i: (i, 0))]
+    span = min(answer.shape[0], 64)
+    skip = start // span
+    block = pl.BlockSpec((span, width), lambda i: (skip + i, 0))
+    specs = [block, block, pl.BlockSpec((span, width), lambda i: (i, 0))]
     specs.append(pl.BlockSpec((1, width), lambda i: (0, 0)))
-    operands = [stream, shared, own, answer, gain.reshape(1, width)]
+    operands = [stream, base, answer, gain.reshape(1, width)]
     aliases = {}
     if so_far is not None:
         specs.insert(0, pl.BlockSpec(memory_space=pl.ANY))
@@ -323,16 +359,16 @@
         aliases = {0: 0}
     return pl.pallas_call(
         combine_kernel,
-        grid=(steps,),
+        grid=(answer.shape[0] // span,),
         in_specs=specs,
         out_specs=block,
         out_shape=jax.ShapeDtypeStruct((rows, width), BF16),
         input_output_aliases=aliases,
         compiler_params=pltpu.CompilerParams(dimension_semantics=("arbitrary",)),
         cost_estimate=pl.CostEstimate(
-            flops=rows * width, bytes_accessed=14 * rows * width // chunks, transcendentals=0
-        ),
-        name="combine%d" % chunk,
+            flops=answer.size, bytes_accessed=10 * answer.size, transcendentals=0
+        ),
+        name="combine%d" % start,
     )(*operands)
 
 
@@ -415,15 +451,19 @@
         held = lax.all_gather(packed, (inner, "tp"))
         held = held.reshape((lax.axis_size(inner), peers) + packed.shape)
         experts_all = lax.axis_size(outer) * lax.axis_size(inner)
-        numbers = jnp.arange(experts_all, dtype=jnp.int32)
-        share = jnp.sum(
-            (routed_expert_index[:, :, None] == numbers) * routed_expert_weight[:, :, None], axis=1
+        share = jnp.stack(
+            [
+                jnp.sum(jnp.where(routed_expert_index == e, routed_expert_weight, 0.0), axis=1)
+                for e in range(experts_all)
+            ]
         )
-        share = share.reshape(rows, lax.axis_size(outer), lax.axis_size(inner))
+        pair = lax.axis_size(inner)
         swap = [(0, 1), (1, 0)]
-        here = lax.axis_index(outer)
-        own_share = jnp.where(here == 0, share[:, 0], share[:, 1])
-        far_share = lax.ppermute(jnp.where(here == 0, share[:, 1], share[:, 0]), outer, swap)
+        here = lax.axis_index(outer) == 0
+        filler = jnp.zeros((8 - pair, rows), F32)
+        own_share = jnp.concatenate([jnp.where(here, share[:pair], share[pair:]), filler])
+        far_share = jnp.concatenate([jnp.where(here, share[pair:], share[:pair]), filler])
+        far_share = lax.ppermute(far_share, outer, swap)
 
     local, lifted, final = scan_call(
         query_values, forget_preact, value_written, forget_margin, sudden_decay
@@ -436,15 +476,20 @@
         mixed.reshape(peers, tokens // peers, channels), "tp", split_axis=0, concat_axis=0, tiled=True
     )
     if channels % 128 == 0:
-        stream, normed = project_call(
-            mixed, output_weight_matrix, residual, mixer_norm_gain, feedforward_gain
+        stream, normed, shared = project_call(
+            mixed,
+            output_weight_matrix,
+            residual,
+            mixer_norm_gain,
+            feedforward_gain,
+            (common_gate_matrix, common_up_matrix, common_down_matrix),
         )
     else:
         mixed = mixed.transpose(1, 0, 2).reshape(rows, peers * channels)
         projected = jnp.dot(mixed, output_weight_matrix, preferred_element_type=F32).astype(BF16)
         stream = (residual.astype(F32) + rms_scale(projected.astype(F32)) * mixer_norm_gain).astype(BF16)
         normed = (rms_scale(stream.astype(F32)) * feedforward_gain).astype(BF16)
-    shared = shared_expert(normed, common_gate_matrix, common_up_matrix, common_down_matrix)
+        shared = shared_expert(normed, common_gate_matrix, common_up_matrix, common_down_matrix)
     if not paired:
         routed = routed_by_slots(
             normed,
@@ -457,19 +502,21 @@
         )
         layer_out = stream.astype(F32) + rms_scale(shared + routed) * final_norm_gain
         return layer_out.astype(BF16)
-    far_rows = lax.ppermute(normed, outer, swap)
-    far_rows, shared = lax.optimization_barrier((far_rows, shared))
-    chunks = 2
-    answers = []
-    for c in range(chunks):
-        partial = expert_call(far_rows, far_share, held, BF16, "far%d" % c, c, chunks)
-        answers.append(lax.ppermute(partial, outer, swap))
-    own = expert_call(normed, own_share, held, F32, "own", 0, 1)
+    first = 3 * rows // 8
+    far_first = lax.ppermute(normed[:first], outer, swap)
+    far_rest = lax.ppermute(normed[first:], outer, swap)
+    (partial,) = expert_call(far_first, far_share[:, :first], held, None, (first,), BF16, "far0", 4)
+    answers = [lax.ppermute(partial, outer, swap)]
+    far_rest, _ = lax.optimization_barrier((far_rest, partial))
+    sizes = (rows - 2 * first, first)
+    partials = expert_call(far_rest, far_share[:, first:], held, None, sizes, BF16, "far1", 4)
+    answers += [lax.ppermute(partial, outer, swap) for partial in partials]
+    own_rows, _ = lax.optimization_barrier((normed, partials[1]))
+    (base,) = expert_call(own_rows, own_share, held, shared, (rows,), F32, "own", 2)
     layer_out = None
-    for c in range(chunks):
-        layer_out = combine_call(
-            layer_out, stream, shared, own, answers[c], final_norm_gain, c, chunks
-        )
+    starts = (0, first, first + sizes[0])
+    for c in (0, 2, 1):
+        layer_out = combine_call(layer_out, stream, base, answers[c], final_norm_gain, starts[c])
     return layer_out
 
 

time: 236 us -> 231 us (0.979)
  matrix products: 9.87 us -> 0 us
  starting transfers between devices: 4.18 us -> 6.99 us
    dot_general x2 -> x0, matrix products: 9.87 us -> none  [the longest x1 6.45 us: shared_expert(): return jnp.dot(hidden, down_w, preferred_element_type=F32)]
    slice x1 -> x4, local copies, waits for them, and re-layouts: 0.01 us -> 3.67 us  [the longest x1 2.67 us: body(): far_rest = lax.ppermute(normed[first:], outer, swap)]
    ppermute x4 -> x6, starting transfers between devices: 4.18 us -> 6.99 us  [the longest x2 2.09 us: body(): answers += [lax.ppermute(partial, outer, swap) for partial in partials]]
    pallas_call x5 -> x6, Pallas kernels: 55.7 us -> 54.1 us  [the longest x3 44.2 us: expert_call(): pl.pallas_call(functools.partial(expert_kernel, based=base is not None),...]
    ppermute x4 -> x6, waiting for transfers between devices: 45.1 us -> 45.8 us  [the longest x1 43.3 us: body(): far_share = lax.ppermute(far_share, outer, swap)]
  transfers between devices with their start and end apart: 5 -> 7, of which waited for: 4 -> 3; matrix products, arithmetic and copies ran while one was open for 6% -> 2% of each run, Pallas kernels for 33% -> 41%
where the time goes in v2:
time: 231 us; the launch traced here: 230 us
  Pallas kernels  98.6 us (43%)
  blocking collectives  55.7 us (24%)
  waiting for transfers between devices  49.6 us (21%)
  between operations  13.5 us (6%)
  starting transfers between devices  6.99 us (3%)
  local copies, waits for them, and re-layouts  5.22 us (2%)
    all_to_all x1, blocking collectives, body(): lax.all_to_all(mixed.reshape(peers, tokens // peers, channels), 'tp', spl...  45 us
    pallas_call x3, Pallas kernels, expert_call(): pl.pallas_call(functools.partial(expert_kernel, based=base is not None),...  44.2 us
    ppermute x1, waiting for transfers between devices, body(): far_share = lax.ppermute(far_share, outer, swap)  43.3 us
    pallas_call x1, Pallas kernels, scan_call(): pl.pallas_call(scan_kernel, grid=(tokens // span,), in_specs=[block, bloc...  25.2 us
    all_gather x1, blocking collectives, body(): pieces = lax.all_gather(final, sp)  10.7 us
    pallas_call x1, Pallas kernels, project_call(): pl.pallas_call(project_kernel, grid=(rows // span,), in_specs=[pl.BlockSp...  9.95 us
    pallas_call x3, Pallas kernels, combine_call(): pl.pallas_call(combine_kernel, grid=(answer.shape[0] // span,), in_specs=...  9.86 us
    pallas_call x1, Pallas kernels, gate_call(): pl.pallas_call(gate_kernel, grid=(tokens // span,), in_specs=[pl.BlockSpe...  6.55 us
  transfers between devices with their start and end apart: 7, of which 3 were waited for; matrix products, arithmetic and copies ran while one was open for 2% of the time, Pallas kernels for 41%

profile of v2, /device:TPU:8, one launch (start us, length us, event | category | flops | bytes accessed | tf_op | source)
XLA Modules:
  0.0 229.7 jit_solution(15772481092910596718)
XLA Ops:
  6.5 0.0 copy-start.9
  6.5 0.0 all-gather.4.cloned.1.call-start
  6.5 2.8 %pack.1 = bf16[3072,256]{1,0:T(8,128)(2,1)} custom-call(bf16[1,2048,128]{2,1,0:T(8,128)(2,1)} %gate_ref.3, bf16[1,2048,128]{2,1,0:T(8,128)(2,1)} %up_ref.3, bf16[1,2048,128]{2,1,0:T(8,128)(2,1)} %down_ref.3), custom_call_target="tpu_custom_call" | custom-call | bytes 3145728 | tf_op jit(solution)/shard_map/pack/pallas_call | solution.py:262
  9.4 0.0 all-gather.4.cloned.1.call-update
  9.4 0.0 copy-done.9
  9.4 0.6 reshape_tile.3.gain_ref
  10.0 25.2 %scan.1 = (f32[4096,128]{1,0:T(8,128)}, f32[4096,128]{1,0:T(8,128)}, f32[136,128]{1,0:T(8,128)}) custom-call(bf16[4096,128]{1,0:T(8,128)(2,1)} %q_ref.1, bf16[4096,128]{1,0:T(8,128)(2,1)} %f_ref.1, bf16[4096,128]{1,0:T(8,128)(2,1)} %v_ref.1, f32[1,128]{1,0:T(1,128)} %bitcast.26, f32[2,4096]{1,0:T(2,128)} %sudden_ref.1), custom_call_target="tpu_custom_call" | custom-call | flops 1048576000 | bytes 7340032 | tf_op jit(solution)/shard_map/scan/pallas_call | solution.py:122
  35.2 10.7 %all-gather = f32[544,128]{1,0:T(8,128)} all-gather(f32[136,128]{1,0:T(8,128)} %get-tuple-element.17), channel_id=2, replica_groups=mesh['far'=2,'near'=2,'tp'=8] {'far','near'}, dimensions={0}, use_global_device_ids=true | all-gather | bytes 348160 | tf_op jit(solution)/shard_map/all_gather | solution.py:471
  45.9 0.0 copy-start.3
  45.9 0.0 copy-start.4
  45.9 0.0 copy-start.5
  45.9 6.5 %gate.1 = bf16[4096,128]{1,0:T(8,128)(2,1)} custom-call(s32[1]{0:T(128)} %bitcast.mine_ref, f32[4096,128]{1,0:T(8,128)} %get-tuple-element.15.local_ref, f32[4096,128]{1,0:T(8,128)} %get-tuple-element.16.lifted_ref, bf16[4096,128]{1,0:T(8,128)(2,1)} %open_ref.1, f32[4,136,128]{2,1,0:T(8,128)} %bitcast.18, f32[1,128]{1,0:T(1,128)} %reshape_tile.3.gain_ref), custom_call_target="tpu_custom_call" | custom-call | flops 419430400 | bytes 5242880 | tf_op jit(solution)/shard_map/gate/pallas_call | solution.py:172
  52.5 0.0 copy-start.1
  52.5 0.0 copy-start.2
  52.5 45.0 %all_to_all.5.mixed_ref = bf16[8,512,128]{2,1,0:T(8,128)(2,1)S(1)} all-to-all(bf16[8,512,128]{2,1,0:T(8,128)(2,1)} %bitcast.17), channel_id=1, replica_groups=mesh['far'=2,'near'=2,'tp'=8] {'tp'}, dimensions={0} | all-to-all | bytes 2097152 | tf_op jit(solution)/shard_map/all_to_all | solution.py:475
  97.5 0.0 copy-done.3
  97.5 0.0 copy-done.4
  97.5 0.0 copy-done.5
  97.5 0.0 copy-done.1
  97.5 0.0 copy-done.2
  97.5 10.0 %project.1 = (bf16[512,2048]{1,0:T(8,128)(2,1)}, bf16[512,2048]{1,0:T(8,128)(2,1)}, f32[512,2048]{1,0:T(8,128)}) custom-call(bf16[8,512,128]{2,1,0:T(8,128)(2,1)S(1)} %all_to_all.5.mixed_ref, bf16[1024,2048]{1,0:T(8,128)(2,1)} %weight_ref.1, bf16[512,2048]{1,0:T(8,128)(2,1)} %residual_ref.1, f32[1,2048]{1,0:T(1,128)S(1)} %bitcast.12, ...), custom_call_target="tpu_custom_call" | custom-call | flops 3758096384 | bytes 16777216 | tf_op jit(solution)/shard_map/project/pallas_call | solution.py:228
  107.5 0.0 copy-start
  107.5 0.0 copy-start.7
  107.5 0.0 copy-start.8
  107.5 2.7 %slice.18 = bf16[320,2048]{1,0:T(8,128)(2,1)} slice(bf16[512,2048]{1,0:T(8,128)(2,1)} %get-tuple-element.22.refs_0_), slice={[192:512], [0:2048]} | slice | bytes 2621440 | tf_op jit(solution)/shard_map/slice | solution.py:507
  110.2 1.3 collective-permute-start
  111.4 0.0 copy-done
  111.4 0.9 slice.19
  112.4 0.8 collective-permute-start.1
  113.1 0.0 copy-done.7
  113.1 0.0 copy-done.8
  113.2 1.3 collective-permute-start.2
  114.6 43.3 %collective-permute-done.2 = f32[8,512]{1,0:T(8,128)S(1)} collective-permute-done((f32[8,512]{1,0:T(8,128)S(1)}, f32[8,512]{1,0:T(8,128)S(1)}, u32[]{:S(2)}, u32[]{:S(2)}) %collective-permute-start.2) | collective-permute-done | bytes 16416 | tf_op jit(solution)/shard_map/ppermute | solution.py:466
  157.9 0.1 slice.23.refs_1_
  157.9 0.0 collective-permute-done.1.refs_0_
  157.9 3.8 %all-gather.4.cloned.1.call-done = bf16[49152,256]{1,0:T(8,128)(2,1)} async-done(((bf16[3072,256]{1,0:T(8,128)(2,1)}), bf16[49152,256]{1,0:T(8,128)(2,1)}) %all-gather.4.cloned.1.call-update) | async-done | bytes 25165840 | tf_op jit(solution)/shard_map/all_gather | solution.py:451
  161.7 10.7 %far0.1 = bf16[192,2048]{1,0:T(8,128)(2,1)S(1)} custom-call(bf16[192,2048]{1,0:T(8,128)(2,1)S(1)} %collective-permute-done.1.refs_0_, f32[8,192]{1,0:T(8,128)S(1)} %slice.22.refs_1_, bf16[2,8,3072,256]{3,2,1,0:T(8,128)(2,1)} %bitcast.14), custom_call_target="tpu_custom_call" | custom-call | flops 4831838208 | bytes 25165824 | tf_op jit(solution)/shard_map/far0/pallas_call | solution.py:324
  172.4 1.5 collective-permute-start.3
  174.0 0.0 collective-permute-done.refs_0_
  174.0 13.0 %far1.1 = (bf16[128,2048]{1,0:T(8,128)(2,1)S(1)}, bf16[192,2048]{1,0:T(8,128)(2,1)S(1)}) custom-call(bf16[320,2048]{1,0:T(8,128)(2,1)} %collective-permute-done.refs_0_, f32[8,320]{1,0:T(8,128)S(1)} %slice.23.refs_1_, bf16[2,8,3072,256]{3,2,1,0:T(8,128)(2,1)} %bitcast.15), custom_call_target="tpu_custom_call" | custom-call | flops 8053063680 | bytes 25165824 | tf_op jit(solution)/shard_map/far1/pallas_call | solution.py:324
  187.0 0.6 collective-permute-start.4
  187.6 1.5 collective-permute-start.5
  189.1 20.5 %own.1.refs_1_.refs_2_ = f32[512,2048]{1,0:T(8,128)} custom-call(bf16[512,2048]{1,0:T(8,128)(2,1)S(1)} %copy-done, f32[8,512]{1,0:T(8,128)S(1)} %concatenate.9.refs_1_, bf16[2,8,3072,256]{3,2,1,0:T(8,128)(2,1)} %bitcast.16, f32[512,2048]{1,0:T(8,128)} %get-tuple-element.23.refs_3_), custom_call_target="tpu_custom_call" | custom-call | flops 12884901888 | bytes 25165824 | tf_op jit(solution)/shard_map/own/pallas_call | solution.py:324
  209.6 0.0 collective-permute-done.3.refs_2_
  209.6 0.0 copy-start.6
  209.6 0.9 copy-done.6
  210.5 3.7 %combine0.1.refs_0_ = bf16[512,2048]{1,0:T(8,128)(2,1)} custom-call(bf16[512,2048]{1,0:T(8,128)(2,1)} %get-tuple-element.18.refs_0_.refs_1_, f32[512,2048]{1,0:T(8,128)} %own.1.refs_1_.refs_2_, bf16[192,2048]{1,0:T(8,128)(2,1)} %copy-done.6, f32[1,2048]{1,0:T(1,128)} %bitcast.19), custom_call_target="tpu_custom_call" | custom-call | flops 393216 | bytes 3932160 | tf_op jit(solution)/shard_map/combine0/pallas_call | solution.py:360
  214.2 0.0 collective-permute-done.4.refs_3_
  214.2 3.7 %combine320.1.refs_0_ = bf16[512,2048]{1,0:T(8,128)(2,1)} custom-call(bf16[512,2048]{1,0:T(8,128)(2,1)} %combine0.1.refs_0_, bf16[512,2048]{1,0:T(8,128)(2,1)} %get-tuple-element.18.refs_0_.refs_1_, f32[512,2048]{1,0:T(8,128)} %own.1.refs_1_.refs_2_, bf16[192,2048]{1,0:T(8,128)(2,1)} %collective-permute-done.4.refs_3_, ...), custom_call_target="tpu_custom_call", output_to_operand_aliasing={{}: (0, {})} | custom-call | flops 393216 | bytes 3932160 | tf_op jit(solution)/shard_map/combine320/pallas_call | solution.py:360
  217.9 2.5 %collective-permute-done.5.refs_3_ = bf16[128,2048]{1,0:T(8,128)(2,1)} collective-permute-done((bf16[128,2048]{1,0:T(8,128)(2,1)S(1)}, bf16[128,2048]{1,0:T(8,128)(2,1)}, u32[]{:S(2)}, u32[]{:S(2)}) %collective-permute-start.5) | collective-permute-done | bytes 524320 | tf_op jit(solution)/shard_map/ppermute | solution.py:513
  220.4 2.4 %combine192.1 = bf16[512,2048]{1,0:T(8,128)(2,1)} custom-call(bf16[512,2048]{1,0:T(8,128)(2,1)} %combine320.1.refs_0_, bf16[512,2048]{1,0:T(8,128)(2,1)} %get-tuple-element.18.refs_0_.refs_1_, f32[512,2048]{1,0:T(8,128)} %own.1.refs_1_.refs_2_, bf16[128,2048]{1,0:T(8,128)(2,1)} %collective-permute-done.5.refs_3_, ...), custom_call_target="tpu_custom_call", output_to_operand_aliasing={{}: (0, {})} | custom-call | flops 262144 | bytes 2621440 | tf_op jit(solution)/shard_map/combine192/pallas_call | solution.py:360
  (6 shorter events, 0.1 us)
Async XLA Ops:
  6.5 2.9 %copy-start.9 = (f32[64]{0:T(128)S(1)}, f32[64]{0:T(128)}, u32[]{:S(2)}) copy-start(f32[64]{0:T(128)} %param.27) | copy-start | bytes 772
  6.5 155.2 %all-gather.4.cloned.1.call-start = ((), (), s32[]{:S(2)}) async-start(), calls=%async_computation.1 | async-start | bytes 26738688 | tf_op jit(solution)/shard_map/all_gather | solution.py:451
  45.9 51.6 %copy-start.3 = (bf16[256,2048]{1,0:T(8,128)(2,1)S(1)}, bf16[256,2048]{1,0:T(8,128)(2,1)}, u32[]{:S(2)}) copy-start(bf16[256,2048]{1,0:T(8,128)(2,1)} %down_ref.2) | copy-start | bytes 3145732
  45.9 51.6 %copy-start.4 = (f32[2048]{0:T(1024)S(1)}, f32[2048]{0:T(1024)}, u32[]{:S(2)}) copy-start(f32[2048]{0:T(1024)} %param.29) | copy-start | bytes 24580
  45.9 51.6 %copy-start.5 = (f32[2048]{0:T(1024)S(1)}, f32[2048]{0:T(1024)}, u32[]{:S(2)}) copy-start(f32[2048]{0:T(1024)} %param.30) | copy-start | bytes 24580
  52.5 45.1 %copy-start.1 = (bf16[2048,256]{1,0:T(8,128)(2,1)S(1)}, bf16[2048,256]{1,0:T(8,128)(2,1)}, u32[]{:S(2)}) copy-start(bf16[2048,256]{1,0:T(8,128)(2,1)} %gate_ref.2) | copy-start | bytes 3145732
  52.5 45.1 %copy-start.2 = (bf16[2048,256]{1,0:T(8,128)(2,1)S(1)}, bf16[2048,256]{1,0:T(8,128)(2,1)}, u32[]{:S(2)}) copy-start(bf16[2048,256]{1,0:T(8,128)(2,1)} %up_ref.2) | copy-start | bytes 3145732
  107.5 4.0 %copy-start = (bf16[512,2048]{1,0:T(8,128)(2,1)S(1)}, bf16[512,2048]{1,0:T(8,128)(2,1)}, u32[]{:S(2)}) copy-start(bf16[512,2048]{1,0:T(8,128)(2,1)} %get-tuple-element.22.refs_0_) | copy-start | bytes 6291460
  107.5 5.6 %copy-start.7 = (f32[512,2]{0,1:T(2,128)S(1)}, f32[512,2]{0,1:T(2,128)}, u32[]{:S(2)}) copy-start(f32[512,2]{0,1:T(2,128)} %param.32) | copy-start | bytes 12292
  107.5 5.6 %copy-start.8 = (s32[512,2]{0,1:T(2,128)S(1)}, s32[512,2]{0,1:T(2,128)}, u32[]{:S(2)}) copy-start(s32[512,2]{0,1:T(2,128)} %param.31) | copy-start | bytes 12292
  110.2 63.8 %collective-permute-start = (bf16[320,2048]{1,0:T(8,128)(2,1)}, bf16[320,2048]{1,0:T(8,128)(2,1)}, u32[]{:S(2)}, u32[]{:S(2)}) collective-permute-start(bf16[320,2048]{1,0:T(8,128)(2,1)} %slice.18), channel_id=1, source_target_pairs={{0,16},{16,0},{1,17},{17,1},{2,18},{18,2},{3,19},{19,3},{4,20},{20... | collective-permute-start | bytes 3932168 | tf_op jit(solution)/shard_map/ppermute | solution.py:507
  112.4 45.6 %collective-permute-start.1 = (bf16[192,2048]{1,0:T(8,128)(2,1)}, bf16[192,2048]{1,0:T(8,128)(2,1)S(1)}, u32[]{:S(2)}, u32[]{:S(2)}) collective-permute-start(bf16[192,2048]{1,0:T(8,128)(2,1)} %slice.19), channel_id=1, source_target_pairs={{0,16},{16,0},{1,17},{17,1},{2,18},{18,2},{3,19},{19,3},{4,20},{20... | collective-permute-start | bytes 2359304 | tf_op jit(solution)/shard_map/ppermute | solution.py:506
  113.2 44.7 %collective-permute-start.2 = (f32[8,512]{1,0:T(8,128)S(1)}, f32[8,512]{1,0:T(8,128)S(1)}, u32[]{:S(2)}, u32[]{:S(2)}) collective-permute-start(f32[8,512]{1,0:T(8,128)S(1)} %concatenate.8), channel_id=1, source_target_pairs={{0,16},{16,0},{1,17},{17,1},{2,18},{18,2},{3,19},{19,3},{4,20},{20... | collective-permute-start | bytes 49160 | tf_op jit(solution)/shard_map/ppermute | solution.py:466
  172.4 37.2 %collective-permute-start.3 = (bf16[192,2048]{1,0:T(8,128)(2,1)S(1)}, bf16[192,2048]{1,0:T(8,128)(2,1)S(1)}, u32[]{:S(2)}, u32[]{:S(2)}) collective-permute-start(bf16[192,2048]{1,0:T(8,128)(2,1)S(1)} %far0.1), channel_id=1, source_target_pairs={{0,16},{16,0},{1,17},{17,1},{2,18},{18,2},{3,19},{19,3},{4,20},{20... | collective-permute-start | bytes 2359304 | tf_op jit(solution)/shard_map/ppermute | solution.py:509
  187.0 27.2 %collective-permute-start.4 = (bf16[192,2048]{1,0:T(8,128)(2,1)S(1)}, bf16[192,2048]{1,0:T(8,128)(2,1)}, u32[]{:S(2)}, u32[]{:S(2)}) collective-permute-start(bf16[192,2048]{1,0:T(8,128)(2,1)S(1)} %get-tuple-element.21), channel_id=1, source_target_pairs={{0,16},{16,0},{1,17},{17,1},{2,18},{18,2},{3,19},{19,3},{4,20},{20... | collective-permute-start | bytes 2359304 | tf_op jit(solution)/shard_map/ppermute | solution.py:513
  187.6 32.8 %collective-permute-start.5 = (bf16[128,2048]{1,0:T(8,128)(2,1)S(1)}, bf16[128,2048]{1,0:T(8,128)(2,1)}, u32[]{:S(2)}, u32[]{:S(2)}) collective-permute-start(bf16[128,2048]{1,0:T(8,128)(2,1)S(1)} %get-tuple-element.24), channel_id=1, source_target_pairs={{0,16},{16,0},{1,17},{17,1},{2,18},{18,2},{3,19},{19,3},{4,20},{20... | collective-permute-start | bytes 1572872 | tf_op jit(solution)/shard_map/ppermute | solution.py:513
  209.6 0.9 copy-start.6
Sparse Core Ops, SparseCore 0:
  9.5 152.1 all-gather.3

commit v3 on v2

--- a/solution.py
+++ b/solution.py
@@ -6,6 +6,7 @@
 from jax.experimental import pallas as pl
 from jax.experimental.pallas import tpu as pltpu
 from jax.sharding import Mesh, PartitionSpec as P
+
 
 HEAD_CHANNELS = 64
 BLOCK = 64
@@ -145,11 +146,12 @@
 
 
 def gate_kernel(mine_ref, local_ref, lifted_ref, open_ref, pieces_ref, gain_ref, mixed_ref):
-    span, channels = local_ref.shape
+    _, channels = local_ref.shape
     mine = mine_ref[0]
     incoming = jnp.zeros((channels, channels), F32)
     for j in range(pieces_ref.shape[0] - 1):
-        longer = incoming * pieces_ref[j, channels : channels + 1, :] + pieces_ref[j, 0:channels, :]
+        at = mine_ref[1 + j]
+        longer = incoming * pieces_ref[at, channels : channels + 1, :] + pieces_ref[at, 0:channels, :]
         incoming = jnp.where(j < mine, longer, incoming)
     heads_out = local_ref[...] + fine_mm(halves(lifted_ref[...]), halves(incoming))
     own_head = (
@@ -248,94 +250,116 @@
     )(mixed, weight, residual, *vectors, *shared_weights)
 
 
-def pack_kernel(gate_ref, up_ref, down_ref, packed_ref):
+def pack_kernel(gate_ref, up_ref, down_ref, upper_ref, lower_ref):
     width, units = gate_ref.shape[1:]
-    packed_ref[0:width, 0:units] = gate_ref[0]
-    packed_ref[0:width, units:] = up_ref[0]
+    half = upper_ref.shape[0]
+    upper_ref[:, 0:units] = gate_ref[0, 0:half, :]
+    upper_ref[:, units:] = up_ref[0, 0:half, :]
+    lower_ref[0 : width - half, 0:units] = gate_ref[0, half:, :]
+    lower_ref[0 : width - half, units:] = up_ref[0, half:, :]
     for j in range(width // (2 * units)):
         turned = down_ref[0, j * 2 * units : (j + 1) * 2 * units, :].T
-        packed_ref[width + j * units : width + (j + 1) * units, :] = turned
+        lower_ref[width - half + j * units : width - half + (j + 1) * units, :] = turned
 
 
 def pack_call(gate, up, down):
     _, width, units = gate.shape
     return pl.pallas_call(
         pack_kernel,
-        out_shape=jax.ShapeDtypeStruct((width + width // 2, 2 * units), gate.dtype),
+        out_shape=[jax.ShapeDtypeStruct((3 * width // 4, 2 * units), gate.dtype)] * 2,
         cost_estimate=pl.CostEstimate(flops=0, bytes_accessed=12 * width * units, transcendentals=0),
         name="pack",
     )(gate, up, down)
 
 
-def expert_kernel(*refs, based):
-    rows_ref, share_ref, weights_ref = refs[:3]
-    out_refs, sum_ref = refs[3 + based : -1], refs[-1]
-    expert, piece = pl.program_id(0), pl.program_id(1)
-    first = jnp.logical_and(expert == 0, piece == 0)
-    last = jnp.logical_and(expert == pl.num_programs(0) - 1, piece == pl.num_programs(1) - 1)
+def expert_kernel(*refs, based, sources):
+    which_ref, rows_ref, share_ref = refs[:3]
+    piece_refs = refs[3 + based : 3 + based + len(sources)]
+    out_refs = refs[3 + based + len(sources) : -4]
+    held_ref, sum_ref, wide_ref, sems = refs[-4:]
     width = rows_ref.shape[1]
-    shards, _, double = weights_ref.shape[1:]
+    pieces, _, double = held_ref.shape
     units = double // 2
-
-    @pl.when(first)
-    def _():
-        sum_ref[...] = jnp.zeros_like(sum_ref)
-
+    for ref, (slot, start) in zip(piece_refs, sources):
+        into = held_ref.at[slot, start : start + ref.shape[0]]
+        pltpu.make_async_copy(ref, into, sems.at[slot]).start()
+    sum_ref[...] = jnp.zeros_like(sum_ref)
     share = share_ref[...].T
-    lanes = lax.broadcasted_iota(jnp.int32, share.shape, 1)
-    share = jnp.sum(jnp.where(lanes == expert, share, 0.0), axis=1, keepdims=True)
-    hidden = []
-    for j in range(shards):
-        both = mm(rows_ref[...], weights_ref[0, j, 0:width, :])
-        gate, up = both[:, :units], both[:, units:]
-        hidden.append((gate * jax.nn.sigmoid(gate) * up * share).astype(BF16))
-    hidden = jnp.concatenate(hidden, axis=1)
-    for c in range(width // double):
-        at = slice(width + c * units, width + (c + 1) * units)
-        down = jnp.concatenate([weights_ref[0, j, at, :] for j in range(shards)], axis=0)
-        sum_ref[:, c * double : (c + 1) * double] += mm(hidden, down)
-
-    @pl.when(last)
-    def _():
-        start = 0
-        for out_ref in out_refs:
-            at = slice(start, start + out_ref.shape[0])
-            total = sum_ref[at, :] + refs[3][at, :] if based else sum_ref[at, :]
-            out_ref[...] = total.astype(out_ref.dtype)
-            start += out_ref.shape[0]
-
-
-def expert_call(rows, share, weights, base, pieces, kind, name, together):
+    for e in range(wide_ref.shape[0]):
+        wide_ref[e] = jnp.broadcast_to(share[:, e : e + 1], wide_ref.shape[1:])
+
+    for g in range(pieces // TOGETHER):
+        slots = range(g * TOGETHER, (g + 1) * TOGETHER)
+        for slot in slots:
+            pltpu.make_async_copy(held_ref.at[slot], held_ref.at[slot], sems.at[slot]).wait()
+        hidden = []
+        for slot in slots:
+            part = wide_ref[which_ref[slot]]
+            both = mm(rows_ref[...], held_ref[slot, 0:width, :])
+            gate, up = both[:, :units], both[:, units:]
+            hidden.append((gate * jax.nn.sigmoid(gate) * up * part).astype(BF16))
+        hidden = jnp.concatenate(hidden, axis=1)
+        for c in range(width // double):
+            at = slice(width + c * units, width + (c + 1) * units)
+            down = jnp.concatenate([held_ref[slot, at, :] for slot in slots], axis=0)
+            sum_ref[:, c * double : (c + 1) * double] += mm(hidden, down)
+    start = 0
+    for out_ref in out_refs:
+        at = slice(start, start + out_ref.shape[0])
+        total = sum_ref[at, :] + refs[3][at, :] if based else sum_ref[at, :]
+        out_ref[...] = total.astype(out_ref.dtype)
+        start += out_ref.shape[0]
+
+
+TOGETHER = 2
+
+
+def expert_call(which, rows, share, held, base, sizes, kind):
     count, width = rows.shape
-    experts, shards, depth, double = weights.shape
-
-    def whole(size):
-        return pl.BlockSpec((size, width), lambda e, s: (0, 0))
-
-    specs = [
-        whole(count),
-        pl.BlockSpec(share.shape, lambda e, s: (0, 0)),
-        pl.BlockSpec((1, together, depth, double), lambda e, s: (e, s, 0, 0)),
-    ]
-    operands = [rows, share, weights]
+    arrays = [array for array, _, _ in held]
+    sources = [(slot, start) for _, slot, start in held]
+    double = arrays[0].shape[1]
+    depth = width + width // 2
+    pieces = 1 + max(slot for slot, _ in sources)
+    specs = [pl.BlockSpec(memory_space=pltpu.SMEM)] + [pl.BlockSpec(memory_space=pltpu.VMEM)] * 2
+    operands = [which, rows, share]
     if base is not None:
-        specs.append(whole(count))
+        specs.append(pl.BlockSpec(memory_space=pltpu.VMEM))
         operands.append(base)
+    specs += [pl.BlockSpec(memory_space=pltpu.HBM)] * len(arrays)
     return pl.pallas_call(
-        functools.partial(expert_kernel, based=base is not None),
-        grid=(experts, shards // together),
+        functools.partial(expert_kernel, based=base is not None, sources=sources),
         in_specs=specs,
-        out_specs=[whole(size) for size in pieces],
-        out_shape=[jax.ShapeDtypeStruct((size, width), kind) for size in pieces],
-        scratch_shapes=[pltpu.VMEM((count, width), F32)],
-        compiler_params=pltpu.CompilerParams(
-            dimension_semantics=("arbitrary", "arbitrary"), vmem_limit_bytes=48 * 1024 * 1024
+        out_specs=[pl.BlockSpec(memory_space=pltpu.VMEM)] * len(sizes),
+        out_shape=[jax.ShapeDtypeStruct((size, width), kind) for size in sizes],
+        scratch_shapes=[
+            pltpu.VMEM((pieces, depth, double), BF16),
+            pltpu.VMEM((count, width), F32),
+            pltpu.VMEM((2, count, double // 2), F32),
+            pltpu.SemaphoreType.DMA((pieces,)),
+        ],
+        compiler_params=pltpu.CompilerParams(vmem_limit_bytes=60 * 1024 * 1024),
+        cost_estimate=pl.CostEstimate(
+            flops=2 * count * pieces * depth * double,
+            bytes_accessed=2 * pieces * depth * double,
+            transcendentals=0,
         ),
-        cost_estimate=pl.CostEstimate(
-            flops=2 * count * weights.size, bytes_accessed=2 * weights.size, transcendentals=0
-        ),
-        name=name,
-    )(*operands)
+    )(*operands, *arrays)
+
+
+def ring_hops(columns, peers):
+    long = peers // 2
+    size = columns * long
+
+    def device(r, core):
+        column, level = (0, r) if r < long else (1, size - 1 - r)
+        return column * peers + level * 2 + core
+
+    def shift(by):
+        return [(device(r, c), device((r + by) % size, c)) for r in range(size) for c in (0, 1)]
+
+    swap = [(z * 2 + c, z * 2 + 1 - c) for z in range(long) for c in (0, 1)]
+    return shift(1), shift(-1), swap
 
 
 def combine_kernel(*refs):
@@ -368,7 +392,6 @@
         cost_estimate=pl.CostEstimate(
             flops=answer.size, bytes_accessed=10 * answer.size, transcendentals=0
         ),
-        name="combine%d" % start,
     )(*operands)
 
 
@@ -447,9 +470,25 @@
     paired = len(sp) == 2
     if paired:
         outer, inner = sp
-        packed = pack_call(expert_gate_matrix, expert_up_matrix, expert_down_matrix)
-        held = lax.all_gather(packed, (inner, "tp"))
-        held = held.reshape((lax.axis_size(inner), peers) + packed.shape)
+        ring = (inner, "tp")
+        forward, backward, partner = ring_hops(lax.axis_size(inner), peers)
+        upper, lower = pack_call(expert_gate_matrix, expert_up_matrix, expert_down_matrix)
+        hops = {"long": ([upper], [lower]), "short": ([lower], [upper])}
+
+        def hop(kind):
+            for perm, chain in zip((forward, backward), hops[kind]):
+                chain.append(lax.ppermute(chain[-1], ring, perm))
+
+        hop("long")
+        hop("short")
+        level = lax.axis_index("tp") // 2
+        size = peers
+        place = jnp.where(lax.axis_index(inner) == 0, level, size - 1 - level)
+        origin = [place, place]
+        for k in range(1, size // 2):
+            origin += [place - k, place - k, place + k, place + k]
+        origin += [place + size // 2] * 2
+        which = ((jnp.stack(origin) % size) >= size // 2).astype(jnp.int32)
         experts_all = lax.axis_size(outer) * lax.axis_size(inner)
         share = jnp.stack(
             [
@@ -468,13 +507,27 @@
     local, lifted, final = scan_call(
         query_values, forget_preact, value_written, forget_margin, sudden_decay
     )
-    pieces = lax.all_gather(final, sp)
-    mine = lax.axis_index(sp).reshape(1)
+    mine = lax.axis_index(sp)
+    if paired:
+        others = [
+            lax.ppermute(final, sp, [(i, i ^ other) for i in range(4)]) for other in (1, 2, 3)
+        ]
+        pieces = jnp.stack([final] + others)
+        order = mine ^ jnp.arange(4)
+        hop("long")
+        hop("short")
+    else:
+        pieces = lax.all_gather(final, sp)
+        order = jnp.arange(pieces.shape[0])
+    mine = jnp.concatenate([mine.reshape(1), order])
     gain = jnp.tile(head_norm_gain, channels // HEAD_CHANNELS).reshape(1, channels)
     mixed = gate_call(mine, local, lifted, output_gate_preact, pieces, gain)
     mixed = lax.all_to_all(
         mixed.reshape(peers, tokens // peers, channels), "tp", split_axis=0, concat_axis=0, tiled=True
     )
+    if paired:
+        hop("long")
+        hop("short")
     if channels % 128 == 0:
         stream, normed, shared = project_call(
             mixed,
@@ -505,14 +558,33 @@
     first = 3 * rows // 8
     far_first = lax.ppermute(normed[:first], outer, swap)
     far_rest = lax.ppermute(normed[first:], outer, swap)
-    (partial,) = expert_call(far_first, far_share[:, :first], held, None, (first,), BF16, "far0", 4)
+    hop("long")
+
+    held = []
+
+    def hold(slot, start, array):
+        held.append((array, slot, start))
+        held.append((lax.ppermute(array, "tp", partner), slot + 1, start))
+
+    half = upper.shape[0]
+    (long_a, long_b), (short_a, short_b) = hops["long"], hops["short"]
+    hold(0, 0, upper)
+    hold(0, half, lower)
+    for k in range(1, 4):
+        hold(4 * k - 2, 0, long_a[k])
+        hold(4 * k - 2, half, short_a[k])
+        hold(4 * k, 0, short_b[k])
+        hold(4 * k, half, long_b[k])
+    hold(14, 0, long_a[4])
+    hold(14, half, long_b[4])
+    (partial,) = expert_call(which, far_first, far_share[:, :first], held, None, (first,), BF16)
     answers = [lax.ppermute(partial, outer, swap)]
     far_rest, _ = lax.optimization_barrier((far_rest, partial))
     sizes = (rows - 2 * first, first)
-    partials = expert_call(far_rest, far_share[:, first:], held, None, sizes, BF16, "far1", 4)
+    partials = expert_call(which, far_rest, far_share[:, first:], held, None, sizes, BF16)
     answers += [lax.ppermute(partial, outer, swap) for partial in partials]
     own_rows, _ = lax.optimization_barrier((normed, partials[1]))
-    (base,) = expert_call(own_rows, own_share, held, shared, (rows,), F32, "own", 2)
+    (base,) = expert_call(which, own_rows, own_share, held, shared, (rows,), F32)
     layer_out = None
     starts = (0, first, first + sizes[0])
     for c in (0, 2, 1):
@@ -552,6 +624,8 @@
         P(),
         P(),
     )
-    return jax.shard_map(
-        functools.partial(body, sp=sp), mesh=mesh, in_specs=placed, out_specs=every, check_vma=False
-    )
+
+    def step(*arrays):
+        return body(*arrays, sp=sp)
+
+    return jax.shard_map(step, mesh=mesh, in_specs=placed, out_specs=every, check_vma=False)

time: 231 us -> 267 us (1.16)
  waiting for transfers between devices: 49.6 us -> 117 us
  blocking collectives: 55.7 us -> 0 us
  starting transfers between devices: 6.99 us -> 32.2 us
  between operations: 13.5 us -> 0.27 us
  local copies, waits for them, and re-layouts: 5.22 us -> 10.8 us
  other arithmetic: 0.05 us -> 2.92 us
    ppermute x0 -> x33, waiting for transfers between devices: none -> 87 us  [the longest x14 83.9 us: hop(): chain.append(lax.ppermute(chain[-1], ring, perm))]
    all_to_all x1 -> x0, blocking collectives: 45 us -> none  [body(): lax.all_to_all(mixed.reshape(peers, tokens // peers, channels), 'tp', spl...]
    ppermute x1, waiting for transfers between devices: 43.3 us -> 3.23 us  [body(): far_share = lax.ppermute(far_share, outer, swap)]
    ppermute x0 -> x33, starting transfers between devices: none -> 20.4 us  [the longest x14 13.9 us: hop(): chain.append(lax.ppermute(chain[-1], ring, perm))]
    ppermute x1, waiting for transfers between devices: 0.01 us -> 14.4 us  [body(): far_first = lax.ppermute(normed[:first], outer, swap)]
    ppermute x1, waiting for transfers between devices: 0.01 us -> 12.1 us  [body(): far_rest = lax.ppermute(normed[first:], outer, swap)]
    all_gather x1 -> x0, blocking collectives: 10.7 us -> none  [body(): pieces = lax.all_gather(final, sp)]
    all_to_all x0 -> x1, starting transfers between devices: none -> 5.53 us  [body(): lax.all_to_all(mixed.reshape(peers, tokens // peers, channels), 'tp', spl...]
  transfers between devices with their start and end apart: 7 -> 40, of which waited for: 3 -> 12; matrix products, arithmetic and copies ran while one was open for 2% -> 3% of each run, Pallas kernels for 41% -> 36%
where the time goes in v3:
time: 267 us; the launch traced here: 264 us
  waiting for transfers between devices  117 us (44%)
  Pallas kernels  101 us (38%)
  starting transfers between devices  32.2 us (12%)
  local copies, waits for them, and re-layouts  10.8 us (4%)
  other arithmetic  2.92 us (1%)
    ppermute x14, waiting for transfers between devices, hop(): chain.append(lax.ppermute(chain[-1], ring, perm))  83.9 us
    pallas_call x3, Pallas kernels, expert_call(): pl.pallas_call(functools.partial(expert_kernel, based=base is not None, s...  46.6 us
    pallas_call x1, Pallas kernels, scan_call(): pl.pallas_call(scan_kernel, grid=(tokens // span,), in_specs=[block, bloc...  25.2 us
    ppermute x1, waiting for transfers between devices, body(): far_first = lax.ppermute(normed[:first], outer, swap)  14.4 us
    ppermute x14, starting transfers between devices, hop(): chain.append(lax.ppermute(chain[-1], ring, perm))  13.9 us
    ppermute x1, waiting for transfers between devices, body(): far_rest = lax.ppermute(normed[first:], outer, swap)  12.1 us
    pallas_call x1, Pallas kernels, project_call(): pl.pallas_call(project_kernel, grid=(rows // span,), in_specs=[pl.BlockSp...  10 us
    pallas_call x3, Pallas kernels, combine_call(): pl.pallas_call(combine_kernel, grid=(answer.shape[0] // span,), in_specs=...  9.97 us
  transfers between devices with their start and end apart: 40, of which 12 were waited for; matrix products, arithmetic and copies ran while one was open for 3% of the time, Pallas kernels for 36%

profile of v3, /device:TPU:8, one launch (start us, length us, event | category | flops | bytes accessed | tf_op | source)
XLA Modules:
  0.0 264.0 jit_solution(16083351604283237866)
XLA Ops:
  0.0 2.8 %pack.1 = (bf16[1536,256]{1,0:T(8,128)(2,1)}, bf16[1536,256]{1,0:T(8,128)(2,1)}) custom-call(bf16[1,2048,128]{2,1,0:T(8,128)(2,1)} %gate_ref.3, bf16[1,2048,128]{2,1,0:T(8,128)(2,1)} %up_ref.3, bf16[1,2048,128]{2,1,0:T(8,128)(2,1)} %down_ref.3), custom_call_target="tpu_custom_call" | custom-call | bytes 3145728 | tf_op jit(solution)/shard_map/pack/pallas_call | solution.py:267
  2.9 2.0 collective-permute-start.8
  4.9 25.2 %scan.1 = (f32[4096,128]{1,0:T(8,128)}, f32[4096,128]{1,0:T(8,128)}, f32[136,128]{1,0:T(8,128)}) custom-call(bf16[4096,128]{1,0:T(8,128)(2,1)} %q_ref.1, bf16[4096,128]{1,0:T(8,128)(2,1)} %f_ref.1, bf16[4096,128]{1,0:T(8,128)(2,1)} %v_ref.1, f32[1,128]{1,0:T(1,128)} %bitcast.36, f32[2,4096]{1,0:T(2,128)} %sudden_ref.1), custom_call_target="tpu_custom_call" | custom-call | flops 1048576000 | bytes 7340032 | tf_op jit(solution)/shard_map/scan/pallas_call | solution.py:123
  30.1 2.5 collective-permute-start.2
  32.6 0.6 collective-permute-start.5
  33.2 3.2 %collective-permute-done.5 = f32[8,512]{1,0:T(8,128)S(1)} collective-permute-done((f32[8,512]{1,0:T(8,128)S(1)}, f32[8,512]{1,0:T(8,128)S(1)}, u32[]{:S(2)}, u32[]{:S(2)}) %collective-permute-start.5) | collective-permute-done | bytes 16416 | tf_op jit(solution)/shard_map/ppermute | solution.py:505
  36.5 1.2 collective-permute-start.1
  37.7 1.3 collective-permute-start
  39.0 2.0 collective-permute-done.1
  41.0 0.4 collective-permute-start.14
  41.4 0.8 collective-permute-done
  42.2 1.6 collective-permute-start.10
  43.8 0.5 collective-permute-start.20
  44.3 0.2 collective-permute-start.13
  44.6 0.7 pad_add_fusion.mine_ref
  45.2 0.6 reshape_tile.3.gain_ref
  45.8 15.7 %collective-permute-done.14.refs_13_.refs_14_ = bf16[1536,256]{1,0:T(8,128)(2,1)} collective-permute-done((bf16[1536,256]{1,0:T(8,128)(2,1)S(1)}, bf16[1536,256]{1,0:T(8,128)(2,1)}, u32[]{:S(2)}, u32[]{:S(2)}) %collective-permute-start.14) | collective-permute-done | bytes 786464 | tf_op jit(solution)/shard_map/ppermute | solution.py:480
  61.5 1.6 collective-permute-start.16
  63.1 0.5 collective-permute-start.22
  63.6 14.6 %collective-permute-done.20.refs_19_.refs_20_ = bf16[1536,256]{1,0:T(8,128)(2,1)S(1)} collective-permute-done((bf16[1536,256]{1,0:T(8,128)(2,1)}, bf16[1536,256]{1,0:T(8,128)(2,1)S(1)}, u32[]{:S(2)}, u32[]{:S(2)}) %collective-permute-start.20) | collective-permute-done | bytes 786464 | tf_op jit(solution)/shard_map/ppermute | solution.py:480
  78.3 1.6 pad_maximum_fusion.pieces_ref
  79.9 6.3 %gate.1 = bf16[4096,128]{1,0:T(8,128)(2,1)} custom-call(s32[5]{0:T(128)} %pad_add_fusion.mine_ref, f32[4096,128]{1,0:T(8,128)} %get-tuple-element.17.local_ref, f32[4096,128]{1,0:T(8,128)} %get-tuple-element.18.lifted_ref, bf16[4096,128]{1,0:T(8,128)(2,1)} %open_ref.1, f32[4,136,128]{2,1,0:T(8,128)} %pad_maximum_fusion.pieces_ref, f32[1,128]{1,0:T(1,128)} %reshape_tile.3.gain_ref), custom_call_target="tpu_custom_call" | custom-call | flops 419430400 | bytes 5242880 | tf_op jit(solution)/shard_map/gate/pallas_call | solution.py:174
  86.3 5.5 %all-to-all-start = ((bf16[8,512,128]{2,1,0:T(8,128)(2,1)}), bf16[8,512,128]{2,1,0:T(8,128)(2,1)S(1)}, u32[]{:S(2)}, u32[]{:S(2)}) async-start(bf16[8,512,128]{2,1,0:T(8,128)(2,1)} %bitcast.24), calls=%async_computation | async-start | bytes 2097152 | tf_op jit(solution)/shard_map/all_to_all | solution.py:525
  91.8 1.5 collective-permute-start.18
  93.3 0.6 collective-permute-start.28
  93.9 0.2 collective-permute-start.21
  94.1 1.5 collective-permute-start.24
  95.5 36.3 %collective-permute-done.18.refs_17_.refs_18_ = bf16[1536,256]{1,0:T(8,128)(2,1)} collective-permute-done((bf16[1536,256]{1,0:T(8,128)(2,1)}, bf16[1536,256]{1,0:T(8,128)(2,1)}, u32[]{:S(2)}, u32[]{:S(2)}) %collective-permute-start.18) | collective-permute-done | bytes 786464 | tf_op jit(solution)/shard_map/ppermute | solution.py:480
  131.9 1.9 collective-permute-done.28.refs_27_.refs_28_
  133.8 1.1 collective-permute-start.26
  135.0 13.8 %collective-permute-done.24.refs_23_.refs_24_ = bf16[1536,256]{1,0:T(8,128)(2,1)S(1)} collective-permute-done((bf16[1536,256]{1,0:T(8,128)(2,1)}, bf16[1536,256]{1,0:T(8,128)(2,1)S(1)}, u32[]{:S(2)}, u32[]{:S(2)}) %collective-permute-start.24) | collective-permute-done | bytes 786464 | tf_op jit(solution)/shard_map/ppermute | solution.py:480
  148.7 0.9 copy-done.13
  149.7 1.2 copy-done.2
  150.9 10.0 %project.1 = (bf16[512,2048]{1,0:T(8,128)(2,1)}, bf16[512,2048]{1,0:T(8,128)(2,1)}, f32[512,2048]{1,0:T(8,128)}) custom-call(bf16[8,512,128]{2,1,0:T(8,128)(2,1)S(1)} %all-to-all-done.mixed_ref, bf16[1024,2048]{1,0:T(8,128)(2,1)} %weight_ref.1, bf16[512,2048]{1,0:T(8,128)(2,1)} %residual_ref.1, f32[1,2048]{1,0:T(1,128)S(1)} %bitcast.22, ...), custom_call_target="tpu_custom_call" | custom-call | flops 3758096384 | bytes 16777216 | tf_op jit(solution)/shard_map/project/pallas_call | solution.py:230
  160.9 1.2 slice.19
  162.1 1.3 collective-permute-start.4
  163.4 0.2 collective-permute-start.29
  163.7 2.4 collective-permute-start.32
  166.2 0.1 collective-permute-start.34
  166.3 1.4 slice.18
  167.7 14.4 %collective-permute-done.4.refs_1_ = bf16[192,2048]{1,0:T(8,128)(2,1)S(1)} collective-permute-done((bf16[192,2048]{1,0:T(8,128)(2,1)S(1)}, bf16[192,2048]{1,0:T(8,128)(2,1)S(1)}, u32[]{:S(2)}, u32[]{:S(2)}) %collective-permute-start.4) | collective-permute-done | bytes 786464 | tf_op jit(solution)/shard_map/ppermute | solution.py:559
  182.1 1.2 collective-permute-start.3
  183.4 0.5 collective-permute-start.27
  183.9 0.9 copy-done.17
  184.8 0.2 collective-permute-start.33
  185.0 1.6 collective-permute-done.34.refs_33_.refs_34_
  186.5 0.6 concatenate.13.refs_2_
  187.2 0.6 compare_convert_fusion.refs_0_
  187.8 0.6 slice.22.refs_2_
  188.4 0.7 slice.23.refs_2_
  189.1 0.3 collective-permute-done.35.refs_34_.refs_35_
  189.4 11.3 %shard_map.190 = bf16[192,2048]{1,0:T(8,128)(2,1)} custom-call(s32[16]{0:T(128)} %compare_convert_fusion.refs_0_, bf16[192,2048]{1,0:T(8,128)(2,1)} %copy-done.18, f32[8,192]{1,0:T(8,128)} %slice.22.refs_2_, bf16[1536,256]{1,0:T(8,128)(2,1)} %get-tuple-element.22.refs_3_.refs_4_, bf16[1536,256]{1,0:T(8,128)(2,1)} %copy-done.6, ...), custom_call_target="tpu_custom_call" | custom-call | flops 4831838208 | bytes 25165824 | tf_op jit(solution)/shard_map/pallas_call | solution.py:330
  200.7 1.1 collective-permute-start.36
  201.7 12.1 %collective-permute-done.3.refs_1_ = bf16[320,2048]{1,0:T(8,128)(2,1)} collective-permute-done((bf16[320,2048]{1,0:T(8,128)(2,1)S(1)}, bf16[320,2048]{1,0:T(8,128)(2,1)}, u32[]{:S(2)}, u32[]{:S(2)}) %collective-permute-start.3) | collective-permute-done | bytes 1310752 | tf_op jit(solution)/shard_map/ppermute | solution.py:560
  213.9 14.2 %shard_map.191 = (bf16[128,2048]{1,0:T(8,128)(2,1)}, bf16[192,2048]{1,0:T(8,128)(2,1)}) custom-call(s32[16]{0:T(128)} %compare_convert_fusion.refs_0_, bf16[320,2048]{1,0:T(8,128)(2,1)} %collective-permute-done.3.refs_1_, f32[8,320]{1,0:T(8,128)} %slice.23.refs_2_, bf16[1536,256]{1,0:T(8,128)(2,1)} %get-tuple-element.22.refs_3_.refs_4_, ...), custom_call_target="tpu_custom_call" | custom-call | flops 8053063680 | bytes 25165824 | tf_op jit(solution)/shard_map/pallas_call | solution.py:330
  228.1 1.3 collective-permute-start.37
  229.4 0.8 collective-permute-start.38
  230.2 21.2 %shard_map.192.refs_1_.refs_2_ = f32[512,2048]{1,0:T(8,128)} custom-call(s32[16]{0:T(128)} %compare_convert_fusion.refs_0_, bf16[512,2048]{1,0:T(8,128)(2,1)} %get-tuple-element.26.refs_1_, f32[8,512]{1,0:T(8,128)} %concatenate.13.refs_2_, f32[512,2048]{1,0:T(8,128)} %get-tuple-element.27.refs_3_, bf16[1536,256]{1,0:T(8,128)(2,1)} %get-tuple-element.22.refs_3_.refs_4_, ...), custom_call_target="tpu_custom_call" | custom-call | flops 12884901888 | bytes 25165824 | tf_op jit(solution)/shard_map/pallas_call | solution.py:330
  251.4 0.9 copy-done.20
  252.3 3.7 %shard_map.193.refs_0_ = bf16[512,2048]{1,0:T(8,128)(2,1)} custom-call(bf16[512,2048]{1,0:T(8,128)(2,1)} %get-tuple-element.20.refs_0_.refs_1_, f32[512,2048]{1,0:T(8,128)} %shard_map.192.refs_1_.refs_2_, bf16[192,2048]{1,0:T(8,128)(2,1)} %copy-done.20, f32[1,2048]{1,0:T(1,128)} %bitcast.25), custom_call_target="tpu_custom_call" | custom-call | flops 393216 | bytes 3932160 | tf_op jit(solution)/shard_map/pallas_call | solution.py:384
  256.0 0.9 copy-done.19
  256.9 3.8 %shard_map.194.refs_0_ = bf16[512,2048]{1,0:T(8,128)(2,1)} custom-call(bf16[512,2048]{1,0:T(8,128)(2,1)} %shard_map.193.refs_0_, bf16[512,2048]{1,0:T(8,128)(2,1)} %get-tuple-element.20.refs_0_.refs_1_, f32[512,2048]{1,0:T(8,128)} %shard_map.192.refs_1_.refs_2_, bf16[192,2048]{1,0:T(8,128)(2,1)} %copy-done.19, ...), custom_call_target="tpu_custom_call", output_to_operand_aliasing={{}: (0, {})} | custom-call | flops 393216 | bytes 3932160 | tf_op jit(solution)/shard_map/pallas_call | solution.py:384
  260.7 0.8 copy-done.21
  261.6 2.4 shard_map.195
  (91 shorter events, 0.6 us)
Async XLA Ops:
  2.8 29.8 %copy-start.22 = (f32[512,2]{0,1:T(2,128)S(1)}, f32[512,2]{0,1:T(2,128)}, u32[]{:S(2)}) copy-start(f32[512,2]{0,1:T(2,128)} %param.32) | copy-start | bytes 12292
  2.8 29.8 %copy-start.23 = (s32[512,2]{0,1:T(2,128)S(1)}, s32[512,2]{0,1:T(2,128)}, u32[]{:S(2)}) copy-start(s32[512,2]{0,1:T(2,128)} %param.31) | copy-start | bytes 12292
  2.8 38.2 %copy-start.5 = (bf16[1536,256]{1,0:T(8,128)(2,1)S(1)}, bf16[1536,256]{1,0:T(8,128)(2,1)}, u32[]{:S(2)}) copy-start(bf16[1536,256]{1,0:T(8,128)(2,1)} %get-tuple-element.23.refs_5_.refs_6_) | copy-start | bytes 2359300
  2.8 42.4 %copy-start.24 = (f32[64]{0:T(128)S(1)}, f32[64]{0:T(128)}, u32[]{:S(2)}) copy-start(f32[64]{0:T(128)} %param.27) | copy-start | bytes 772
  2.8 41.0 %collective-permute-start.12 = (bf16[1536,256]{1,0:T(8,128)(2,1)}, bf16[1536,256]{1,0:T(8,128)(2,1)}, u32[]{:S(2)}, u32[]{:S(2)}) collective-permute-start(bf16[1536,256]{1,0:T(8,128)(2,1)} %get-tuple-element.22.refs_3_.refs_4_), channel_id=1, source_target_pairs={{0,8},{1,9},{2,0},{3,1},{4,2},{5,3},{6,4},{7,5},{14,6},{15,7},{12,... | collective-permute-start | bytes 2359304 | tf_op jit(solution)/shard_map/ppermute | solution.py:480
  2.9 40.9 %collective-permute-start.8 = (bf16[1536,256]{1,0:T(8,128)(2,1)}, bf16[1536,256]{1,0:T(8,128)(2,1)}, u32[]{:S(2)}, u32[]{:S(2)}) collective-permute-start(bf16[1536,256]{1,0:T(8,128)(2,1)} %get-tuple-element.22.refs_3_.refs_4_), channel_id=1, source_target_pairs={{0,2},{1,3},{2,4},{3,5},{4,6},{5,7},{6,14},{7,15},{14,12},{15,13},... | collective-permute-start | bytes 2359304 | tf_op jit(solution)/shard_map/ppermute | solution.py:480
  4.9 39.4 %collective-permute-start.6 = (bf16[1536,256]{1,0:T(8,128)(2,1)}, bf16[1536,256]{1,0:T(8,128)(2,1)S(1)}, u32[]{:S(2)}, u32[]{:S(2)}) collective-permute-start(bf16[1536,256]{1,0:T(8,128)(2,1)} %get-tuple-element.22.refs_3_.refs_4_), channel_id=1, source_target_pairs={{0,1},{1,0},{2,3},{3,2},{4,5},{5,4},{6,7},{7,6},{8,9},{9,8},{10,11... | collective-permute-start | bytes 2359304 | tf_op jit(solution)/shard_map/ppermute | solution.py:567
  30.1 7.6 %collective-permute-start.2 = (f32[136,128]{1,0:T(8,128)}, f32[136,128]{1,0:T(8,128)S(1)}, u32[]{:S(2)}, u32[]{:S(2)}) collective-permute-start(f32[136,128]{1,0:T(8,128)} %get-tuple-element.19), channel_id=1, source_target_pairs={{0,24},{8,16},{16,8},{24,0},{1,25},{9,17},{17,9},{25,1},{2,26},{10... | collective-permute-start | bytes 208904 | tf_op jit(solution)/shard_map/ppermute | solution.py:513
  32.6 3.8 %collective-permute-start.5 = (f32[8,512]{1,0:T(8,128)S(1)}, f32[8,512]{1,0:T(8,128)S(1)}, u32[]{:S(2)}, u32[]{:S(2)}) collective-permute-start(f32[8,512]{1,0:T(8,128)S(1)} %concatenate.12), channel_id=1, source_target_pairs={{0,16},{16,0},{1,17},{17,1},{2,18},{18,2},{3,19},{19,3},{4,20},{20... | collective-permute-start | bytes 49160 | tf_op jit(solution)/shard_map/ppermute | solution.py:505
  36.5 4.5 %collective-permute-start.1 = (f32[136,128]{1,0:T(8,128)}, f32[136,128]{1,0:T(8,128)S(1)}, u32[]{:S(2)}, u32[]{:S(2)}) collective-permute-start(f32[136,128]{1,0:T(8,128)} %get-tuple-element.19), channel_id=1, source_target_pairs={{0,16},{8,24},{16,0},{24,8},{1,17},{9,25},{17,1},{25,9},{2,18},{10... | collective-permute-start | bytes 208904 | tf_op jit(solution)/shard_map/ppermute | solution.py:513
  37.7 4.5 %collective-permute-start = (f32[136,128]{1,0:T(8,128)}, f32[136,128]{1,0:T(8,128)S(1)}, u32[]{:S(2)}, u32[]{:S(2)}) collective-permute-start(f32[136,128]{1,0:T(8,128)} %get-tuple-element.19), channel_id=1, source_target_pairs={{0,8},{8,0},{16,24},{24,16},{1,9},{9,1},{17,25},{25,17},{2,10},{10... | collective-permute-start | bytes 208904 | tf_op jit(solution)/shard_map/ppermute | solution.py:513
  41.0 20.5 %collective-permute-start.14 = (bf16[1536,256]{1,0:T(8,128)(2,1)S(1)}, bf16[1536,256]{1,0:T(8,128)(2,1)}, u32[]{:S(2)}, u32[]{:S(2)}) collective-permute-start(bf16[1536,256]{1,0:T(8,128)(2,1)S(1)} %copy-done.5), channel_id=1, source_target_pairs={{0,8},{1,9},{2,0},{3,1},{4,2},{5,3},{6,4},{7,5},{14,6},{15,7},{12,... | collective-permute-start | bytes 2359304 | tf_op jit(solution)/shard_map/ppermute | solution.py:480
  42.2 20.9 %collective-permute-start.10 = (bf16[1536,256]{1,0:T(8,128)(2,1)S(1)}, bf16[1536,256]{1,0:T(8,128)(2,1)}, u32[]{:S(2)}, u32[]{:S(2)}) collective-permute-start(bf16[1536,256]{1,0:T(8,128)(2,1)S(1)} %copy-done.5), channel_id=1, source_target_pairs={{0,2},{1,3},{2,4},{3,5},{4,6},{5,7},{6,14},{7,15},{14,12},{15,13},... | collective-permute-start | bytes 2359304 | tf_op jit(solution)/shard_map/ppermute | solution.py:480
  43.8 19.3 %collective-permute-start.7 = (bf16[1536,256]{1,0:T(8,128)(2,1)S(1)}, bf16[1536,256]{1,0:T(8,128)(2,1)S(1)}, u32[]{:S(2)}, u32[]{:S(2)}) collective-permute-start(bf16[1536,256]{1,0:T(8,128)(2,1)S(1)} %copy-done.5), channel_id=1, source_target_pairs={{0,1},{1,0},{2,3},{3,2},{4,5},{5,4},{6,7},{7,6},{8,9},{9,8},{10,11... | collective-permute-start | bytes 2359304 | tf_op jit(solution)/shard_map/ppermute | solution.py:567
  43.8 34.4 %collective-permute-start.20 = (bf16[1536,256]{1,0:T(8,128)(2,1)}, bf16[1536,256]{1,0:T(8,128)(2,1)S(1)}, u32[]{:S(2)}, u32[]{:S(2)}) collective-permute-start(bf16[1536,256]{1,0:T(8,128)(2,1)} %collective-permute-done.12.refs_11_.refs_12_), channel_id=1, source_target_pairs={{0,8},{1,9},{2,0},{3,1},{4,2},{5,3},{6,4},{7,5},{14,6},{15,7},{12,... | collective-permute-start | bytes 2359304 | tf_op jit(solution)/shard_map/ppermute | solution.py:480
  44.3 35.6 %copy-start.6 = (bf16[1536,256]{1,0:T(8,128)(2,1)}, bf16[1536,256]{1,0:T(8,128)(2,1)S(1)}, u32[]{:S(2)}) copy-start(bf16[1536,256]{1,0:T(8,128)(2,1)S(1)} %collective-permute-done.6.refs_4_.refs_5_) | copy-start | bytes 2359300
  44.3 47.5 %collective-permute-start.13 = (bf16[1536,256]{1,0:T(8,128)(2,1)}, bf16[1536,256]{1,0:T(8,128)(2,1)}, u32[]{:S(2)}, u32[]{:S(2)}) collective-permute-start(bf16[1536,256]{1,0:T(8,128)(2,1)} %collective-permute-done.12.refs_11_.refs_12_), channel_id=1, source_target_pairs={{0,1},{1,0},{2,3},{3,2},{4,5},{5,4},{6,7},{7,6},{8,9},{9,8},{10,11... | collective-permute-start | bytes 2359304 | tf_op jit(solution)/shard_map/ppermute | solution.py:567
  61.5 31.8 %collective-permute-start.16 = (bf16[1536,256]{1,0:T(8,128)(2,1)}, bf16[1536,256]{1,0:T(8,128)(2,1)}, u32[]{:S(2)}, u32[]{:S(2)}) collective-permute-start(bf16[1536,256]{1,0:T(8,128)(2,1)} %collective-permute-done.8.refs_7_.refs_8_), channel_id=1, source_target_pairs={{0,2},{1,3},{2,4},{3,5},{4,6},{5,7},{6,14},{7,15},{14,12},{15,13},... | collective-permute-start | bytes 2359304 | tf_op jit(solution)/shard_map/ppermute | solution.py:480
  63.1 30.2 %collective-permute-start.9 = (bf16[1536,256]{1,0:T(8,128)(2,1)}, bf16[1536,256]{1,0:T(8,128)(2,1)}, u32[]{:S(2)}, u32[]{:S(2)}) collective-permute-start(bf16[1536,256]{1,0:T(8,128)(2,1)} %collective-permute-done.8.refs_7_.refs_8_), channel_id=1, source_target_pairs={{0,1},{1,0},{2,3},{3,2},{4,5},{5,4},{6,7},{7,6},{8,9},{9,8},{10,11... | collective-permute-start | bytes 2359304 | tf_op jit(solution)/shard_map/ppermute | solution.py:567
  63.1 16.8 %copy-start.7 = (bf16[1536,256]{1,0:T(8,128)(2,1)}, bf16[1536,256]{1,0:T(8,128)(2,1)S(1)}, u32[]{:S(2)}) copy-start(bf16[1536,256]{1,0:T(8,128)(2,1)S(1)} %collective-permute-done.7.refs_6_.refs_7_) | copy-start | bytes 2359300
  63.1 30.8 %collective-permute-start.22 = (bf16[1536,256]{1,0:T(8,128)(2,1)}, bf16[1536,256]{1,0:T(8,128)(2,1)}, u32[]{:S(2)}, u32[]{:S(2)}) collective-permute-start(bf16[1536,256]{1,0:T(8,128)(2,1)} %collective-permute-done.14.refs_13_.refs_14_), channel_id=1, source_target_pairs={{0,8},{1,9},{2,0},{3,1},{4,2},{5,3},{6,4},{7,5},{14,6},{15,7},{12,... | collective-permute-start | bytes 2359304 | tf_op jit(solution)/shard_map/ppermute | solution.py:480
  78.2 8.0 %copy-start.8 = (bf16[1536,256]{1,0:T(8,128)(2,1)}, bf16[1536,256]{1,0:T(8,128)(2,1)S(1)}, u32[]{:S(2)}) copy-start(bf16[1536,256]{1,0:T(8,128)(2,1)S(1)} %collective-permute-done.20.refs_19_.refs_20_) | copy-start | bytes 2359300
  78.2 15.8 %collective-permute-start.15 = (bf16[1536,256]{1,0:T(8,128)(2,1)}, bf16[1536,256]{1,0:T(8,128)(2,1)}, u32[]{:S(2)}, u32[]{:S(2)}) collective-permute-start(bf16[1536,256]{1,0:T(8,128)(2,1)} %collective-permute-done.14.refs_13_.refs_14_), channel_id=1, source_target_pairs={{0,1},{1,0},{2,3},{3,2},{4,5},{5,4},{6,7},{7,6},{8,9},{9,8},{10,11... | collective-permute-start | bytes 2359304 | tf_op jit(solution)/shard_map/ppermute | solution.py:567
  79.9 69.7 %copy-start.3 = (f32[2048]{0:T(1024)S(1)}, f32[2048]{0:T(1024)}, u32[]{:S(2)}) copy-start(f32[2048]{0:T(1024)} %param.29) | copy-start | bytes 24580
  79.9 69.7 %copy-start.4 = (f32[2048]{0:T(1024)S(1)}, f32[2048]{0:T(1024)}, u32[]{:S(2)}) copy-start(f32[2048]{0:T(1024)} %param.30) | copy-start | bytes 24580
  86.2 63.4 %copy-start = (bf16[2048,256]{1,0:T(8,128)(2,1)S(1)}, bf16[2048,256]{1,0:T(8,128)(2,1)}, u32[]{:S(2)}) copy-start(bf16[2048,256]{1,0:T(8,128)(2,1)} %gate_ref.2) | copy-start | bytes 3145732
  86.2 63.4 %copy-start.1 = (bf16[2048,256]{1,0:T(8,128)(2,1)S(1)}, bf16[2048,256]{1,0:T(8,128)(2,1)}, u32[]{:S(2)}) copy-start(bf16[2048,256]{1,0:T(8,128)(2,1)} %up_ref.2) | copy-start | bytes 3145732
  86.3 63.4 %all-to-all-start = ((bf16[8,512,128]{2,1,0:T(8,128)(2,1)}), bf16[8,512,128]{2,1,0:T(8,128)(2,1)S(1)}, u32[]{:S(2)}, u32[]{:S(2)}) async-start(bf16[8,512,128]{2,1,0:T(8,128)(2,1)} %bitcast.24), calls=%async_computation | async-start | bytes 2097152 | tf_op jit(solution)/shard_map/all_to_all | solution.py:525
  91.8 40.1 %collective-permute-start.18 = (bf16[1536,256]{1,0:T(8,128)(2,1)}, bf16[1536,256]{1,0:T(8,128)(2,1)}, u32[]{:S(2)}, u32[]{:S(2)}) collective-permute-start(bf16[1536,256]{1,0:T(8,128)(2,1)} %collective-permute-done.10.refs_9_.refs_10_), channel_id=1, source_target_pairs={{0,2},{1,3},{2,4},{3,5},{4,6},{5,7},{6,14},{7,15},{14,12},{15,13},... | collective-permute-start | bytes 2359304 | tf_op jit(solution)/shard_map/ppermute | solution.py:480
  93.3 38.6 %collective-permute-start.11 = (bf16[1536,256]{1,0:T(8,128)(2,1)}, bf16[1536,256]{1,0:T(8,128)(2,1)S(1)}, u32[]{:S(2)}, u32[]{:S(2)}) collective-permute-start(bf16[1536,256]{1,0:T(8,128)(2,1)} %collective-permute-done.10.refs_9_.refs_10_), channel_id=1, source_target_pairs={{0,1},{1,0},{2,3},{3,2},{4,5},{5,4},{6,7},{7,6},{8,9},{9,8},{10,11... | collective-permute-start | bytes 2359304 | tf_op jit(solution)/shard_map/ppermute | solution.py:567
  93.3 40.5 %collective-permute-start.28 = (bf16[1536,256]{1,0:T(8,128)(2,1)}, bf16[1536,256]{1,0:T(8,128)(2,1)S(1)}, u32[]{:S(2)}, u32[]{:S(2)}) collective-permute-start(bf16[1536,256]{1,0:T(8,128)(2,1)} %copy-done.8), channel_id=1, source_target_pairs={{0,8},{1,9},{2,0},{3,1},{4,2},{5,3},{6,4},{7,5},{14,6},{15,7},{12,... | collective-permute-start | bytes 2359304 | tf_op jit(solution)/shard_map/ppermute | solution.py:480
  93.9 39.9 %collective-permute-start.21 = (bf16[1536,256]{1,0:T(8,128)(2,1)}, bf16[1536,256]{1,0:T(8,128)(2,1)S(1)}, u32[]{:S(2)}, u32[]{:S(2)}) collective-permute-start(bf16[1536,256]{1,0:T(8,128)(2,1)} %copy-done.8), channel_id=1, source_target_pairs={{0,1},{1,0},{2,3},{3,2},{4,5},{5,4},{6,7},{7,6},{8,9},{9,8},{10,11... | collective-permute-start | bytes 2359304 | tf_op jit(solution)/shard_map/ppermute | solution.py:567
  94.1 54.6 %collective-permute-start.24 = (bf16[1536,256]{1,0:T(8,128)(2,1)}, bf16[1536,256]{1,0:T(8,128)(2,1)S(1)}, u32[]{:S(2)}, u32[]{:S(2)}) collective-permute-start(bf16[1536,256]{1,0:T(8,128)(2,1)} %collective-permute-done.16.refs_15_.refs_16_), channel_id=1, source_target_pairs={{0,2},{1,3},{2,4},{3,5},{4,6},{5,7},{6,14},{7,15},{14,12},{15,13},... | collective-permute-start | bytes 2359304 | tf_op jit(solution)/shard_map/ppermute | solution.py:480
  131.9 30.3 %collective-permute-start.17 = (bf16[1536,256]{1,0:T(8,128)(2,1)}, bf16[1536,256]{1,0:T(8,128)(2,1)}, u32[]{:S(2)}, u32[]{:S(2)}) collective-permute-start(bf16[1536,256]{1,0:T(8,128)(2,1)} %collective-permute-done.16.refs_15_.refs_16_), channel_id=1, source_target_pairs={{0,1},{1,0},{2,3},{3,2},{4,5},{5,4},{6,7},{7,6},{8,9},{9,8},{10,11... | collective-permute-start | bytes 2359304 | tf_op jit(solution)/shard_map/ppermute | solution.py:567
  131.9 16.8 %copy-start.9 = (bf16[1536,256]{1,0:T(8,128)(2,1)}, bf16[1536,256]{1,0:T(8,128)(2,1)S(1)}, u32[]{:S(2)}) copy-start(bf16[1536,256]{1,0:T(8,128)(2,1)S(1)} %collective-permute-done.11.refs_10_.refs_11_) | copy-start | bytes 2359300
  131.9 31.6 %collective-permute-start.30 = (bf16[1536,256]{1,0:T(8,128)(2,1)}, bf16[1536,256]{1,0:T(8,128)(2,1)}, u32[]{:S(2)}, u32[]{:S(2)}) collective-permute-start(bf16[1536,256]{1,0:T(8,128)(2,1)} %collective-permute-done.22.refs_21_.refs_22_), channel_id=1, source_target_pairs={{0,8},{1,9},{2,0},{3,1},{4,2},{5,3},{6,4},{7,5},{14,6},{15,7},{12,... | collective-permute-start | bytes 2359304 | tf_op jit(solution)/shard_map/ppermute | solution.py:480
  133.8 14.9 %copy-start.10 = (bf16[1536,256]{1,0:T(8,128)(2,1)}, bf16[1536,256]{1,0:T(8,128)(2,1)S(1)}, u32[]{:S(2)}) copy-start(bf16[1536,256]{1,0:T(8,128)(2,1)S(1)} %collective-permute-done.28.refs_27_.refs_28_) | copy-start | bytes 2359300
  133.8 29.9 %collective-permute-start.23 = (bf16[1536,256]{1,0:T(8,128)(2,1)}, bf16[1536,256]{1,0:T(8,128)(2,1)}, u32[]{:S(2)}, u32[]{:S(2)}) collective-permute-start(bf16[1536,256]{1,0:T(8,128)(2,1)} %collective-permute-done.22.refs_21_.refs_22_), channel_id=1, source_target_pairs={{0,1},{1,0},{2,3},{3,2},{4,5},{5,4},{6,7},{7,6},{8,9},{9,8},{10,11... | collective-permute-start | bytes 2359304 | tf_op jit(solution)/shard_map/ppermute | solution.py:567
  133.8 14.9 %copy-start.12 = (bf16[1536,256]{1,0:T(8,128)(2,1)}, bf16[1536,256]{1,0:T(8,128)(2,1)S(1)}, u32[]{:S(2)}) copy-start(bf16[1536,256]{1,0:T(8,128)(2,1)S(1)} %collective-permute-done.21.refs_20_.refs_21_) | copy-start | bytes 2359300
  133.8 32.2 %collective-permute-start.26 = (bf16[1536,256]{1,0:T(8,128)(2,1)}, bf16[1536,256]{1,0:T(8,128)(2,1)}, u32[]{:S(2)}, u32[]{:S(2)}) collective-permute-start(bf16[1536,256]{1,0:T(8,128)(2,1)} %collective-permute-done.18.refs_17_.refs_18_), channel_id=1, source_target_pairs={{0,2},{1,3},{2,4},{3,5},{4,6},{5,7},{6,14},{7,15},{14,12},{15,13},... | collective-permute-start | bytes 2359304 | tf_op jit(solution)/shard_map/ppermute | solution.py:480
  148.7 0.9 copy-start.13
  149.6 16.6 %collective-permute-start.19 = (bf16[1536,256]{1,0:T(8,128)(2,1)}, bf16[1536,256]{1,0:T(8,128)(2,1)}, u32[]{:S(2)}, u32[]{:S(2)}) collective-permute-start(bf16[1536,256]{1,0:T(8,128)(2,1)} %collective-permute-done.18.refs_17_.refs_18_), channel_id=1, source_target_pairs={{0,1},{1,0},{2,3},{3,2},{4,5},{5,4},{6,7},{7,6},{8,9},{9,8},{10,11... | collective-permute-start | bytes 2359304 | tf_op jit(solution)/shard_map/ppermute | solution.py:567
  149.7 1.2 copy-start.2
  150.9 12.6 %copy-start.11 = (bf16[1536,256]{1,0:T(8,128)(2,1)S(1)}, bf16[1536,256]{1,0:T(8,128)(2,1)}, u32[]{:S(2)}) copy-start(bf16[1536,256]{1,0:T(8,128)(2,1)} %copy-done.10) | copy-start | bytes 2359300
  150.9 12.8 %copy-start.14 = (bf16[1536,256]{1,0:T(8,128)(2,1)S(1)}, bf16[1536,256]{1,0:T(8,128)(2,1)}, u32[]{:S(2)}) copy-start(bf16[1536,256]{1,0:T(8,128)(2,1)} %copy-done.13) | copy-start | bytes 2359300
  162.1 20.0 %collective-permute-start.4 = (bf16[192,2048]{1,0:T(8,128)(2,1)S(1)}, bf16[192,2048]{1,0:T(8,128)(2,1)S(1)}, u32[]{:S(2)}, u32[]{:S(2)}) collective-permute-start(bf16[192,2048]{1,0:T(8,128)(2,1)S(1)} %slice.19), channel_id=1, source_target_pairs={{0,16},{16,0},{1,17},{17,1},{2,18},{18,2},{3,19},{19,3},{4,20},{20... | collective-permute-start | bytes 2359304 | tf_op jit(solution)/shard_map/ppermute | solution.py:559
  163.4 19.9 %collective-permute-start.29 = (bf16[1536,256]{1,0:T(8,128)(2,1)S(1)}, bf16[1536,256]{1,0:T(8,128)(2,1)S(1)}, u32[]{:S(2)}, u32[]{:S(2)}) collective-permute-start(bf16[1536,256]{1,0:T(8,128)(2,1)S(1)} %copy-done.11), channel_id=1, source_target_pairs={{0,1},{1,0},{2,3},{3,2},{4,5},{5,4},{6,7},{7,6},{8,9},{9,8},{10,11... | collective-permute-start | bytes 2359304 | tf_op jit(solution)/shard_map/ppermute | solution.py:567
  163.7 19.7 %collective-permute-start.32 = (bf16[1536,256]{1,0:T(8,128)(2,1)S(1)}, bf16[1536,256]{1,0:T(8,128)(2,1)S(1)}, u32[]{:S(2)}, u32[]{:S(2)}) collective-permute-start(bf16[1536,256]{1,0:T(8,128)(2,1)S(1)} %copy-done.14), channel_id=1, source_target_pairs={{0,2},{1,3},{2,4},{3,5},{4,6},{5,7},{6,14},{7,15},{14,12},{15,13},... | collective-permute-start | bytes 2359304 | tf_op jit(solution)/shard_map/ppermute | solution.py:480
  166.0 17.9 %collective-permute-start.25 = (bf16[1536,256]{1,0:T(8,128)(2,1)S(1)}, bf16[1536,256]{1,0:T(8,128)(2,1)S(1)}, u32[]{:S(2)}, u32[]{:S(2)}) collective-permute-start(bf16[1536,256]{1,0:T(8,128)(2,1)S(1)} %copy-done.14), channel_id=1, source_target_pairs={{0,1},{1,0},{2,3},{3,2},{4,5},{5,4},{6,7},{7,6},{8,9},{9,8},{10,11... | collective-permute-start | bytes 2359304 | tf_op jit(solution)/shard_map/ppermute | solution.py:567
  166.2 20.4 %collective-permute-start.34 = (bf16[1536,256]{1,0:T(8,128)(2,1)}, bf16[1536,256]{1,0:T(8,128)(2,1)}, u32[]{:S(2)}, u32[]{:S(2)}) collective-permute-start(bf16[1536,256]{1,0:T(8,128)(2,1)} %collective-permute-done.30.refs_29_.refs_30_), channel_id=1, source_target_pairs={{0,8},{1,9},{2,0},{3,1},{4,2},{5,3},{6,4},{7,5},{14,6},{15,7},{12,... | collective-permute-start | bytes 2359304 | tf_op jit(solution)/shard_map/ppermute | solution.py:480
  182.1 2.8 %copy-start.18 = (bf16[192,2048]{1,0:T(8,128)(2,1)}, bf16[192,2048]{1,0:T(8,128)(2,1)S(1)}, u32[]{:S(2)}) copy-start(bf16[192,2048]{1,0:T(8,128)(2,1)S(1)} %collective-permute-done.4.refs_1_) | copy-start | bytes 2359300
  182.1 31.8 %collective-permute-start.3 = (bf16[320,2048]{1,0:T(8,128)(2,1)S(1)}, bf16[320,2048]{1,0:T(8,128)(2,1)}, u32[]{:S(2)}, u32[]{:S(2)}) collective-permute-start(bf16[320,2048]{1,0:T(8,128)(2,1)S(1)} %slice.18), channel_id=1, source_target_pairs={{0,16},{16,0},{1,17},{17,1},{2,18},{18,2},{3,19},{19,3},{4,20},{20... | collective-permute-start | bytes 3932168 | tf_op jit(solution)/shard_map/ppermute | solution.py:560
  183.4 6.0 %copy-start.15 = (bf16[1536,256]{1,0:T(8,128)(2,1)}, bf16[1536,256]{1,0:T(8,128)(2,1)S(1)}, u32[]{:S(2)}) copy-start(bf16[1536,256]{1,0:T(8,128)(2,1)S(1)} %collective-permute-done.29.refs_28_.refs_29_) | copy-start | bytes 2359300
  183.4 5.7 %collective-permute-start.31 = (bf16[1536,256]{1,0:T(8,128)(2,1)}, bf16[1536,256]{1,0:T(8,128)(2,1)}, u32[]{:S(2)}, u32[]{:S(2)}) collective-permute-start(bf16[1536,256]{1,0:T(8,128)(2,1)} %collective-permute-done.30.refs_29_.refs_30_), channel_id=1, source_target_pairs={{0,1},{1,0},{2,3},{3,2},{4,5},{5,4},{6,7},{7,6},{8,9},{9,8},{10,11... | collective-permute-start | bytes 2359304 | tf_op jit(solution)/shard_map/ppermute | solution.py:567
  183.4 6.0 %copy-start.16 = (bf16[1536,256]{1,0:T(8,128)(2,1)}, bf16[1536,256]{1,0:T(8,128)(2,1)S(1)}, u32[]{:S(2)}) copy-start(bf16[1536,256]{1,0:T(8,128)(2,1)S(1)} %collective-permute-done.32.refs_31_.refs_32_) | copy-start | bytes 2359300
  183.4 5.7 %collective-permute-start.27 = (bf16[1536,256]{1,0:T(8,128)(2,1)}, bf16[1536,256]{1,0:T(8,128)(2,1)}, u32[]{:S(2)}, u32[]{:S(2)}) collective-permute-start(bf16[1536,256]{1,0:T(8,128)(2,1)} %collective-permute-done.26.refs_25_.refs_26_), channel_id=1, source_target_pairs={{0,1},{1,0},{2,3},{3,2},{4,5},{5,4},{6,7},{7,6},{8,9},{9,8},{10,11... | collective-permute-start | bytes 2359304 | tf_op jit(solution)/shard_map/ppermute | solution.py:567
  183.9 0.9 copy-start.17
  184.8 4.3 %collective-permute-start.33 = (bf16[1536,256]{1,0:T(8,128)(2,1)S(1)}, bf16[1536,256]{1,0:T(8,128)(2,1)}, u32[]{:S(2)}, u32[]{:S(2)}) collective-permute-start(bf16[1536,256]{1,0:T(8,128)(2,1)S(1)} %collective-permute-done.32.refs_31_.refs_32_), channel_id=1, source_target_pairs={{0,1},{1,0},{2,3},{3,2},{4,5},{5,4},{6,7},{7,6},{8,9},{9,8},{10,11... | collective-permute-start | bytes 2359304 | tf_op jit(solution)/shard_map/ppermute | solution.py:567
  186.5 2.9 %collective-permute-start.35 = (bf16[1536,256]{1,0:T(8,128)(2,1)}, bf16[1536,256]{1,0:T(8,128)(2,1)}, u32[]{:S(2)}, u32[]{:S(2)}) collective-permute-start(bf16[1536,256]{1,0:T(8,128)(2,1)} %collective-permute-done.34.refs_33_.refs_34_), channel_id=1, source_target_pairs={{0,1},{1,0},{2,3},{3,2},{4,5},{5,4},{6,7},{7,6},{8,9},{9,8},{10,11... | collective-permute-start | bytes 2359304 | tf_op jit(solution)/shard_map/ppermute | solution.py:567
  200.7 50.7 %collective-permute-start.36 = (bf16[192,2048]{1,0:T(8,128)(2,1)}, bf16[192,2048]{1,0:T(8,128)(2,1)S(1)}, u32[]{:S(2)}, u32[]{:S(2)}) collective-permute-start(bf16[192,2048]{1,0:T(8,128)(2,1)} %shard_map.190), channel_id=1, source_target_pairs={{0,16},{16,0},{1,17},{17,1},{2,18},{18,2},{3,19},{19,3},{4,20},{20... | collective-permute-start | bytes 2359304 | tf_op jit(solution)/shard_map/ppermute | solution.py:581
  228.1 27.9 %collective-permute-start.37 = (bf16[192,2048]{1,0:T(8,128)(2,1)}, bf16[192,2048]{1,0:T(8,128)(2,1)S(1)}, u32[]{:S(2)}, u32[]{:S(2)}) collective-permute-start(bf16[192,2048]{1,0:T(8,128)(2,1)} %get-tuple-element.25), channel_id=1, source_target_pairs={{0,16},{16,0},{1,17},{17,1},{2,18},{18,2},{3,19},{19,3},{4,20},{20... | collective-permute-start | bytes 2359304 | tf_op jit(solution)/shard_map/ppermute | solution.py:585
  229.4 31.3 %collective-permute-start.38 = (bf16[128,2048]{1,0:T(8,128)(2,1)}, bf16[128,2048]{1,0:T(8,128)(2,1)S(1)}, u32[]{:S(2)}, u32[]{:S(2)}) collective-permute-start(bf16[128,2048]{1,0:T(8,128)(2,1)} %get-tuple-element.28), channel_id=1, source_target_pairs={{0,16},{16,0},{1,17},{17,1},{2,18},{18,2},{3,19},{19,3},{4,20},{20... | collective-permute-start | bytes 1572872 | tf_op jit(solution)/shard_map/ppermute | solution.py:585
  251.4 0.9 copy-start.20
  256.0 0.9 copy-start.19
  (1 other events, 0.8 us)

commit v4 on v3

--- a/solution.py
+++ b/solution.py
@@ -272,7 +272,7 @@
     )(gate, up, down)
 
 
-def expert_kernel(*refs, based, sources):
+def expert_kernel(*refs, based, sources, skip):
     which_ref, rows_ref, share_ref = refs[:3]
     piece_refs = refs[3 + based : 3 + based + len(sources)]
     out_refs = refs[3 + based + len(sources) : -4]
@@ -284,7 +284,7 @@
         into = held_ref.at[slot, start : start + ref.shape[0]]
         pltpu.make_async_copy(ref, into, sems.at[slot]).start()
     sum_ref[...] = jnp.zeros_like(sum_ref)
-    share = share_ref[...].T
+    share = share_ref[...].T[skip : skip + rows_ref.shape[0]]
     for e in range(wide_ref.shape[0]):
         wide_ref[e] = jnp.broadcast_to(share[:, e : e + 1], wide_ref.shape[1:])
 
@@ -314,7 +314,7 @@
 TOGETHER = 2
 
 
-def expert_call(which, rows, share, held, base, sizes, kind):
+def expert_call(which, rows, share, held, base, sizes, kind, skip=0):
     count, width = rows.shape
     arrays = [array for array, _, _ in held]
     sources = [(slot, start) for _, slot, start in held]
@@ -328,7 +328,7 @@
         operands.append(base)
     specs += [pl.BlockSpec(memory_space=pltpu.HBM)] * len(arrays)
     return pl.pallas_call(
-        functools.partial(expert_kernel, based=base is not None, sources=sources),
+        functools.partial(expert_kernel, based=base is not None, sources=sources, skip=skip),
         in_specs=specs,
         out_specs=[pl.BlockSpec(memory_space=pltpu.VMEM)] * len(sizes),
         out_shape=[jax.ShapeDtypeStruct((size, width), kind) for size in sizes],
@@ -362,35 +362,53 @@
     return shift(1), shift(-1), swap
 
 
-def combine_kernel(*refs):
-    stream_ref, base_ref, answer_ref, gain_ref, out_ref = refs[-5:]
-    summed = base_ref[...] + answer_ref[...].astype(F32)
+def combine_kernel(*refs, counts, followed):
+    stream_ref, base_ref = refs[followed : followed + 2]
+    answer_refs = refs[followed + 2 : -2]
+    gain_ref, out_ref = refs[-2:]
+    answer = answer_refs[0][...]
+    if len(counts) == 2:
+        answer = jnp.where(pl.program_id(0) < counts[0], answer, answer_refs[1][...])
+    summed = base_ref[...] + answer.astype(F32)
     out_ref[...] = (stream_ref[...].astype(F32) + rms_scale(summed) * gain_ref[...]).astype(BF16)
 
 
-def combine_call(so_far, stream, base, answer, gain, start):
+def combine_call(so_far, stream, base, answers, gain, starts):
     rows, width = stream.shape
-    span = min(answer.shape[0], 64)
-    skip = start // span
-    block = pl.BlockSpec((span, width), lambda i: (skip + i, 0))
-    specs = [block, block, pl.BlockSpec((span, width), lambda i: (i, 0))]
+    span = min(answers[0].shape[0], 64)
+    counts = [answer.shape[0] // span for answer in answers]
+    skips = [start // span for start in starts]
+
+    def place(i):
+        if len(counts) == 1:
+            return skips[0] + i, 0
+        return jnp.where(i < counts[0], skips[0] + i, skips[1] + i - counts[0]), 0
+
+    places = [
+        lambda i: (jnp.minimum(i, counts[0] - 1), 0),
+        lambda i: (jnp.maximum(i - counts[0], 0), 0),
+    ]
+    block = pl.BlockSpec((span, width), place)
+    specs = [block, block] + [pl.BlockSpec((span, width), at) for at in places[: len(counts)]]
     specs.append(pl.BlockSpec((1, width), lambda i: (0, 0)))
-    operands = [stream, base, answer, gain.reshape(1, width)]
+    operands = [stream, base, *answers, gain.reshape(1, width)]
     aliases = {}
     if so_far is not None:
         specs.insert(0, pl.BlockSpec(memory_space=pl.ANY))
         operands.insert(0, so_far)
         aliases = {0: 0}
     return pl.pallas_call(
-        combine_kernel,
-        grid=(answer.shape[0] // span,),
+        functools.partial(combine_kernel, counts=counts, followed=int(so_far is not None)),
+        grid=(sum(counts),),
         in_specs=specs,
         out_specs=block,
         out_shape=jax.ShapeDtypeStruct((rows, width), BF16),
         input_output_aliases=aliases,
         compiler_params=pltpu.CompilerParams(dimension_semantics=("arbitrary",)),
         cost_estimate=pl.CostEstimate(
-            flops=answer.size, bytes_accessed=10 * answer.size, transcendentals=0
+            flops=sum(counts) * span * width,
+            bytes_accessed=10 * sum(counts) * span * width,
+            transcendentals=0,
         ),
     )(*operands)
 
@@ -528,6 +546,27 @@
     if paired:
         hop("long")
         hop("short")
+        held = []
+
+        def hold(slot, start, array):
+            held.append((array, slot, start))
+            held.append((lax.ppermute(array, "tp", partner), slot + 1, start))
+
+        def hold_hop(k):
+            hold(4 * k - 2, 0, long_a[k])
+            hold(4 * k - 2, half, short_a[k])
+            hold(4 * k, 0, short_b[k])
+            hold(4 * k, half, long_b[k])
+
+        half = upper.shape[0]
+        (long_a, long_b), (short_a, short_b) = hops["long"], hops["short"]
+        hold(0, 0, upper)
+        hold(0, half, lower)
+        hold_hop(1)
+        mixed, which, own_share, far_share, early = lax.optimization_barrier(
+            (mixed, which, own_share, far_share, [array for array, _, _ in held])
+        )
+        held = [(array, slot, start) for array, (_, slot, start) in zip(early, held)]
     if channels % 128 == 0:
         stream, normed, shared = project_call(
             mixed,
@@ -560,35 +599,29 @@
     far_rest = lax.ppermute(normed[first:], outer, swap)
     hop("long")
 
-    held = []
-
-    def hold(slot, start, array):
-        held.append((array, slot, start))
-        held.append((lax.ppermute(array, "tp", partner), slot + 1, start))
-
-    half = upper.shape[0]
-    (long_a, long_b), (short_a, short_b) = hops["long"], hops["short"]
-    hold(0, 0, upper)
-    hold(0, half, lower)
-    for k in range(1, 4):
-        hold(4 * k - 2, 0, long_a[k])
-        hold(4 * k - 2, half, short_a[k])
-        hold(4 * k, 0, short_b[k])
-        hold(4 * k, half, long_b[k])
+    hold_hop(2)
+    hold_hop(3)
     hold(14, 0, long_a[4])
     hold(14, half, long_b[4])
-    (partial,) = expert_call(which, far_first, far_share[:, :first], held, None, (first,), BF16)
+    (partial,) = expert_call(which, far_first, far_share, held, None, (first,), BF16)
     answers = [lax.ppermute(partial, outer, swap)]
     far_rest, _ = lax.optimization_barrier((far_rest, partial))
     sizes = (rows - 2 * first, first)
-    partials = expert_call(which, far_rest, far_share[:, first:], held, None, sizes, BF16)
+    partials = expert_call(which, far_rest, far_share, held, None, sizes, BF16, first)
     answers += [lax.ppermute(partial, outer, swap) for partial in partials]
     own_rows, _ = lax.optimization_barrier((normed, partials[1]))
     (base,) = expert_call(which, own_rows, own_share, held, shared, (rows,), F32)
+    starts = (0, first, first + sizes[0])
     layer_out = None
-    starts = (0, first, first + sizes[0])
-    for c in (0, 2, 1):
-        layer_out = combine_call(layer_out, stream, base, answers[c], final_norm_gain, starts[c])
+    for chosen in ((0, 2), (1,)):
+        layer_out = combine_call(
+            layer_out,
+            stream,
+            base,
+            [answers[c] for c in chosen],
+            final_norm_gain,
+            [starts[c] for c in chosen],
+        )
     return layer_out
 
 

time: 267 us -> 265 us (level)
  waiting for transfers between devices: 117 us -> 120 us
    pallas_call x3 -> x2, Pallas kernels: 9.97 us -> 8.43 us  [combine_call(): pl.pallas_call(functools.partial(combine_kernel, counts=counts, followed=...]
    unnamed x50 -> x48, local copies, waits for them, and re-layouts: 5.68 us -> 4.16 us
  transfers between devices with their start and end apart: 40 -> 40, of which waited for: 12 -> 15; matrix products, arithmetic and copies ran while one was open for 3% -> 3% of each run, Pallas kernels for 36% -> 36%
where the time goes in v4:
time: 265 us; the launch traced here: 262 us
  waiting for transfers between devices  120 us (45%)
  Pallas kernels  99.2 us (37%)
  starting transfers between devices  31.8 us (12%)
  local copies, waits for them, and re-layouts  8.17 us (3%)
  other arithmetic  2.87 us (1%)
    ppermute x14, waiting for transfers between devices, hop(): chain.append(lax.ppermute(chain[-1], ring, perm))  84.9 us
    pallas_call x3, Pallas kernels, expert_call(): pl.pallas_call(functools.partial(expert_kernel, based=base is not None, s...  46.7 us
    pallas_call x1, Pallas kernels, scan_call(): pl.pallas_call(scan_kernel, grid=(tokens // span,), in_specs=[block, bloc...  25.2 us
    ppermute x1, waiting for transfers between devices, body(): far_first = lax.ppermute(normed[:first], outer, swap)  14.3 us
    ppermute x14, starting transfers between devices, hop(): chain.append(lax.ppermute(chain[-1], ring, perm))  14 us
    ppermute x1, waiting for transfers between devices, body(): far_rest = lax.ppermute(normed[first:], outer, swap)  12.3 us
    pallas_call x1, Pallas kernels, project_call(): pl.pallas_call(project_kernel, grid=(rows // span,), in_specs=[pl.BlockSp...  9.9 us
    pallas_call x2, Pallas kernels, combine_call(): pl.pallas_call(functools.partial(combine_kernel, counts=counts, followed=...  8.43 us
  transfers between devices with their start and end apart: 40, of which 15 were waited for; matrix products, arithmetic and copies ran while one was open for 3% of the time, Pallas kernels for 36%

profile of v4, /device:TPU:8, one launch (start us, length us, event | category | flops | bytes accessed | tf_op | source)
XLA Modules:
  0.0 262.1 jit_solution(16917746747762650975)
XLA Ops:
  0.0 2.8 %pack.1 = (bf16[1536,256]{1,0:T(8,128)(2,1)}, bf16[1536,256]{1,0:T(8,128)(2,1)}) custom-call(bf16[1,2048,128]{2,1,0:T(8,128)(2,1)} %gate_ref.2, bf16[1,2048,128]{2,1,0:T(8,128)(2,1)} %up_ref.2, bf16[1,2048,128]{2,1,0:T(8,128)(2,1)} %down_ref.2), custom_call_target="tpu_custom_call" | custom-call | bytes 3145728 | tf_op jit(solution)/shard_map/pack/pallas_call | solution.py:267
  2.9 2.0 collective-permute-start.6
  4.9 25.2 %scan.1 = (f32[4096,128]{1,0:T(8,128)}, f32[4096,128]{1,0:T(8,128)}, f32[136,128]{1,0:T(8,128)}) custom-call(bf16[4096,128]{1,0:T(8,128)(2,1)} %q_ref.1, bf16[4096,128]{1,0:T(8,128)(2,1)} %f_ref.1, bf16[4096,128]{1,0:T(8,128)(2,1)} %v_ref.1, f32[1,128]{1,0:T(1,128)} %bitcast.35, f32[2,4096]{1,0:T(2,128)} %sudden_ref.1), custom_call_target="tpu_custom_call" | custom-call | flops 1048576000 | bytes 7340032 | tf_op jit(solution)/shard_map/scan/pallas_call | solution.py:123
  30.0 2.5 collective-permute-start.2
  32.6 0.6 collective-permute-start.3
  33.2 3.2 %collective-permute-done.3.refs_2_ = f32[8,512]{1,0:T(8,128)S(1)} collective-permute-done((f32[8,512]{1,0:T(8,128)S(1)}, f32[8,512]{1,0:T(8,128)S(1)}, u32[]{:S(2)}, u32[]{:S(2)}) %collective-permute-start.3) | collective-permute-done | bytes 16416 | tf_op jit(solution)/shard_map/ppermute | solution.py:523
  36.4 1.2 collective-permute-start.1
  37.7 1.3 collective-permute-start
  39.0 2.0 collective-permute-done.1
  41.0 0.5 collective-permute-start.12
  41.4 0.8 collective-permute-done
  42.2 1.6 collective-permute-start.8
  43.8 0.5 collective-permute-start.20
  44.3 0.2 collective-permute-start.11
  44.5 0.7 pad_add_fusion.mine_ref
  45.2 0.7 reshape_tile.3.gain_ref
  45.9 15.6 %collective-permute-done.12.refs_13_.refs_14_ = bf16[1536,256]{1,0:T(8,128)(2,1)} collective-permute-done((bf16[1536,256]{1,0:T(8,128)(2,1)S(1)}, bf16[1536,256]{1,0:T(8,128)(2,1)}, u32[]{:S(2)}, u32[]{:S(2)}) %collective-permute-start.12) | collective-permute-done | bytes 786464 | tf_op jit(solution)/shard_map/ppermute | solution.py:498
  61.5 1.6 collective-permute-start.16
  63.1 0.5 collective-permute-start.22
  63.6 14.7 %collective-permute-done.20.refs_19_.refs_20_ = bf16[1536,256]{1,0:T(8,128)(2,1)} collective-permute-done((bf16[1536,256]{1,0:T(8,128)(2,1)}, bf16[1536,256]{1,0:T(8,128)(2,1)}, u32[]{:S(2)}, u32[]{:S(2)}) %collective-permute-start.20) | collective-permute-done | bytes 786464 | tf_op jit(solution)/shard_map/ppermute | solution.py:498
  78.3 1.6 pad_maximum_fusion.pieces_ref
  79.9 6.3 %gate.1 = bf16[4096,128]{1,0:T(8,128)(2,1)} custom-call(s32[5]{0:T(128)} %pad_add_fusion.mine_ref, f32[4096,128]{1,0:T(8,128)} %get-tuple-element.33.local_ref, f32[4096,128]{1,0:T(8,128)} %get-tuple-element.34.lifted_ref, bf16[4096,128]{1,0:T(8,128)(2,1)} %open_ref.1, f32[4,136,128]{2,1,0:T(8,128)} %pad_maximum_fusion.pieces_ref, f32[1,128]{1,0:T(1,128)} %reshape_tile.3.gain_ref), custom_call_target="tpu_custom_call" | custom-call | flops 419430400 | bytes 5242880 | tf_op jit(solution)/shard_map/gate/pallas_call | solution.py:174
  86.3 5.6 %all-to-all-start = ((bf16[8,512,128]{2,1,0:T(8,128)(2,1)}), bf16[8,512,128]{2,1,0:T(8,128)(2,1)S(1)}, u32[]{:S(2)}, u32[]{:S(2)}) async-start(bf16[8,512,128]{2,1,0:T(8,128)(2,1)} %bitcast.24), calls=%async_computation | async-start | bytes 2097152 | tf_op jit(solution)/shard_map/all_to_all | solution.py:543
  91.9 1.5 collective-permute-start.18
  93.3 0.6 collective-permute-start.28
  94.0 0.2 collective-permute-start.21
  94.1 1.5 collective-permute-start.24
  95.6 36.3 %collective-permute-done.18.refs_17_.refs_18_ = bf16[1536,256]{1,0:T(8,128)(2,1)} collective-permute-done((bf16[1536,256]{1,0:T(8,128)(2,1)}, bf16[1536,256]{1,0:T(8,128)(2,1)}, u32[]{:S(2)}, u32[]{:S(2)}) %collective-permute-start.18) | collective-permute-done | bytes 786464 | tf_op jit(solution)/shard_map/ppermute | solution.py:498
  132.0 2.0 collective-permute-done.28.refs_27_.refs_28_
  134.0 1.0 collective-permute-start.26
  135.0 13.8 %collective-permute-done.24.refs_23_.refs_24_ = bf16[1536,256]{1,0:T(8,128)(2,1)} collective-permute-done((bf16[1536,256]{1,0:T(8,128)(2,1)}, bf16[1536,256]{1,0:T(8,128)(2,1)}, u32[]{:S(2)}, u32[]{:S(2)}) %collective-permute-start.24) | collective-permute-done | bytes 786464 | tf_op jit(solution)/shard_map/ppermute | solution.py:498
  148.8 0.6 concatenate.12.refs_2_
  149.4 0.1 stack.80
  149.5 0.6 compare_convert_fusion.refs_0_
  150.1 1.2 copy-done.2
  151.3 9.9 %project.1 = (bf16[512,2048]{1,0:T(8,128)(2,1)}, bf16[512,2048]{1,0:T(8,128)(2,1)}, f32[512,2048]{1,0:T(8,128)}) custom-call(bf16[8,512,128]{2,1,0:T(8,128)(2,1)S(1)} %all-to-all-done.mixed_ref, bf16[1024,2048]{1,0:T(8,128)(2,1)} %weight_ref.1, bf16[512,2048]{1,0:T(8,128)(2,1)} %residual_ref.1, f32[1,2048]{1,0:T(1,128)S(1)} %bitcast.22, ...), custom_call_target="tpu_custom_call" | custom-call | flops 3758096384 | bytes 16777216 | tf_op jit(solution)/shard_map/project/pallas_call | solution.py:230
  161.2 1.2 slice.13
  162.4 1.3 collective-permute-start.15
  163.7 0.2 collective-permute-start.29
  164.0 2.5 collective-permute-start.32
  166.5 0.2 collective-permute-start.34
  166.7 1.5 slice.12
  168.2 14.3 %collective-permute-done.15.refs_1_ = bf16[192,2048]{1,0:T(8,128)(2,1)S(1)} collective-permute-done((bf16[192,2048]{1,0:T(8,128)(2,1)S(1)}, bf16[192,2048]{1,0:T(8,128)(2,1)S(1)}, u32[]{:S(2)}, u32[]{:S(2)}) %collective-permute-start.15) | collective-permute-done | bytes 786464 | tf_op jit(solution)/shard_map/ppermute | solution.py:598
  182.4 1.2 collective-permute-start.14
  183.7 0.3 collective-permute-done.32.refs_31_.refs_32_
  184.0 0.2 collective-permute-start.27
  184.2 0.3 collective-permute-start.33
  184.5 2.1 collective-permute-done.34.refs_33_.refs_34_
  186.6 0.7 collective-permute-done.27.refs_26_.refs_27_
  187.3 1.1 collective-permute-done.33.refs_32_.refs_33_
  188.5 0.9 copy-done.16
  189.4 0.3 collective-permute-done.35.refs_34_.refs_35_
  189.7 11.3 %shard_map.190 = bf16[192,2048]{1,0:T(8,128)(2,1)} custom-call(s32[16]{0:T(128)} %compare_convert_fusion.refs_0_, bf16[192,2048]{1,0:T(8,128)(2,1)} %copy-done.15, f32[8,512]{1,0:T(8,128)} %copy-done.20, bf16[1536,256]{1,0:T(8,128)(2,1)} %get-tuple-element.43.refs_3_.refs_4_, bf16[1536,256]{1,0:T(8,128)(2,1)} %copy-done.6, ...), custom_call_target="tpu_custom_call" | custom-call | flops 4831838208 | bytes 25165824 | tf_op jit(solution)/shard_map/pallas_call | solution.py:330
  201.0 0.8 collective-permute-start.36
  201.9 12.3 %collective-permute-done.14.refs_1_ = bf16[320,2048]{1,0:T(8,128)(2,1)} collective-permute-done((bf16[320,2048]{1,0:T(8,128)(2,1)S(1)}, bf16[320,2048]{1,0:T(8,128)(2,1)}, u32[]{:S(2)}, u32[]{:S(2)}) %collective-permute-start.14) | collective-permute-done | bytes 1310752 | tf_op jit(solution)/shard_map/ppermute | solution.py:599
  214.2 14.2 %shard_map.191 = (bf16[128,2048]{1,0:T(8,128)(2,1)}, bf16[192,2048]{1,0:T(8,128)(2,1)}) custom-call(s32[16]{0:T(128)} %compare_convert_fusion.refs_0_, bf16[320,2048]{1,0:T(8,128)(2,1)} %collective-permute-done.14.refs_1_, f32[8,512]{1,0:T(8,128)} %copy-done.20, bf16[1536,256]{1,0:T(8,128)(2,1)} %get-tuple-element.43.refs_3_.refs_4_, ...), custom_call_target="tpu_custom_call" | custom-call | flops 8053063680 | bytes 25165824 | tf_op jit(solution)/shard_map/pallas_call | solution.py:330
  228.4 1.3 collective-permute-start.37
  229.7 0.8 collective-permute-start.38
  230.5 21.2 %shard_map.192.refs_1_.refs_2_ = f32[512,2048]{1,0:T(8,128)} custom-call(s32[16]{0:T(128)} %compare_convert_fusion.refs_0_, bf16[512,2048]{1,0:T(8,128)(2,1)} %get-tuple-element.57.refs_1_, f32[8,512]{1,0:T(8,128)} %concatenate.12.refs_2_, f32[512,2048]{1,0:T(8,128)} %get-tuple-element.59.refs_3_, bf16[1536,256]{1,0:T(8,128)(2,1)} %get-tuple-element.43.refs_3_.refs_4_, ...), custom_call_target="tpu_custom_call" | custom-call | flops 12884901888 | bytes 25165824 | tf_op jit(solution)/shard_map/pallas_call | solution.py:330
  251.7 0.9 copy-done.17
  252.6 0.3 copy-done.18
  252.8 6.0 %shard_map.193.refs_0_ = bf16[512,2048]{1,0:T(8,128)(2,1)} custom-call(bf16[512,2048]{1,0:T(8,128)(2,1)} %get-tuple-element.39.refs_0_.refs_1_, f32[512,2048]{1,0:T(8,128)} %shard_map.192.refs_1_.refs_2_, bf16[192,2048]{1,0:T(8,128)(2,1)} %copy-done.17, bf16[192,2048]{1,0:T(8,128)(2,1)} %copy-done.18, f32[1,2048]{1,0:T(1,128)} %bitcast.29), custom_call_target="tpu_custom_call" | custom-call | flops 786432 | bytes 7864320 | tf_op jit(solution)/shard_map/pallas_call | solution.py:400
  258.9 0.8 copy-done.19
  259.7 2.4 shard_map.194
  (86 shorter events, 0.3 us)
Async XLA Ops:
  2.8 29.8 %copy-start.21 = (f32[512,2]{0,1:T(2,128)S(1)}, f32[512,2]{0,1:T(2,128)}, u32[]{:S(2)}) copy-start(f32[512,2]{0,1:T(2,128)} %param.32) | copy-start | bytes 12292
  2.8 29.8 %copy-start.22 = (s32[512,2]{0,1:T(2,128)S(1)}, s32[512,2]{0,1:T(2,128)}, u32[]{:S(2)}) copy-start(s32[512,2]{0,1:T(2,128)} %param.31) | copy-start | bytes 12292
  2.8 38.2 %copy-start.5 = (bf16[1536,256]{1,0:T(8,128)(2,1)S(1)}, bf16[1536,256]{1,0:T(8,128)(2,1)}, u32[]{:S(2)}) copy-start(bf16[1536,256]{1,0:T(8,128)(2,1)} %get-tuple-element.45.refs_5_.refs_6_) | copy-start | bytes 2359300
  2.8 42.4 %copy-start.23 = (f32[64]{0:T(128)S(1)}, f32[64]{0:T(128)}, u32[]{:S(2)}) copy-start(f32[64]{0:T(128)} %param.27) | copy-start | bytes 772
  2.8 41.0 %collective-permute-start.10 = (bf16[1536,256]{1,0:T(8,128)(2,1)}, bf16[1536,256]{1,0:T(8,128)(2,1)}, u32[]{:S(2)}, u32[]{:S(2)}) collective-permute-start(bf16[1536,256]{1,0:T(8,128)(2,1)} %get-tuple-element.43.refs_3_.refs_4_), channel_id=1, source_target_pairs={{0,8},{1,9},{2,0},{3,1},{4,2},{5,3},{6,4},{7,5},{14,6},{15,7},{12,... | collective-permute-start | bytes 2359304 | tf_op jit(solution)/shard_map/ppermute | solution.py:498
  2.9 40.9 %collective-permute-start.6 = (bf16[1536,256]{1,0:T(8,128)(2,1)}, bf16[1536,256]{1,0:T(8,128)(2,1)}, u32[]{:S(2)}, u32[]{:S(2)}) collective-permute-start(bf16[1536,256]{1,0:T(8,128)(2,1)} %get-tuple-element.43.refs_3_.refs_4_), channel_id=1, source_target_pairs={{0,2},{1,3},{2,4},{3,5},{4,6},{5,7},{6,14},{7,15},{14,12},{15,13},... | collective-permute-start | bytes 2359304 | tf_op jit(solution)/shard_map/ppermute | solution.py:498
  4.9 39.4 %collective-permute-start.4 = (bf16[1536,256]{1,0:T(8,128)(2,1)}, bf16[1536,256]{1,0:T(8,128)(2,1)S(1)}, u32[]{:S(2)}, u32[]{:S(2)}) collective-permute-start(bf16[1536,256]{1,0:T(8,128)(2,1)} %get-tuple-element.43.refs_3_.refs_4_), channel_id=1, source_target_pairs={{0,1},{1,0},{2,3},{3,2},{4,5},{5,4},{6,7},{7,6},{8,9},{9,8},{10,11... | collective-permute-start | bytes 2359304 | tf_op jit(solution)/shard_map/ppermute | solution.py:553
  30.0 7.6 %collective-permute-start.2 = (f32[136,128]{1,0:T(8,128)}, f32[136,128]{1,0:T(8,128)S(1)}, u32[]{:S(2)}, u32[]{:S(2)}) collective-permute-start(f32[136,128]{1,0:T(8,128)} %get-tuple-element.35), channel_id=1, source_target_pairs={{0,24},{8,16},{16,8},{24,0},{1,25},{9,17},{17,9},{25,1},{2,26},{10... | collective-permute-start | bytes 208904 | tf_op jit(solution)/shard_map/ppermute | solution.py:531
  32.6 3.8 %collective-permute-start.3 = (f32[8,512]{1,0:T(8,128)S(1)}, f32[8,512]{1,0:T(8,128)S(1)}, u32[]{:S(2)}, u32[]{:S(2)}) collective-permute-start(f32[8,512]{1,0:T(8,128)S(1)} %concatenate.13), channel_id=1, source_target_pairs={{0,16},{16,0},{1,17},{17,1},{2,18},{18,2},{3,19},{19,3},{4,20},{20... | collective-permute-start | bytes 49160 | tf_op jit(solution)/shard_map/ppermute | solution.py:523
  36.4 49.8 %copy-start.20 = (f32[8,512]{1,0:T(8,128)}, f32[8,512]{1,0:T(8,128)S(1)}, u32[]{:S(2)}) copy-start(f32[8,512]{1,0:T(8,128)S(1)} %collective-permute-done.3.refs_2_) | copy-start | bytes 49156
  36.4 4.5 %collective-permute-start.1 = (f32[136,128]{1,0:T(8,128)}, f32[136,128]{1,0:T(8,128)S(1)}, u32[]{:S(2)}, u32[]{:S(2)}) collective-permute-start(f32[136,128]{1,0:T(8,128)} %get-tuple-element.35), channel_id=1, source_target_pairs={{0,16},{8,24},{16,0},{24,8},{1,17},{9,25},{17,1},{25,9},{2,18},{10... | collective-permute-start | bytes 208904 | tf_op jit(solution)/shard_map/ppermute | solution.py:531
  37.7 4.5 %collective-permute-start = (f32[136,128]{1,0:T(8,128)}, f32[136,128]{1,0:T(8,128)S(1)}, u32[]{:S(2)}, u32[]{:S(2)}) collective-permute-start(f32[136,128]{1,0:T(8,128)} %get-tuple-element.35), channel_id=1, source_target_pairs={{0,8},{8,0},{16,24},{24,16},{1,9},{9,1},{17,25},{25,17},{2,10},{10... | collective-permute-start | bytes 208904 | tf_op jit(solution)/shard_map/ppermute | solution.py:531
  41.0 20.5 %collective-permute-start.12 = (bf16[1536,256]{1,0:T(8,128)(2,1)S(1)}, bf16[1536,256]{1,0:T(8,128)(2,1)}, u32[]{:S(2)}, u32[]{:S(2)}) collective-permute-start(bf16[1536,256]{1,0:T(8,128)(2,1)S(1)} %copy-done.5), channel_id=1, source_target_pairs={{0,8},{1,9},{2,0},{3,1},{4,2},{5,3},{6,4},{7,5},{14,6},{15,7},{12,... | collective-permute-start | bytes 2359304 | tf_op jit(solution)/shard_map/ppermute | solution.py:498
  42.2 20.9 %collective-permute-start.8 = (bf16[1536,256]{1,0:T(8,128)(2,1)S(1)}, bf16[1536,256]{1,0:T(8,128)(2,1)S(1)}, u32[]{:S(2)}, u32[]{:S(2)}) collective-permute-start(bf16[1536,256]{1,0:T(8,128)(2,1)S(1)} %copy-done.5), channel_id=1, source_target_pairs={{0,2},{1,3},{2,4},{3,5},{4,6},{5,7},{6,14},{7,15},{14,12},{15,13},... | collective-permute-start | bytes 2359304 | tf_op jit(solution)/shard_map/ppermute | solution.py:498
  43.8 19.3 %collective-permute-start.5 = (bf16[1536,256]{1,0:T(8,128)(2,1)S(1)}, bf16[1536,256]{1,0:T(8,128)(2,1)S(1)}, u32[]{:S(2)}, u32[]{:S(2)}) collective-permute-start(bf16[1536,256]{1,0:T(8,128)(2,1)S(1)} %copy-done.5), channel_id=1, source_target_pairs={{0,1},{1,0},{2,3},{3,2},{4,5},{5,4},{6,7},{7,6},{8,9},{9,8},{10,11... | collective-permute-start | bytes 2359304 | tf_op jit(solution)/shard_map/ppermute | solution.py:553
  43.8 34.5 %collective-permute-start.20 = (bf16[1536,256]{1,0:T(8,128)(2,1)}, bf16[1536,256]{1,0:T(8,128)(2,1)}, u32[]{:S(2)}, u32[]{:S(2)}) collective-permute-start(bf16[1536,256]{1,0:T(8,128)(2,1)} %collective-permute-done.10.refs_11_.refs_12_), channel_id=1, source_target_pairs={{0,8},{1,9},{2,0},{3,1},{4,2},{5,3},{6,4},{7,5},{14,6},{15,7},{12,... | collective-permute-start | bytes 2359304 | tf_op jit(solution)/shard_map/ppermute | solution.py:498
  44.3 35.6 %copy-start.6 = (bf16[1536,256]{1,0:T(8,128)(2,1)}, bf16[1536,256]{1,0:T(8,128)(2,1)S(1)}, u32[]{:S(2)}) copy-start(bf16[1536,256]{1,0:T(8,128)(2,1)S(1)} %collective-permute-done.4.refs_4_.refs_5_) | copy-start | bytes 2359300
  44.3 47.6 %collective-permute-start.11 = (bf16[1536,256]{1,0:T(8,128)(2,1)}, bf16[1536,256]{1,0:T(8,128)(2,1)}, u32[]{:S(2)}, u32[]{:S(2)}) collective-permute-start(bf16[1536,256]{1,0:T(8,128)(2,1)} %collective-permute-done.10.refs_11_.refs_12_), channel_id=1, source_target_pairs={{0,1},{1,0},{2,3},{3,2},{4,5},{5,4},{6,7},{7,6},{8,9},{9,8},{10,11... | collective-permute-start | bytes 2359304 | tf_op jit(solution)/shard_map/ppermute | solution.py:553
  61.5 31.9 %collective-permute-start.16 = (bf16[1536,256]{1,0:T(8,128)(2,1)}, bf16[1536,256]{1,0:T(8,128)(2,1)}, u32[]{:S(2)}, u32[]{:S(2)}) collective-permute-start(bf16[1536,256]{1,0:T(8,128)(2,1)} %collective-permute-done.6.refs_7_.refs_8_), channel_id=1, source_target_pairs={{0,2},{1,3},{2,4},{3,5},{4,6},{5,7},{6,14},{7,15},{14,12},{15,13},... | collective-permute-start | bytes 2359304 | tf_op jit(solution)/shard_map/ppermute | solution.py:498
  63.1 16.9 %copy-start.7 = (bf16[1536,256]{1,0:T(8,128)(2,1)}, bf16[1536,256]{1,0:T(8,128)(2,1)S(1)}, u32[]{:S(2)}) copy-start(bf16[1536,256]{1,0:T(8,128)(2,1)S(1)} %collective-permute-done.8.refs_9_.refs_10_) | copy-start | bytes 2359300
  63.1 30.3 %collective-permute-start.7 = (bf16[1536,256]{1,0:T(8,128)(2,1)}, bf16[1536,256]{1,0:T(8,128)(2,1)}, u32[]{:S(2)}, u32[]{:S(2)}) collective-permute-start(bf16[1536,256]{1,0:T(8,128)(2,1)} %collective-permute-done.6.refs_7_.refs_8_), channel_id=1, source_target_pairs={{0,1},{1,0},{2,3},{3,2},{4,5},{5,4},{6,7},{7,6},{8,9},{9,8},{10,11... | collective-permute-start | bytes 2359304 | tf_op jit(solution)/shard_map/ppermute | solution.py:553
  63.1 23.2 %copy-start.8 = (bf16[1536,256]{1,0:T(8,128)(2,1)}, bf16[1536,256]{1,0:T(8,128)(2,1)S(1)}, u32[]{:S(2)}) copy-start(bf16[1536,256]{1,0:T(8,128)(2,1)S(1)} %collective-permute-done.5.refs_6_.refs_7_) | copy-start | bytes 2359300
  63.1 30.9 %collective-permute-start.22 = (bf16[1536,256]{1,0:T(8,128)(2,1)}, bf16[1536,256]{1,0:T(8,128)(2,1)}, u32[]{:S(2)}, u32[]{:S(2)}) collective-permute-start(bf16[1536,256]{1,0:T(8,128)(2,1)} %collective-permute-done.12.refs_13_.refs_14_), channel_id=1, source_target_pairs={{0,8},{1,9},{2,0},{3,1},{4,2},{5,3},{6,4},{7,5},{14,6},{15,7},{12,... | collective-permute-start | bytes 2359304 | tf_op jit(solution)/shard_map/ppermute | solution.py:498
  78.3 15.8 %collective-permute-start.13 = (bf16[1536,256]{1,0:T(8,128)(2,1)}, bf16[1536,256]{1,0:T(8,128)(2,1)}, u32[]{:S(2)}, u32[]{:S(2)}) collective-permute-start(bf16[1536,256]{1,0:T(8,128)(2,1)} %collective-permute-done.12.refs_13_.refs_14_), channel_id=1, source_target_pairs={{0,1},{1,0},{2,3},{3,2},{4,5},{5,4},{6,7},{7,6},{8,9},{9,8},{10,11... | collective-permute-start | bytes 2359304 | tf_op jit(solution)/shard_map/ppermute | solution.py:553
  86.2 63.8 %copy-start = (bf16[2048,256]{1,0:T(8,128)(2,1)S(1)}, bf16[2048,256]{1,0:T(8,128)(2,1)}, u32[]{:S(2)}) copy-start(bf16[2048,256]{1,0:T(8,128)(2,1)} %gate_ref.3) | copy-start | bytes 3145732
  86.3 63.8 %copy-start.1 = (bf16[2048,256]{1,0:T(8,128)(2,1)S(1)}, bf16[2048,256]{1,0:T(8,128)(2,1)}, u32[]{:S(2)}) copy-start(bf16[2048,256]{1,0:T(8,128)(2,1)} %up_ref.3) | copy-start | bytes 3145732
  86.3 63.8 %copy-start.3 = (f32[2048]{0:T(1024)S(1)}, f32[2048]{0:T(1024)}, u32[]{:S(2)}) copy-start(f32[2048]{0:T(1024)} %param.29) | copy-start | bytes 24580
  86.3 63.8 %copy-start.4 = (f32[2048]{0:T(1024)S(1)}, f32[2048]{0:T(1024)}, u32[]{:S(2)}) copy-start(f32[2048]{0:T(1024)} %param.30) | copy-start | bytes 24580
  86.3 63.8 %all-to-all-start = ((bf16[8,512,128]{2,1,0:T(8,128)(2,1)}), bf16[8,512,128]{2,1,0:T(8,128)(2,1)S(1)}, u32[]{:S(2)}, u32[]{:S(2)}) async-start(bf16[8,512,128]{2,1,0:T(8,128)(2,1)} %bitcast.24), calls=%async_computation | async-start | bytes 2097152 | tf_op jit(solution)/shard_map/all_to_all | solution.py:543
  91.9 40.1 %collective-permute-start.18 = (bf16[1536,256]{1,0:T(8,128)(2,1)}, bf16[1536,256]{1,0:T(8,128)(2,1)}, u32[]{:S(2)}, u32[]{:S(2)}) collective-permute-start(bf16[1536,256]{1,0:T(8,128)(2,1)} %copy-done.7), channel_id=1, source_target_pairs={{0,2},{1,3},{2,4},{3,5},{4,6},{5,7},{6,14},{7,15},{14,12},{15,13},... | collective-permute-start | bytes 2359304 | tf_op jit(solution)/shard_map/ppermute | solution.py:498
  93.3 38.6 %collective-permute-start.9 = (bf16[1536,256]{1,0:T(8,128)(2,1)}, bf16[1536,256]{1,0:T(8,128)(2,1)}, u32[]{:S(2)}, u32[]{:S(2)}) collective-permute-start(bf16[1536,256]{1,0:T(8,128)(2,1)} %copy-done.7), channel_id=1, source_target_pairs={{0,1},{1,0},{2,3},{3,2},{4,5},{5,4},{6,7},{7,6},{8,9},{9,8},{10,11... | collective-permute-start | bytes 2359304 | tf_op jit(solution)/shard_map/ppermute | solution.py:553
  93.3 40.6 %collective-permute-start.28 = (bf16[1536,256]{1,0:T(8,128)(2,1)}, bf16[1536,256]{1,0:T(8,128)(2,1)}, u32[]{:S(2)}, u32[]{:S(2)}) collective-permute-start(bf16[1536,256]{1,0:T(8,128)(2,1)} %collective-permute-done.20.refs_19_.refs_20_), channel_id=1, source_target_pairs={{0,8},{1,9},{2,0},{3,1},{4,2},{5,3},{6,4},{7,5},{14,6},{15,7},{12,... | collective-permute-start | bytes 2359304 | tf_op jit(solution)/shard_map/ppermute | solution.py:498
  94.0 40.0 %collective-permute-start.21 = (bf16[1536,256]{1,0:T(8,128)(2,1)}, bf16[1536,256]{1,0:T(8,128)(2,1)}, u32[]{:S(2)}, u32[]{:S(2)}) collective-permute-start(bf16[1536,256]{1,0:T(8,128)(2,1)} %collective-permute-done.20.refs_19_.refs_20_), channel_id=1, source_target_pairs={{0,1},{1,0},{2,3},{3,2},{4,5},{5,4},{6,7},{7,6},{8,9},{9,8},{10,11... | collective-permute-start | bytes 2359304 | tf_op jit(solution)/shard_map/ppermute | solution.py:553
  94.1 54.6 %collective-permute-start.24 = (bf16[1536,256]{1,0:T(8,128)(2,1)}, bf16[1536,256]{1,0:T(8,128)(2,1)}, u32[]{:S(2)}, u32[]{:S(2)}) collective-permute-start(bf16[1536,256]{1,0:T(8,128)(2,1)} %collective-permute-done.16.refs_15_.refs_16_), channel_id=1, source_target_pairs={{0,2},{1,3},{2,4},{3,5},{4,6},{5,7},{6,14},{7,15},{14,12},{15,13},... | collective-permute-start | bytes 2359304 | tf_op jit(solution)/shard_map/ppermute | solution.py:498
  131.9 30.5 %collective-permute-start.17 = (bf16[1536,256]{1,0:T(8,128)(2,1)}, bf16[1536,256]{1,0:T(8,128)(2,1)}, u32[]{:S(2)}, u32[]{:S(2)}) collective-permute-start(bf16[1536,256]{1,0:T(8,128)(2,1)} %collective-permute-done.16.refs_15_.refs_16_), channel_id=1, source_target_pairs={{0,1},{1,0},{2,3},{3,2},{4,5},{5,4},{6,7},{7,6},{8,9},{9,8},{10,11... | collective-permute-start | bytes 2359304 | tf_op jit(solution)/shard_map/ppermute | solution.py:553
  132.0 31.8 %collective-permute-start.30 = (bf16[1536,256]{1,0:T(8,128)(2,1)}, bf16[1536,256]{1,0:T(8,128)(2,1)}, u32[]{:S(2)}, u32[]{:S(2)}) collective-permute-start(bf16[1536,256]{1,0:T(8,128)(2,1)} %collective-permute-done.22.refs_21_.refs_22_), channel_id=1, source_target_pairs={{0,8},{1,9},{2,0},{3,1},{4,2},{5,3},{6,4},{7,5},{14,6},{15,7},{12,... | collective-permute-start | bytes 2359304 | tf_op jit(solution)/shard_map/ppermute | solution.py:498
  134.0 30.0 %collective-permute-start.23 = (bf16[1536,256]{1,0:T(8,128)(2,1)}, bf16[1536,256]{1,0:T(8,128)(2,1)}, u32[]{:S(2)}, u32[]{:S(2)}) collective-permute-start(bf16[1536,256]{1,0:T(8,128)(2,1)} %collective-permute-done.22.refs_21_.refs_22_), channel_id=1, source_target_pairs={{0,1},{1,0},{2,3},{3,2},{4,5},{5,4},{6,7},{7,6},{8,9},{9,8},{10,11... | collective-permute-start | bytes 2359304 | tf_op jit(solution)/shard_map/ppermute | solution.py:553
  134.0 32.5 %collective-permute-start.26 = (bf16[1536,256]{1,0:T(8,128)(2,1)}, bf16[1536,256]{1,0:T(8,128)(2,1)}, u32[]{:S(2)}, u32[]{:S(2)}) collective-permute-start(bf16[1536,256]{1,0:T(8,128)(2,1)} %collective-permute-done.18.refs_17_.refs_18_), channel_id=1, source_target_pairs={{0,2},{1,3},{2,4},{3,5},{4,6},{5,7},{6,14},{7,15},{14,12},{15,13},... | collective-permute-start | bytes 2359304 | tf_op jit(solution)/shard_map/ppermute | solution.py:498
  148.8 17.7 %collective-permute-start.19 = (bf16[1536,256]{1,0:T(8,128)(2,1)}, bf16[1536,256]{1,0:T(8,128)(2,1)}, u32[]{:S(2)}, u32[]{:S(2)}) collective-permute-start(bf16[1536,256]{1,0:T(8,128)(2,1)} %collective-permute-done.18.refs_17_.refs_18_), channel_id=1, source_target_pairs={{0,1},{1,0},{2,3},{3,2},{4,5},{5,4},{6,7},{7,6},{8,9},{9,8},{10,11... | collective-permute-start | bytes 2359304 | tf_op jit(solution)/shard_map/ppermute | solution.py:553
  150.1 1.2 copy-start.2
  162.4 20.0 %collective-permute-start.15 = (bf16[192,2048]{1,0:T(8,128)(2,1)S(1)}, bf16[192,2048]{1,0:T(8,128)(2,1)S(1)}, u32[]{:S(2)}, u32[]{:S(2)}) collective-permute-start(bf16[192,2048]{1,0:T(8,128)(2,1)S(1)} %slice.13), channel_id=1, source_target_pairs={{0,16},{16,0},{1,17},{17,1},{2,18},{18,2},{3,19},{19,3},{4,20},{20... | collective-permute-start | bytes 2359304 | tf_op jit(solution)/shard_map/ppermute | solution.py:598
  163.7 19.9 %collective-permute-start.29 = (bf16[1536,256]{1,0:T(8,128)(2,1)}, bf16[1536,256]{1,0:T(8,128)(2,1)S(1)}, u32[]{:S(2)}, u32[]{:S(2)}) collective-permute-start(bf16[1536,256]{1,0:T(8,128)(2,1)} %collective-permute-done.28.refs_27_.refs_28_), channel_id=1, source_target_pairs={{0,1},{1,0},{2,3},{3,2},{4,5},{5,4},{6,7},{7,6},{8,9},{9,8},{10,11... | collective-permute-start | bytes 2359304 | tf_op jit(solution)/shard_map/ppermute | solution.py:553
  164.0 20.1 %collective-permute-start.32 = (bf16[1536,256]{1,0:T(8,128)(2,1)}, bf16[1536,256]{1,0:T(8,128)(2,1)S(1)}, u32[]{:S(2)}, u32[]{:S(2)}) collective-permute-start(bf16[1536,256]{1,0:T(8,128)(2,1)} %collective-permute-done.24.refs_23_.refs_24_), channel_id=1, source_target_pairs={{0,2},{1,3},{2,4},{3,5},{4,6},{5,7},{6,14},{7,15},{14,12},{15,13},... | collective-permute-start | bytes 2359304 | tf_op jit(solution)/shard_map/ppermute | solution.py:498
  166.5 17.8 %collective-permute-start.25 = (bf16[1536,256]{1,0:T(8,128)(2,1)}, bf16[1536,256]{1,0:T(8,128)(2,1)S(1)}, u32[]{:S(2)}, u32[]{:S(2)}) collective-permute-start(bf16[1536,256]{1,0:T(8,128)(2,1)} %collective-permute-done.24.refs_23_.refs_24_), channel_id=1, source_target_pairs={{0,1},{1,0},{2,3},{3,2},{4,5},{5,4},{6,7},{7,6},{8,9},{9,8},{10,11... | collective-permute-start | bytes 2359304 | tf_op jit(solution)/shard_map/ppermute | solution.py:553
  166.5 20.2 %collective-permute-start.34 = (bf16[1536,256]{1,0:T(8,128)(2,1)}, bf16[1536,256]{1,0:T(8,128)(2,1)S(1)}, u32[]{:S(2)}, u32[]{:S(2)}) collective-permute-start(bf16[1536,256]{1,0:T(8,128)(2,1)} %collective-permute-done.30.refs_29_.refs_30_), channel_id=1, source_target_pairs={{0,8},{1,9},{2,0},{3,1},{4,2},{5,3},{6,4},{7,5},{14,6},{15,7},{12,... | collective-permute-start | bytes 2359304 | tf_op jit(solution)/shard_map/ppermute | solution.py:498
  182.4 6.0 %copy-start.15 = (bf16[192,2048]{1,0:T(8,128)(2,1)}, bf16[192,2048]{1,0:T(8,128)(2,1)S(1)}, u32[]{:S(2)}) copy-start(bf16[192,2048]{1,0:T(8,128)(2,1)S(1)} %collective-permute-done.15.refs_1_) | copy-start | bytes 2359300
  182.4 31.8 %collective-permute-start.14 = (bf16[320,2048]{1,0:T(8,128)(2,1)S(1)}, bf16[320,2048]{1,0:T(8,128)(2,1)}, u32[]{:S(2)}, u32[]{:S(2)}) collective-permute-start(bf16[320,2048]{1,0:T(8,128)(2,1)S(1)} %slice.12), channel_id=1, source_target_pairs={{0,16},{16,0},{1,17},{17,1},{2,18},{18,2},{3,19},{19,3},{4,20},{20... | collective-permute-start | bytes 3932168 | tf_op jit(solution)/shard_map/ppermute | solution.py:599
  183.7 6.0 %copy-start.9 = (bf16[1536,256]{1,0:T(8,128)(2,1)}, bf16[1536,256]{1,0:T(8,128)(2,1)S(1)}, u32[]{:S(2)}) copy-start(bf16[1536,256]{1,0:T(8,128)(2,1)S(1)} %collective-permute-done.29.refs_28_.refs_29_) | copy-start | bytes 2359300
  183.7 2.9 %collective-permute-start.31 = (bf16[1536,256]{1,0:T(8,128)(2,1)}, bf16[1536,256]{1,0:T(8,128)(2,1)S(1)}, u32[]{:S(2)}, u32[]{:S(2)}) collective-permute-start(bf16[1536,256]{1,0:T(8,128)(2,1)} %collective-permute-done.30.refs_29_.refs_30_), channel_id=1, source_target_pairs={{0,1},{1,0},{2,3},{3,2},{4,5},{5,4},{6,7},{7,6},{8,9},{9,8},{10,11... | collective-permute-start | bytes 2359304 | tf_op jit(solution)/shard_map/ppermute | solution.py:553
  184.0 5.7 %copy-start.10 = (bf16[1536,256]{1,0:T(8,128)(2,1)}, bf16[1536,256]{1,0:T(8,128)(2,1)S(1)}, u32[]{:S(2)}) copy-start(bf16[1536,256]{1,0:T(8,128)(2,1)S(1)} %collective-permute-done.32.refs_31_.refs_32_) | copy-start | bytes 2359300
  184.0 3.3 %collective-permute-start.27 = (bf16[1536,256]{1,0:T(8,128)(2,1)}, bf16[1536,256]{1,0:T(8,128)(2,1)S(1)}, u32[]{:S(2)}, u32[]{:S(2)}) collective-permute-start(bf16[1536,256]{1,0:T(8,128)(2,1)} %collective-permute-done.26.refs_25_.refs_26_), channel_id=1, source_target_pairs={{0,1},{1,0},{2,3},{3,2},{4,5},{5,4},{6,7},{7,6},{8,9},{9,8},{10,11... | collective-permute-start | bytes 2359304 | tf_op jit(solution)/shard_map/ppermute | solution.py:553
  184.2 5.5 %copy-start.11 = (bf16[1536,256]{1,0:T(8,128)(2,1)}, bf16[1536,256]{1,0:T(8,128)(2,1)S(1)}, u32[]{:S(2)}) copy-start(bf16[1536,256]{1,0:T(8,128)(2,1)S(1)} %collective-permute-done.25.refs_24_.refs_25_) | copy-start | bytes 2359300
  184.2 4.2 %collective-permute-start.33 = (bf16[1536,256]{1,0:T(8,128)(2,1)S(1)}, bf16[1536,256]{1,0:T(8,128)(2,1)S(1)}, u32[]{:S(2)}, u32[]{:S(2)}) collective-permute-start(bf16[1536,256]{1,0:T(8,128)(2,1)S(1)} %collective-permute-done.32.refs_31_.refs_32_), channel_id=1, source_target_pairs={{0,1},{1,0},{2,3},{3,2},{4,5},{5,4},{6,7},{7,6},{8,9},{9,8},{10,11... | collective-permute-start | bytes 2359304 | tf_op jit(solution)/shard_map/ppermute | solution.py:553
  186.6 1.8 copy-start.12
  186.6 3.1 %collective-permute-start.35 = (bf16[1536,256]{1,0:T(8,128)(2,1)S(1)}, bf16[1536,256]{1,0:T(8,128)(2,1)}, u32[]{:S(2)}, u32[]{:S(2)}) collective-permute-start(bf16[1536,256]{1,0:T(8,128)(2,1)S(1)} %collective-permute-done.34.refs_33_.refs_34_), channel_id=1, source_target_pairs={{0,1},{1,0},{2,3},{3,2},{4,5},{5,4},{6,7},{7,6},{8,9},{9,8},{10,11... | collective-permute-start | bytes 2359304 | tf_op jit(solution)/shard_map/ppermute | solution.py:553
  186.6 1.8 copy-start.13
  187.3 1.1 copy-start.14
  188.5 0.9 copy-start.16
  201.0 50.6 %collective-permute-start.36 = (bf16[192,2048]{1,0:T(8,128)(2,1)}, bf16[192,2048]{1,0:T(8,128)(2,1)S(1)}, u32[]{:S(2)}, u32[]{:S(2)}) collective-permute-start(bf16[192,2048]{1,0:T(8,128)(2,1)} %shard_map.190), channel_id=1, source_target_pairs={{0,16},{16,0},{1,17},{17,1},{2,18},{18,2},{3,19},{19,3},{4,20},{20... | collective-permute-start | bytes 2359304 | tf_op jit(solution)/shard_map/ppermute | solution.py:607
  228.4 23.3 %collective-permute-start.37 = (bf16[192,2048]{1,0:T(8,128)(2,1)}, bf16[192,2048]{1,0:T(8,128)(2,1)S(1)}, u32[]{:S(2)}, u32[]{:S(2)}) collective-permute-start(bf16[192,2048]{1,0:T(8,128)(2,1)} %get-tuple-element.56), channel_id=1, source_target_pairs={{0,16},{16,0},{1,17},{17,1},{2,18},{18,2},{3,19},{19,3},{4,20},{20... | collective-permute-start | bytes 2359304 | tf_op jit(solution)/shard_map/ppermute | solution.py:611
  229.7 29.2 %collective-permute-start.38 = (bf16[128,2048]{1,0:T(8,128)(2,1)}, bf16[128,2048]{1,0:T(8,128)(2,1)S(1)}, u32[]{:S(2)}, u32[]{:S(2)}) collective-permute-start(bf16[128,2048]{1,0:T(8,128)(2,1)} %get-tuple-element.60), channel_id=1, source_target_pairs={{0,16},{16,0},{1,17},{17,1},{2,18},{18,2},{3,19},{19,3},{4,20},{20... | collective-permute-start | bytes 1572872 | tf_op jit(solution)/shard_map/ppermute | solution.py:611
  251.7 0.9 copy-start.17
  251.7 1.2 copy-start.18
  258.9 0.8 copy-start.19

commit v5 on v4

--- a/solution.py
+++ b/solution.py
@@ -549,8 +549,8 @@
         held = []
 
         def hold(slot, start, array):
-            held.append((array, slot, start))
-            held.append((lax.ppermute(array, "tp", partner), slot + 1, start))
+            for j, one in enumerate((array, lax.ppermute(array, "tp", partner))):
+                held.append((one, slot + j, start))
 
         def hold_hop(k):
             hold(4 * k - 2, 0, long_a[k])
@@ -566,7 +566,7 @@
         mixed, which, own_share, far_share, early = lax.optimization_barrier(
             (mixed, which, own_share, far_share, [array for array, _, _ in held])
         )
-        held = [(array, slot, start) for array, (_, slot, start) in zip(early, held)]
+        held[:] = [(array, slot, start) for array, (_, slot, start) in zip(early, held)]
     if channels % 128 == 0:
         stream, normed, shared = project_call(
             mixed,
@@ -600,6 +600,9 @@
     hop("long")
 
     hold_hop(2)
+    arrays = [array for array, _, _ in held]
+    arrays, long_a[4], long_b[4] = lax.optimization_barrier((arrays, long_a[4], long_b[4]))
+    held[:] = [(array, slot, start) for array, (_, slot, start) in zip(arrays, held)]
     hold_hop(3)
     hold(14, 0, long_a[4])
     hold(14, half, long_b[4])

time: 265 us -> 267 us (level)
    ppermute x14, waiting for transfers between devices: 84.9 us -> 98.7 us  [hop(): chain.append(lax.ppermute(chain[-1], ring, perm))]
    ppermute x1, waiting for transfers between devices: 14.3 us -> 2.24 us  [body(): far_first = lax.ppermute(normed[:first], outer, swap)]
  transfers between devices with their start and end apart: 40 -> 40, of which waited for: 15 -> 16; matrix products, arithmetic and copies ran while one was open for 3% -> 3% of each run, Pallas kernels for 36% -> 36%
where the time goes in v5:
time: 267 us; the launch traced here: 265 us
  waiting for transfers between devices  121 us (45%)
  Pallas kernels  99.3 us (37%)
  starting transfers between devices  33.5 us (13%)
  local copies, waits for them, and re-layouts  8.2 us (3%)
  other arithmetic  2.84 us (1%)
    ppermute x14, waiting for transfers between devices, hop(): chain.append(lax.ppermute(chain[-1], ring, perm))  98.7 us
    pallas_call x3, Pallas kernels, expert_call(): pl.pallas_call(functools.partial(expert_kernel, based=base is not None, s...  46.7 us
    pallas_call x1, Pallas kernels, scan_call(): pl.pallas_call(scan_kernel, grid=(tokens // span,), in_specs=[block, bloc...  25.2 us
    ppermute x14, starting transfers between devices, hop(): chain.append(lax.ppermute(chain[-1], ring, perm))  14.9 us
    ppermute x1, waiting for transfers between devices, body(): far_rest = lax.ppermute(normed[first:], outer, swap)  10.8 us
    pallas_call x1, Pallas kernels, project_call(): pl.pallas_call(project_kernel, grid=(rows // span,), in_specs=[pl.BlockSp...  9.9 us
    pallas_call x2, Pallas kernels, combine_call(): pl.pallas_call(functools.partial(combine_kernel, counts=counts, followed=...  8.45 us
    pallas_call x1, Pallas kernels, gate_call(): pl.pallas_call(gate_kernel, grid=(tokens // span,), in_specs=[pl.BlockSpe...  6.31 us
  transfers between devices with their start and end apart: 40, of which 16 were waited for; matrix products, arithmetic and copies ran while one was open for 3% of the time, Pallas kernels for 36%

profile of v5, /device:TPU:8, one launch (start us, length us, event | category | flops | bytes accessed | tf_op | source)
XLA Modules:
  0.0 265.0 jit_solution(8222360995666200860)
XLA Ops:
  0.0 2.8 %pack.1 = (bf16[1536,256]{1,0:T(8,128)(2,1)}, bf16[1536,256]{1,0:T(8,128)(2,1)}) custom-call(bf16[1,2048,128]{2,1,0:T(8,128)(2,1)} %gate_ref.2, bf16[1,2048,128]{2,1,0:T(8,128)(2,1)} %up_ref.2, bf16[1,2048,128]{2,1,0:T(8,128)(2,1)} %down_ref.2), custom_call_target="tpu_custom_call" | custom-call | bytes 3145728 | tf_op jit(solution)/shard_map/pack/pallas_call | solution.py:267
  2.9 2.0 collective-permute-start.6
  4.9 25.2 %scan.1 = (f32[4096,128]{1,0:T(8,128)}, f32[4096,128]{1,0:T(8,128)}, f32[136,128]{1,0:T(8,128)}) custom-call(bf16[4096,128]{1,0:T(8,128)(2,1)} %q_ref.1, bf16[4096,128]{1,0:T(8,128)(2,1)} %f_ref.1, bf16[4096,128]{1,0:T(8,128)(2,1)} %v_ref.1, f32[1,128]{1,0:T(1,128)} %bitcast.35, f32[2,4096]{1,0:T(2,128)} %sudden_ref.1), custom_call_target="tpu_custom_call" | custom-call | flops 1048576000 | bytes 7340032 | tf_op jit(solution)/shard_map/scan/pallas_call | solution.py:123
  30.0 2.5 collective-permute-start.2
  32.6 0.6 collective-permute-start.3
  33.2 3.2 %collective-permute-done.3.refs_2_ = f32[8,512]{1,0:T(8,128)S(1)} collective-permute-done((f32[8,512]{1,0:T(8,128)S(1)}, f32[8,512]{1,0:T(8,128)S(1)}, u32[]{:S(2)}, u32[]{:S(2)}) %collective-permute-start.3) | collective-permute-done | bytes 16416 | tf_op jit(solution)/shard_map/ppermute | solution.py:523
  36.4 1.2 collective-permute-start.1
  37.7 1.3 collective-permute-start
  39.0 2.0 collective-permute-done.1
  41.0 0.4 collective-permute-start.12
  41.4 0.8 collective-permute-done
  42.2 1.6 collective-permute-start.8
  43.8 0.5 collective-permute-start.20
  44.3 0.2 collective-permute-start.11
  44.5 17.0 %collective-permute-done.12.refs_13_.refs_14_ = bf16[1536,256]{1,0:T(8,128)(2,1)} collective-permute-done((bf16[1536,256]{1,0:T(8,128)(2,1)S(1)}, bf16[1536,256]{1,0:T(8,128)(2,1)}, u32[]{:S(2)}, u32[]{:S(2)}) %collective-permute-start.12) | collective-permute-done | bytes 786464 | tf_op jit(solution)/shard_map/ppermute | solution.py:498
  61.5 1.6 collective-permute-start.16
  63.1 0.5 collective-permute-start.22
  63.6 14.7 %collective-permute-done.20.refs_19_.refs_20_ = bf16[1536,256]{1,0:T(8,128)(2,1)} collective-permute-done((bf16[1536,256]{1,0:T(8,128)(2,1)}, bf16[1536,256]{1,0:T(8,128)(2,1)}, u32[]{:S(2)}, u32[]{:S(2)}) %collective-permute-start.20) | collective-permute-done | bytes 786464 | tf_op jit(solution)/shard_map/ppermute | solution.py:498
  78.3 0.6 pad_add_fusion.mine_ref
  78.9 0.7 reshape_tile.3.gain_ref
  79.6 1.6 pad_maximum_fusion.pieces_ref
  81.2 6.3 %gate.1 = bf16[4096,128]{1,0:T(8,128)(2,1)} custom-call(s32[5]{0:T(128)} %pad_add_fusion.mine_ref, f32[4096,128]{1,0:T(8,128)} %get-tuple-element.55.local_ref, f32[4096,128]{1,0:T(8,128)} %get-tuple-element.56.lifted_ref, bf16[4096,128]{1,0:T(8,128)(2,1)} %open_ref.1, f32[4,136,128]{2,1,0:T(8,128)} %pad_maximum_fusion.pieces_ref, f32[1,128]{1,0:T(1,128)} %reshape_tile.3.gain_ref), custom_call_target="tpu_custom_call" | custom-call | flops 419430400 | bytes 5242880 | tf_op jit(solution)/shard_map/gate/pallas_call | solution.py:174
  87.6 5.6 %all-to-all-start = ((bf16[8,512,128]{2,1,0:T(8,128)(2,1)}), bf16[8,512,128]{2,1,0:T(8,128)(2,1)S(1)}, u32[]{:S(2)}, u32[]{:S(2)}) async-start(bf16[8,512,128]{2,1,0:T(8,128)(2,1)} %bitcast.24), calls=%async_computation | async-start | bytes 2097152 | tf_op jit(solution)/shard_map/all_to_all | solution.py:543
  93.2 1.5 collective-permute-start.18
  94.7 0.6 collective-permute-start.31
  95.3 0.2 collective-permute-start.21
  95.4 1.5 collective-permute-start.24
  96.9 36.3 %collective-permute-done.18.refs_17_.refs_18_ = bf16[1536,256]{1,0:T(8,128)(2,1)} collective-permute-done((bf16[1536,256]{1,0:T(8,128)(2,1)}, bf16[1536,256]{1,0:T(8,128)(2,1)}, u32[]{:S(2)}, u32[]{:S(2)}) %collective-permute-start.18) | collective-permute-done | bytes 786464 | tf_op jit(solution)/shard_map/ppermute | solution.py:498
  133.3 2.0 collective-permute-done.31.refs_27_.refs_28_
  135.3 0.5 collective-permute-start.19
  135.8 14.3 %collective-permute-done.24.refs_23_.refs_24_ = bf16[1536,256]{1,0:T(8,128)(2,1)} collective-permute-done((bf16[1536,256]{1,0:T(8,128)(2,1)}, bf16[1536,256]{1,0:T(8,128)(2,1)}, u32[]{:S(2)}, u32[]{:S(2)}) %collective-permute-start.24) | collective-permute-done | bytes 786464 | tf_op jit(solution)/shard_map/ppermute | solution.py:498
  150.0 2.5 collective-permute-start.25
  152.5 0.6 concatenate.12.refs_2_
  153.1 0.1 stack.80
  153.2 0.6 compare_convert_fusion.refs_0_
  153.9 1.2 copy-done.2
  155.1 9.9 %project.1 = (bf16[512,2048]{1,0:T(8,128)(2,1)}, bf16[512,2048]{1,0:T(8,128)(2,1)}, f32[512,2048]{1,0:T(8,128)}) custom-call(bf16[8,512,128]{2,1,0:T(8,128)(2,1)S(1)} %all-to-all-done.mixed_ref, bf16[1024,2048]{1,0:T(8,128)(2,1)} %weight_ref.1, bf16[512,2048]{1,0:T(8,128)(2,1)} %residual_ref.1, f32[1,2048]{1,0:T(1,128)S(1)} %bitcast.22, ...), custom_call_target="tpu_custom_call" | custom-call | flops 3758096384 | bytes 16777216 | tf_op jit(solution)/shard_map/project/pallas_call | solution.py:230
  165.0 1.2 slice.13
  166.2 2.2 collective-permute-start.29
  168.4 1.2 collective-permute-start.15
  169.7 1.1 collective-permute-done.25.refs_31_.refs_32_
  170.8 1.4 slice.12
  172.2 1.0 collective-permute-done.27.refs_33_.refs_34_
  173.3 1.2 collective-permute-start.14
  174.5 12.2 %collective-permute-done.29.refs_25_.refs_26_ = bf16[1536,256]{1,0:T(8,128)(2,1)S(1)} collective-permute-done((bf16[1536,256]{1,0:T(8,128)(2,1)}, bf16[1536,256]{1,0:T(8,128)(2,1)S(1)}, u32[]{:S(2)}, u32[]{:S(2)}) %collective-permute-start.29) | collective-permute-done | bytes 786464 | tf_op jit(solution)/shard_map/ppermute | solution.py:498
  186.7 2.2 collective-permute-done.15.refs_1_
  189.0 0.5 collective-permute-start.34
  189.5 0.1 collective-permute-start.35
  189.6 1.6 collective-permute-done.30.refs_26_.refs_27_
  191.3 1.1 collective-permute-done.34.refs_32_.refs_33_
  192.4 0.9 copy-done.15
  193.3 0.3 collective-permute-done.35.refs_34_.refs_35_
  193.6 11.3 %shard_map.190 = bf16[192,2048]{1,0:T(8,128)(2,1)} custom-call(s32[16]{0:T(128)} %compare_convert_fusion.refs_0_, bf16[192,2048]{1,0:T(8,128)(2,1)} %collective-permute-done.15.refs_1_, f32[8,512]{1,0:T(8,128)} %copy-done.19, bf16[1536,256]{1,0:T(8,128)(2,1)} %get-tuple-element.77.refs_3_.refs_4_, bf16[1536,256]{1,0:T(8,128)(2,1)} %copy-done.6, ...), custom_call_target="tpu_custom_call" | custom-call | flops 4831838208 | bytes 25165824 | tf_op jit(solution)/shard_map/pallas_call | solution.py:330
  204.9 1.3 collective-permute-start.36
  206.2 10.8 %collective-permute-done.14.refs_1_ = bf16[320,2048]{1,0:T(8,128)(2,1)} collective-permute-done((bf16[320,2048]{1,0:T(8,128)(2,1)S(1)}, bf16[320,2048]{1,0:T(8,128)(2,1)}, u32[]{:S(2)}, u32[]{:S(2)}) %collective-permute-start.14) | collective-permute-done | bytes 1310752 | tf_op jit(solution)/shard_map/ppermute | solution.py:599
  217.1 14.3 %shard_map.191 = (bf16[128,2048]{1,0:T(8,128)(2,1)}, bf16[192,2048]{1,0:T(8,128)(2,1)}) custom-call(s32[16]{0:T(128)} %compare_convert_fusion.refs_0_, bf16[320,2048]{1,0:T(8,128)(2,1)} %collective-permute-done.14.refs_1_, f32[8,512]{1,0:T(8,128)} %copy-done.19, bf16[1536,256]{1,0:T(8,128)(2,1)} %get-tuple-element.77.refs_3_.refs_4_, ...), custom_call_target="tpu_custom_call" | custom-call | flops 8053063680 | bytes 25165824 | tf_op jit(solution)/shard_map/pallas_call | solution.py:330
  231.3 1.3 collective-permute-start.37
  232.6 0.8 collective-permute-start.38
  233.4 21.2 %shard_map.192.refs_1_.refs_2_ = f32[512,2048]{1,0:T(8,128)} custom-call(s32[16]{0:T(128)} %compare_convert_fusion.refs_0_, bf16[512,2048]{1,0:T(8,128)(2,1)} %get-tuple-element.101.refs_1_, f32[8,512]{1,0:T(8,128)} %concatenate.12.refs_2_, f32[512,2048]{1,0:T(8,128)} %get-tuple-element.103.refs_3_, bf16[1536,256]{1,0:T(8,128)(2,1)} %get-tuple-element.77.refs_3_.refs_4_, ...), custom_call_target="tpu_custom_call" | custom-call | flops 12884901888 | bytes 25165824 | tf_op jit(solution)/shard_map/pallas_call | solution.py:330
  254.6 0.9 copy-done.16
  255.5 0.3 copy-done.17
  255.8 6.0 %shard_map.193.refs_0_ = bf16[512,2048]{1,0:T(8,128)(2,1)} custom-call(bf16[512,2048]{1,0:T(8,128)(2,1)} %get-tuple-element.61.refs_0_.refs_1_, f32[512,2048]{1,0:T(8,128)} %shard_map.192.refs_1_.refs_2_, bf16[192,2048]{1,0:T(8,128)(2,1)} %copy-done.16, bf16[192,2048]{1,0:T(8,128)(2,1)} %copy-done.17, f32[1,2048]{1,0:T(1,128)} %bitcast.29), custom_call_target="tpu_custom_call" | custom-call | flops 786432 | bytes 7864320 | tf_op jit(solution)/shard_map/pallas_call | solution.py:400
  261.8 0.8 copy-done.18
  262.6 2.4 shard_map.194
  (84 shorter events, 0.3 us)
Async XLA Ops:
  2.8 29.8 %copy-start.20 = (f32[512,2]{0,1:T(2,128)S(1)}, f32[512,2]{0,1:T(2,128)}, u32[]{:S(2)}) copy-start(f32[512,2]{0,1:T(2,128)} %param.32) | copy-start | bytes 12292
  2.8 29.8 %copy-start.21 = (s32[512,2]{0,1:T(2,128)S(1)}, s32[512,2]{0,1:T(2,128)}, u32[]{:S(2)}) copy-start(s32[512,2]{0,1:T(2,128)} %param.31) | copy-start | bytes 12292
  2.8 38.2 %copy-start.5 = (bf16[1536,256]{1,0:T(8,128)(2,1)S(1)}, bf16[1536,256]{1,0:T(8,128)(2,1)}, u32[]{:S(2)}) copy-start(bf16[1536,256]{1,0:T(8,128)(2,1)} %get-tuple-element.79.refs_5_.refs_6_) | copy-start | bytes 2359300
  2.8 76.2 %copy-start.22 = (f32[64]{0:T(128)S(1)}, f32[64]{0:T(128)}, u32[]{:S(2)}) copy-start(f32[64]{0:T(128)} %param.27) | copy-start | bytes 772
  2.8 41.0 %collective-permute-start.10 = (bf16[1536,256]{1,0:T(8,128)(2,1)}, bf16[1536,256]{1,0:T(8,128)(2,1)}, u32[]{:S(2)}, u32[]{:S(2)}) collective-permute-start(bf16[1536,256]{1,0:T(8,128)(2,1)} %get-tuple-element.77.refs_3_.refs_4_), channel_id=1, source_target_pairs={{0,8},{1,9},{2,0},{3,1},{4,2},{5,3},{6,4},{7,5},{14,6},{15,7},{12,... | collective-permute-start | bytes 2359304 | tf_op jit(solution)/shard_map/ppermute | solution.py:498
  2.9 40.9 %collective-permute-start.6 = (bf16[1536,256]{1,0:T(8,128)(2,1)}, bf16[1536,256]{1,0:T(8,128)(2,1)}, u32[]{:S(2)}, u32[]{:S(2)}) collective-permute-start(bf16[1536,256]{1,0:T(8,128)(2,1)} %get-tuple-element.77.refs_3_.refs_4_), channel_id=1, source_target_pairs={{0,2},{1,3},{2,4},{3,5},{4,6},{5,7},{6,14},{7,15},{14,12},{15,13},... | collective-permute-start | bytes 2359304 | tf_op jit(solution)/shard_map/ppermute | solution.py:498
  4.9 39.4 %collective-permute-start.4 = (bf16[1536,256]{1,0:T(8,128)(2,1)}, bf16[1536,256]{1,0:T(8,128)(2,1)S(1)}, u32[]{:S(2)}, u32[]{:S(2)}) collective-permute-start(bf16[1536,256]{1,0:T(8,128)(2,1)} %get-tuple-element.77.refs_3_.refs_4_), channel_id=1, source_target_pairs={{0,1},{1,0},{2,3},{3,2},{4,5},{5,4},{6,7},{7,6},{8,9},{9,8},{10,11... | collective-permute-start | bytes 2359304 | tf_op jit(solution)/shard_map/ppermute | solution.py:552
  30.0 7.6 %collective-permute-start.2 = (f32[136,128]{1,0:T(8,128)}, f32[136,128]{1,0:T(8,128)S(1)}, u32[]{:S(2)}, u32[]{:S(2)}) collective-permute-start(f32[136,128]{1,0:T(8,128)} %get-tuple-element.57), channel_id=1, source_target_pairs={{0,24},{8,16},{16,8},{24,0},{1,25},{9,17},{17,9},{25,1},{2,26},{10... | collective-permute-start | bytes 208904 | tf_op jit(solution)/shard_map/ppermute | solution.py:531
  32.6 3.8 %collective-permute-start.3 = (f32[8,512]{1,0:T(8,128)S(1)}, f32[8,512]{1,0:T(8,128)S(1)}, u32[]{:S(2)}, u32[]{:S(2)}) collective-permute-start(f32[8,512]{1,0:T(8,128)S(1)} %concatenate.13), channel_id=1, source_target_pairs={{0,16},{16,0},{1,17},{17,1},{2,18},{18,2},{3,19},{19,3},{4,20},{20... | collective-permute-start | bytes 49160 | tf_op jit(solution)/shard_map/ppermute | solution.py:523
  36.4 51.1 %copy-start.19 = (f32[8,512]{1,0:T(8,128)}, f32[8,512]{1,0:T(8,128)S(1)}, u32[]{:S(2)}) copy-start(f32[8,512]{1,0:T(8,128)S(1)} %collective-permute-done.3.refs_2_) | copy-start | bytes 49156
  36.4 4.5 %collective-permute-start.1 = (f32[136,128]{1,0:T(8,128)}, f32[136,128]{1,0:T(8,128)S(1)}, u32[]{:S(2)}, u32[]{:S(2)}) collective-permute-start(f32[136,128]{1,0:T(8,128)} %get-tuple-element.57), channel_id=1, source_target_pairs={{0,16},{8,24},{16,0},{24,8},{1,17},{9,25},{17,1},{25,9},{2,18},{10... | collective-permute-start | bytes 208904 | tf_op jit(solution)/shard_map/ppermute | solution.py:531
  37.7 4.5 %collective-permute-start = (f32[136,128]{1,0:T(8,128)}, f32[136,128]{1,0:T(8,128)S(1)}, u32[]{:S(2)}, u32[]{:S(2)}) collective-permute-start(f32[136,128]{1,0:T(8,128)} %get-tuple-element.57), channel_id=1, source_target_pairs={{0,8},{8,0},{16,24},{24,16},{1,9},{9,1},{17,25},{25,17},{2,10},{10... | collective-permute-start | bytes 208904 | tf_op jit(solution)/shard_map/ppermute | solution.py:531
  41.0 20.5 %collective-permute-start.12 = (bf16[1536,256]{1,0:T(8,128)(2,1)S(1)}, bf16[1536,256]{1,0:T(8,128)(2,1)}, u32[]{:S(2)}, u32[]{:S(2)}) collective-permute-start(bf16[1536,256]{1,0:T(8,128)(2,1)S(1)} %copy-done.5), channel_id=1, source_target_pairs={{0,8},{1,9},{2,0},{3,1},{4,2},{5,3},{6,4},{7,5},{14,6},{15,7},{12,... | collective-permute-start | bytes 2359304 | tf_op jit(solution)/shard_map/ppermute | solution.py:498
  42.2 20.9 %collective-permute-start.8 = (bf16[1536,256]{1,0:T(8,128)(2,1)S(1)}, bf16[1536,256]{1,0:T(8,128)(2,1)S(1)}, u32[]{:S(2)}, u32[]{:S(2)}) collective-permute-start(bf16[1536,256]{1,0:T(8,128)(2,1)S(1)} %copy-done.5), channel_id=1, source_target_pairs={{0,2},{1,3},{2,4},{3,5},{4,6},{5,7},{6,14},{7,15},{14,12},{15,13},... | collective-permute-start | bytes 2359304 | tf_op jit(solution)/shard_map/ppermute | solution.py:498
  43.8 19.3 %collective-permute-start.5 = (bf16[1536,256]{1,0:T(8,128)(2,1)S(1)}, bf16[1536,256]{1,0:T(8,128)(2,1)S(1)}, u32[]{:S(2)}, u32[]{:S(2)}) collective-permute-start(bf16[1536,256]{1,0:T(8,128)(2,1)S(1)} %copy-done.5), channel_id=1, source_target_pairs={{0,1},{1,0},{2,3},{3,2},{4,5},{5,4},{6,7},{7,6},{8,9},{9,8},{10,11... | collective-permute-start | bytes 2359304 | tf_op jit(solution)/shard_map/ppermute | solution.py:552
  43.8 34.5 %collective-permute-start.20 = (bf16[1536,256]{1,0:T(8,128)(2,1)}, bf16[1536,256]{1,0:T(8,128)(2,1)}, u32[]{:S(2)}, u32[]{:S(2)}) collective-permute-start(bf16[1536,256]{1,0:T(8,128)(2,1)} %collective-permute-done.10.refs_11_.refs_12_), channel_id=1, source_target_pairs={{0,8},{1,9},{2,0},{3,1},{4,2},{5,3},{6,4},{7,5},{14,6},{15,7},{12,... | collective-permute-start | bytes 2359304 | tf_op jit(solution)/shard_map/ppermute | solution.py:498
  44.3 36.9 %copy-start.6 = (bf16[1536,256]{1,0:T(8,128)(2,1)}, bf16[1536,256]{1,0:T(8,128)(2,1)S(1)}, u32[]{:S(2)}) copy-start(bf16[1536,256]{1,0:T(8,128)(2,1)S(1)} %collective-permute-done.4.refs_4_.refs_5_) | copy-start | bytes 2359300
  44.3 48.9 %collective-permute-start.11 = (bf16[1536,256]{1,0:T(8,128)(2,1)}, bf16[1536,256]{1,0:T(8,128)(2,1)}, u32[]{:S(2)}, u32[]{:S(2)}) collective-permute-start(bf16[1536,256]{1,0:T(8,128)(2,1)} %collective-permute-done.10.refs_11_.refs_12_), channel_id=1, source_target_pairs={{0,1},{1,0},{2,3},{3,2},{4,5},{5,4},{6,7},{7,6},{8,9},{9,8},{10,11... | collective-permute-start | bytes 2359304 | tf_op jit(solution)/shard_map/ppermute | solution.py:552
  61.5 33.2 %collective-permute-start.16 = (bf16[1536,256]{1,0:T(8,128)(2,1)}, bf16[1536,256]{1,0:T(8,128)(2,1)}, u32[]{:S(2)}, u32[]{:S(2)}) collective-permute-start(bf16[1536,256]{1,0:T(8,128)(2,1)} %collective-permute-done.6.refs_7_.refs_8_), channel_id=1, source_target_pairs={{0,2},{1,3},{2,4},{3,5},{4,6},{5,7},{6,14},{7,15},{14,12},{15,13},... | collective-permute-start | bytes 2359304 | tf_op jit(solution)/shard_map/ppermute | solution.py:498
  63.1 18.2 %copy-start.7 = (bf16[1536,256]{1,0:T(8,128)(2,1)}, bf16[1536,256]{1,0:T(8,128)(2,1)S(1)}, u32[]{:S(2)}) copy-start(bf16[1536,256]{1,0:T(8,128)(2,1)S(1)} %collective-permute-done.8.refs_9_.refs_10_) | copy-start | bytes 2359300
  63.1 31.6 %collective-permute-start.7 = (bf16[1536,256]{1,0:T(8,128)(2,1)}, bf16[1536,256]{1,0:T(8,128)(2,1)}, u32[]{:S(2)}, u32[]{:S(2)}) collective-permute-start(bf16[1536,256]{1,0:T(8,128)(2,1)} %collective-permute-done.6.refs_7_.refs_8_), channel_id=1, source_target_pairs={{0,1},{1,0},{2,3},{3,2},{4,5},{5,4},{6,7},{7,6},{8,9},{9,8},{10,11... | collective-permute-start | bytes 2359304 | tf_op jit(solution)/shard_map/ppermute | solution.py:552
  63.1 24.5 %copy-start.8 = (bf16[1536,256]{1,0:T(8,128)(2,1)}, bf16[1536,256]{1,0:T(8,128)(2,1)S(1)}, u32[]{:S(2)}) copy-start(bf16[1536,256]{1,0:T(8,128)(2,1)S(1)} %collective-permute-done.5.refs_6_.refs_7_) | copy-start | bytes 2359300
  63.1 32.2 %collective-permute-start.22 = (bf16[1536,256]{1,0:T(8,128)(2,1)}, bf16[1536,256]{1,0:T(8,128)(2,1)}, u32[]{:S(2)}, u32[]{:S(2)}) collective-permute-start(bf16[1536,256]{1,0:T(8,128)(2,1)} %collective-permute-done.12.refs_13_.refs_14_), channel_id=1, source_target_pairs={{0,8},{1,9},{2,0},{3,1},{4,2},{5,3},{6,4},{7,5},{14,6},{15,7},{12,... | collective-permute-start | bytes 2359304 | tf_op jit(solution)/shard_map/ppermute | solution.py:498
  78.3 17.1 %collective-permute-start.13 = (bf16[1536,256]{1,0:T(8,128)(2,1)}, bf16[1536,256]{1,0:T(8,128)(2,1)}, u32[]{:S(2)}, u32[]{:S(2)}) collective-permute-start(bf16[1536,256]{1,0:T(8,128)(2,1)} %collective-permute-done.12.refs_13_.refs_14_), channel_id=1, source_target_pairs={{0,1},{1,0},{2,3},{3,2},{4,5},{5,4},{6,7},{7,6},{8,9},{9,8},{10,11... | collective-permute-start | bytes 2359304 | tf_op jit(solution)/shard_map/ppermute | solution.py:552
  87.5 66.3 %copy-start = (bf16[2048,256]{1,0:T(8,128)(2,1)S(1)}, bf16[2048,256]{1,0:T(8,128)(2,1)}, u32[]{:S(2)}) copy-start(bf16[2048,256]{1,0:T(8,128)(2,1)} %gate_ref.3) | copy-start | bytes 3145732
  87.6 66.3 %copy-start.1 = (bf16[2048,256]{1,0:T(8,128)(2,1)S(1)}, bf16[2048,256]{1,0:T(8,128)(2,1)}, u32[]{:S(2)}) copy-start(bf16[2048,256]{1,0:T(8,128)(2,1)} %up_ref.3) | copy-start | bytes 3145732
  87.6 66.3 %copy-start.3 = (f32[2048]{0:T(1024)S(1)}, f32[2048]{0:T(1024)}, u32[]{:S(2)}) copy-start(f32[2048]{0:T(1024)} %param.29) | copy-start | bytes 24580
  87.6 66.3 %copy-start.4 = (f32[2048]{0:T(1024)S(1)}, f32[2048]{0:T(1024)}, u32[]{:S(2)}) copy-start(f32[2048]{0:T(1024)} %param.30) | copy-start | bytes 24580
  87.6 66.2 %all-to-all-start = ((bf16[8,512,128]{2,1,0:T(8,128)(2,1)}), bf16[8,512,128]{2,1,0:T(8,128)(2,1)S(1)}, u32[]{:S(2)}, u32[]{:S(2)}) async-start(bf16[8,512,128]{2,1,0:T(8,128)(2,1)} %bitcast.24), calls=%async_computation | async-start | bytes 2097152 | tf_op jit(solution)/shard_map/all_to_all | solution.py:543
  93.2 40.1 %collective-permute-start.18 = (bf16[1536,256]{1,0:T(8,128)(2,1)}, bf16[1536,256]{1,0:T(8,128)(2,1)}, u32[]{:S(2)}, u32[]{:S(2)}) collective-permute-start(bf16[1536,256]{1,0:T(8,128)(2,1)} %copy-done.7), channel_id=1, source_target_pairs={{0,2},{1,3},{2,4},{3,5},{4,6},{5,7},{6,14},{7,15},{14,12},{15,13},... | collective-permute-start | bytes 2359304 | tf_op jit(solution)/shard_map/ppermute | solution.py:498
  94.6 38.6 %collective-permute-start.9 = (bf16[1536,256]{1,0:T(8,128)(2,1)}, bf16[1536,256]{1,0:T(8,128)(2,1)}, u32[]{:S(2)}, u32[]{:S(2)}) collective-permute-start(bf16[1536,256]{1,0:T(8,128)(2,1)} %copy-done.7), channel_id=1, source_target_pairs={{0,1},{1,0},{2,3},{3,2},{4,5},{5,4},{6,7},{7,6},{8,9},{9,8},{10,11... | collective-permute-start | bytes 2359304 | tf_op jit(solution)/shard_map/ppermute | solution.py:552
  94.7 40.6 %collective-permute-start.31 = (bf16[1536,256]{1,0:T(8,128)(2,1)}, bf16[1536,256]{1,0:T(8,128)(2,1)}, u32[]{:S(2)}, u32[]{:S(2)}) collective-permute-start(bf16[1536,256]{1,0:T(8,128)(2,1)} %collective-permute-done.20.refs_19_.refs_20_), channel_id=1, source_target_pairs={{0,8},{1,9},{2,0},{3,1},{4,2},{5,3},{6,4},{7,5},{14,6},{15,7},{12,... | collective-permute-start | bytes 2359304 | tf_op jit(solution)/shard_map/ppermute | solution.py:498
  95.3 40.0 %collective-permute-start.21 = (bf16[1536,256]{1,0:T(8,128)(2,1)}, bf16[1536,256]{1,0:T(8,128)(2,1)}, u32[]{:S(2)}, u32[]{:S(2)}) collective-permute-start(bf16[1536,256]{1,0:T(8,128)(2,1)} %collective-permute-done.20.refs_19_.refs_20_), channel_id=1, source_target_pairs={{0,1},{1,0},{2,3},{3,2},{4,5},{5,4},{6,7},{7,6},{8,9},{9,8},{10,11... | collective-permute-start | bytes 2359304 | tf_op jit(solution)/shard_map/ppermute | solution.py:552
  95.4 54.6 %collective-permute-start.24 = (bf16[1536,256]{1,0:T(8,128)(2,1)}, bf16[1536,256]{1,0:T(8,128)(2,1)}, u32[]{:S(2)}, u32[]{:S(2)}) collective-permute-start(bf16[1536,256]{1,0:T(8,128)(2,1)} %collective-permute-done.16.refs_15_.refs_16_), channel_id=1, source_target_pairs={{0,2},{1,3},{2,4},{3,5},{4,6},{5,7},{6,14},{7,15},{14,12},{15,13},... | collective-permute-start | bytes 2359304 | tf_op jit(solution)/shard_map/ppermute | solution.py:498
  133.2 20.6 %collective-permute-start.26 = (bf16[1536,256]{1,0:T(8,128)(2,1)}, bf16[1536,256]{1,0:T(8,128)(2,1)}, u32[]{:S(2)}, u32[]{:S(2)}) collective-permute-start(bf16[1536,256]{1,0:T(8,128)(2,1)} %collective-permute-done.22.refs_21_.refs_22_), channel_id=1, source_target_pairs={{0,8},{1,9},{2,0},{3,1},{4,2},{5,3},{6,4},{7,5},{14,6},{15,7},{12,... | collective-permute-start | bytes 2359304 | tf_op jit(solution)/shard_map/ppermute | solution.py:498
  133.2 33.0 %collective-permute-start.17 = (bf16[1536,256]{1,0:T(8,128)(2,1)}, bf16[1536,256]{1,0:T(8,128)(2,1)}, u32[]{:S(2)}, u32[]{:S(2)}) collective-permute-start(bf16[1536,256]{1,0:T(8,128)(2,1)} %collective-permute-done.16.refs_15_.refs_16_), channel_id=1, source_target_pairs={{0,1},{1,0},{2,3},{3,2},{4,5},{5,4},{6,7},{7,6},{8,9},{9,8},{10,11... | collective-permute-start | bytes 2359304 | tf_op jit(solution)/shard_map/ppermute | solution.py:552
  135.3 33.2 %collective-permute-start.23 = (bf16[1536,256]{1,0:T(8,128)(2,1)}, bf16[1536,256]{1,0:T(8,128)(2,1)}, u32[]{:S(2)}, u32[]{:S(2)}) collective-permute-start(bf16[1536,256]{1,0:T(8,128)(2,1)} %collective-permute-done.22.refs_21_.refs_22_), channel_id=1, source_target_pairs={{0,1},{1,0},{2,3},{3,2},{4,5},{5,4},{6,7},{7,6},{8,9},{9,8},{10,11... | collective-permute-start | bytes 2359304 | tf_op jit(solution)/shard_map/ppermute | solution.py:552
  135.3 34.4 %collective-permute-start.19 = (bf16[1536,256]{1,0:T(8,128)(2,1)}, bf16[1536,256]{1,0:T(8,128)(2,1)}, u32[]{:S(2)}, u32[]{:S(2)}) collective-permute-start(bf16[1536,256]{1,0:T(8,128)(2,1)} %collective-permute-done.18.refs_17_.refs_18_), channel_id=1, source_target_pairs={{0,1},{1,0},{2,3},{3,2},{4,5},{5,4},{6,7},{7,6},{8,9},{9,8},{10,11... | collective-permute-start | bytes 2359304 | tf_op jit(solution)/shard_map/ppermute | solution.py:552
  150.0 20.7 %collective-permute-start.25 = (bf16[1536,256]{1,0:T(8,128)(2,1)}, bf16[1536,256]{1,0:T(8,128)(2,1)}, u32[]{:S(2)}, u32[]{:S(2)}) collective-permute-start(bf16[1536,256]{1,0:T(8,128)(2,1)} %collective-permute-done.24.refs_23_.refs_24_), channel_id=1, source_target_pairs={{0,2},{1,3},{2,4},{3,5},{4,6},{5,7},{6,14},{7,15},{14,12},{15,13},... | collective-permute-start | bytes 2359304 | tf_op jit(solution)/shard_map/ppermute | solution.py:498
  153.8 19.4 %collective-permute-start.27 = (bf16[1536,256]{1,0:T(8,128)(2,1)}, bf16[1536,256]{1,0:T(8,128)(2,1)S(1)}, u32[]{:S(2)}, u32[]{:S(2)}) collective-permute-start(bf16[1536,256]{1,0:T(8,128)(2,1)} %collective-permute-done.26.refs_29_.refs_30_), channel_id=1, source_target_pairs={{0,8},{1,9},{2,0},{3,1},{4,2},{5,3},{6,4},{7,5},{14,6},{15,7},{12,... | collective-permute-start | bytes 2359304 | tf_op jit(solution)/shard_map/ppermute | solution.py:498
  153.9 1.2 copy-start.2
  166.2 20.5 %collective-permute-start.29 = (bf16[1536,256]{1,0:T(8,128)(2,1)}, bf16[1536,256]{1,0:T(8,128)(2,1)S(1)}, u32[]{:S(2)}, u32[]{:S(2)}) collective-permute-start(bf16[1536,256]{1,0:T(8,128)(2,1)} %collective-permute-done.18.refs_17_.refs_18_), channel_id=1, source_target_pairs={{0,2},{1,3},{2,4},{3,5},{4,6},{5,7},{6,14},{7,15},{14,12},{15,13},... | collective-permute-start | bytes 2359304 | tf_op jit(solution)/shard_map/ppermute | solution.py:498
  168.4 20.5 %collective-permute-start.15 = (bf16[192,2048]{1,0:T(8,128)(2,1)S(1)}, bf16[192,2048]{1,0:T(8,128)(2,1)}, u32[]{:S(2)}, u32[]{:S(2)}) collective-permute-start(bf16[192,2048]{1,0:T(8,128)(2,1)S(1)} %slice.13), channel_id=1, source_target_pairs={{0,16},{16,0},{1,17},{17,1},{2,18},{18,2},{3,19},{19,3},{4,20},{20... | collective-permute-start | bytes 2359304 | tf_op jit(solution)/shard_map/ppermute | solution.py:598
  169.7 19.3 %collective-permute-start.32 = (bf16[1536,256]{1,0:T(8,128)(2,1)}, bf16[1536,256]{1,0:T(8,128)(2,1)S(1)}, u32[]{:S(2)}, u32[]{:S(2)}) collective-permute-start(bf16[1536,256]{1,0:T(8,128)(2,1)} %collective-permute-done.31.refs_27_.refs_28_), channel_id=1, source_target_pairs={{0,1},{1,0},{2,3},{3,2},{4,5},{5,4},{6,7},{7,6},{8,9},{9,8},{10,11... | collective-permute-start | bytes 2359304 | tf_op jit(solution)/shard_map/ppermute | solution.py:552
  170.8 18.7 %collective-permute-start.28 = (bf16[1536,256]{1,0:T(8,128)(2,1)}, bf16[1536,256]{1,0:T(8,128)(2,1)S(1)}, u32[]{:S(2)}, u32[]{:S(2)}) collective-permute-start(bf16[1536,256]{1,0:T(8,128)(2,1)} %collective-permute-done.24.refs_23_.refs_24_), channel_id=1, source_target_pairs={{0,1},{1,0},{2,3},{3,2},{4,5},{5,4},{6,7},{7,6},{8,9},{9,8},{10,11... | collective-permute-start | bytes 2359304 | tf_op jit(solution)/shard_map/ppermute | solution.py:552
  173.3 16.2 %copy-start.9 = (bf16[1536,256]{1,0:T(8,128)(2,1)}, bf16[1536,256]{1,0:T(8,128)(2,1)S(1)}, u32[]{:S(2)}) copy-start(bf16[1536,256]{1,0:T(8,128)(2,1)S(1)} %collective-permute-done.27.refs_33_.refs_34_) | copy-start | bytes 2359300
  173.3 43.8 %collective-permute-start.14 = (bf16[320,2048]{1,0:T(8,128)(2,1)S(1)}, bf16[320,2048]{1,0:T(8,128)(2,1)}, u32[]{:S(2)}, u32[]{:S(2)}) collective-permute-start(bf16[320,2048]{1,0:T(8,128)(2,1)S(1)} %slice.12), channel_id=1, source_target_pairs={{0,16},{16,0},{1,17},{17,1},{2,18},{18,2},{3,19},{19,3},{4,20},{20... | collective-permute-start | bytes 3932168 | tf_op jit(solution)/shard_map/ppermute | solution.py:599
  186.7 6.9 %copy-start.10 = (bf16[1536,256]{1,0:T(8,128)(2,1)}, bf16[1536,256]{1,0:T(8,128)(2,1)S(1)}, u32[]{:S(2)}) copy-start(bf16[1536,256]{1,0:T(8,128)(2,1)S(1)} %collective-permute-done.29.refs_25_.refs_26_) | copy-start | bytes 2359300
  186.7 2.9 %collective-permute-start.33 = (bf16[1536,256]{1,0:T(8,128)(2,1)}, bf16[1536,256]{1,0:T(8,128)(2,1)S(1)}, u32[]{:S(2)}, u32[]{:S(2)}) collective-permute-start(bf16[1536,256]{1,0:T(8,128)(2,1)} %collective-permute-done.26.refs_29_.refs_30_), channel_id=1, source_target_pairs={{0,1},{1,0},{2,3},{3,2},{4,5},{5,4},{6,7},{7,6},{8,9},{9,8},{10,11... | collective-permute-start | bytes 2359304 | tf_op jit(solution)/shard_map/ppermute | solution.py:552
  189.0 2.3 collective-permute-start.30
  189.0 4.7 %copy-start.11 = (bf16[1536,256]{1,0:T(8,128)(2,1)}, bf16[1536,256]{1,0:T(8,128)(2,1)S(1)}, u32[]{:S(2)}) copy-start(bf16[1536,256]{1,0:T(8,128)(2,1)S(1)} %collective-permute-done.32.refs_28_.refs_29_) | copy-start | bytes 2359300
  189.0 3.4 %collective-permute-start.34 = (bf16[1536,256]{1,0:T(8,128)(2,1)}, bf16[1536,256]{1,0:T(8,128)(2,1)S(1)}, u32[]{:S(2)}, u32[]{:S(2)}) collective-permute-start(bf16[1536,256]{1,0:T(8,128)(2,1)} %collective-permute-done.25.refs_31_.refs_32_), channel_id=1, source_target_pairs={{0,1},{1,0},{2,3},{3,2},{4,5},{5,4},{6,7},{7,6},{8,9},{9,8},{10,11... | collective-permute-start | bytes 2359304 | tf_op jit(solution)/shard_map/ppermute | solution.py:552
  189.5 4.2 %copy-start.12 = (bf16[1536,256]{1,0:T(8,128)(2,1)}, bf16[1536,256]{1,0:T(8,128)(2,1)S(1)}, u32[]{:S(2)}) copy-start(bf16[1536,256]{1,0:T(8,128)(2,1)S(1)} %collective-permute-done.28.refs_24_.refs_25_) | copy-start | bytes 2359300
  189.5 4.1 %collective-permute-start.35 = (bf16[1536,256]{1,0:T(8,128)(2,1)S(1)}, bf16[1536,256]{1,0:T(8,128)(2,1)}, u32[]{:S(2)}, u32[]{:S(2)}) collective-permute-start(bf16[1536,256]{1,0:T(8,128)(2,1)S(1)} %collective-permute-done.27.refs_33_.refs_34_), channel_id=1, source_target_pairs={{0,1},{1,0},{2,3},{3,2},{4,5},{5,4},{6,7},{7,6},{8,9},{9,8},{10,11... | collective-permute-start | bytes 2359304 | tf_op jit(solution)/shard_map/ppermute | solution.py:552
  189.6 1.6 copy-start.13
  191.3 1.1 copy-start.14
  192.4 0.9 copy-start.15
  204.9 49.7 %collective-permute-start.36 = (bf16[192,2048]{1,0:T(8,128)(2,1)}, bf16[192,2048]{1,0:T(8,128)(2,1)S(1)}, u32[]{:S(2)}, u32[]{:S(2)}) collective-permute-start(bf16[192,2048]{1,0:T(8,128)(2,1)} %shard_map.190), channel_id=1, source_target_pairs={{0,16},{16,0},{1,17},{17,1},{2,18},{18,2},{3,19},{19,3},{4,20},{20... | collective-permute-start | bytes 2359304 | tf_op jit(solution)/shard_map/ppermute | solution.py:610
  231.3 23.3 %collective-permute-start.37 = (bf16[192,2048]{1,0:T(8,128)(2,1)}, bf16[192,2048]{1,0:T(8,128)(2,1)S(1)}, u32[]{:S(2)}, u32[]{:S(2)}) collective-permute-start(bf16[192,2048]{1,0:T(8,128)(2,1)} %get-tuple-element.100), channel_id=1, source_target_pairs={{0,16},{16,0},{1,17},{17,1},{2,18},{18,2},{3,19},{19,3},{4,20},{20... | collective-permute-start | bytes 2359304 | tf_op jit(solution)/shard_map/ppermute | solution.py:614
  232.6 29.2 %collective-permute-start.38 = (bf16[128,2048]{1,0:T(8,128)(2,1)}, bf16[128,2048]{1,0:T(8,128)(2,1)S(1)}, u32[]{:S(2)}, u32[]{:S(2)}) collective-permute-start(bf16[128,2048]{1,0:T(8,128)(2,1)} %get-tuple-element.104), channel_id=1, source_target_pairs={{0,16},{16,0},{1,17},{17,1},{2,18},{18,2},{3,19},{19,3},{4,20},{20... | collective-permute-start | bytes 1572872 | tf_op jit(solution)/shard_map/ppermute | solution.py:614
  254.6 0.9 copy-start.16
  254.6 1.2 copy-start.17
  261.8 0.8 copy-start.18
